TPU v7x, 512 devices: a whole 4x8x8 slice. The times are simulated.
512 devices in a mesh: ep: 128 (over z, y, core), tp: 4 (over x).
Axes of the slice: x: 4, y: 8, z: 8, core: 2. Of those that a mesh axis runs over, the one named last changes fastest.
Arguments:
- tokens: bfloat16 [2048, 1024], P('ep'), may hold values from -6 to 6
- attn_gain: float32 [1024], replicated, may hold values from 0.1 to 1.9
- q_down: bfloat16 [1024, 512], P(None, 'tp'), may hold values from -0.1875 to 0.1875
- kv_down: bfloat16 [1024, 512], P(None, 'tp'), may hold values from -0.1875 to 0.1875
- rope_down: bfloat16 [1024, 32], replicated, may hold values from -0.1875 to 0.1875
- q_latent_gain: float32 [512], replicated, may hold values from 0.1 to 1.9
- kv_latent_gain: float32 [512], replicated, may hold values from 0.1 to 1.9
- q_up: bfloat16 [512, 768], P(None, 'tp'), may hold values from -0.25 to 0.25
- query_gain: float32 [8, 96], P('tp'), may hold values from 0.4 to 48
- key_up: bfloat16 [512, 512], P(None, 'tp'), may hold values from -0.25 to 0.25
- value_up: bfloat16 [512, 512], P(None, 'tp'), may hold values from -0.25 to 0.25
- attn_out: bfloat16 [512, 1024], P('tp'), may hold values from -0.25 to 0.25
- cache_latent: bfloat16 [2048, 512, 512], P(('ep', 'tp')), may hold values from -6 to 6
- cache_rope: bfloat16 [2048, 32, 512], P(('ep', 'tp')), may hold values from -6 to 6
- lengths: int32 [2048], P('ep'), may hold values from 1 to 512, as said below
- moe_gain: float32 [1024], replicated, may hold values from 0.1 to 1.9
- route: int32 [2048, 6], P('ep'), may hold values from 0 to 127, as said below
- route_weight: float32 [2048, 6], P('ep'), may hold values from 0.1 to 1
- expert_gate: bfloat16 [128, 1024, 512], P('ep', None, 'tp'), may hold values from -0.1875 to 0.1875
- expert_up: bfloat16 [128, 1024, 512], P('ep', None, 'tp'), may hold values from -0.1875 to 0.1875
- expert_down: bfloat16 [128, 512, 1024], P('ep', 'tp'), may hold values from -0.25 to 0.25
Outputs:
- mixed_out: bfloat16 [2048, 1024], P('ep', 'tp')
- new_latent: bfloat16 [2048, 512], P('ep', 'tp')
- new_rope: bfloat16 [2048, 32], P('ep')
Inputs may be any that keep to these rules, and one draw needn't show every extreme that they name: `route`: each row names 6 different experts that lie in one group of 8 consecutive expert numbers. Among the rows of the 16 sequences of one index of ep no expert is named more than 2 times, and some expert is named exactly 2 times by the rows of every index of ep. `lengths`: some sequence has exactly 512 cached positions.
All inputs are finite; a program needn't handle non-finite values.
Results may differ from a plain program's by a relative error of at most 0.02.
Values may be sent and summed in bfloat16 or wider, within the bound.
No kernel may reach another device: no remote copies, remote signals or barrier semaphores. Data moves between devices by JAX's collectives and lax.ppermute only.
A program may use at most 64 MiB of HBM per device.

v0:
```python
import jax
import jax.numpy as jnp
from jax import lax
from jax.sharding import Mesh
from jax.sharding import PartitionSpec as P

NOPE = 64
VDIM = 64
QK = 96
EPG = 8
EP = ("ep_0", "ep_1", "ep_2")
EP_TP = ("ep_0", "ep_1", "ep_2", "tp")


EPS = 1e-06
ROPE_BASE = 10000.0


def in_one_piece(arrays, axis, dim, along):
    both = jnp.concatenate(arrays, axis=along)
    filled, at, gathered = (lax.all_gather(both, axis, axis=dim, tiled=True), 0, [])
    for a in arrays:
        gathered.append(lax.slice_in_dim(filled, at, at + a.shape[along], axis=along))
        at += a.shape[along]
    return tuple(gathered)


def sent_together(arrays, axis, split_dim, concat_dim, along):
    ends, at = ([], 0)
    for a in arrays[:-1]:
        at += a.shape[along]
        ends.append(at)
    both = jnp.concatenate(arrays, axis=along)
    return tuple(
        jnp.split(
            lax.all_to_all(both, axis, split_axis=split_dim, concat_axis=concat_dim, tiled=True),
            ends,
            axis=along,
        )
    )


def sent_to_all(shard, axis):
    size = lax.axis_size(axis)
    return lax.all_to_all(
        jnp.broadcast_to(shard[None], (size, *shard.shape)), axis, 0, 0, tiled=True
    )


def of_everyone(shard, axis):
    return sent_to_all(shard, axis).astype(jnp.float32).sum(axis=0)


def in_order(parts, dim):
    shape = list(parts.shape[1:])
    shape[dim] *= parts.shape[0]
    return jnp.moveaxis(parts, 0, dim).reshape(shape)


def gathered_copies(shard, axis, dim):
    parts = sent_to_all(shard, axis)
    return in_order(parts, dim)


def in_blocks(shard, dim, size):
    before, after = (shard.shape[:dim], shard.shape[dim + 1 :])
    return jnp.moveaxis(shard.reshape(*before, size, -1, *after), dim, 0)


def sent_and_summed(shard, axis, dim):
    parts = in_blocks(shard, dim, lax.axis_size(axis))
    arrived = lax.all_to_all(parts, axis, split_axis=0, concat_axis=0, tiled=True)
    return arrived.astype(jnp.float32).sum(axis=0)


def exchange_in_order(parts, axes, turns):
    shape = [lax.axis_size(a) for a in axes]
    parts = parts.reshape(*shape, *parts.shape[1:])
    for k in turns:
        parts = lax.all_to_all(parts, axes[k], split_axis=k, concat_axis=k, tiled=True)
    return parts.reshape(-1, *parts.shape[len(axes) :])


def core_and_chips(shard, groups, turns, split_dim, concat_dim):
    size = lax.axis_size(groups[0]) * lax.axis_size(groups[1])
    parts = in_blocks(shard, split_dim, size)
    return in_order(exchange_in_order(parts, groups, turns), concat_dim)


def rms_scaled(values_in, gain_vec):
    values_in = values_in.astype(jnp.float32)
    return (
        values_in
        * lax.rsqrt(jnp.mean(values_in * values_in, axis=-1, keepdims=True) + EPS)
        * gain_vec
    )


def rotate_last(values_in, positions):
    half_dim = values_in.shape[-1] // 2
    inverse = ROPE_BASE ** (-jnp.arange(half_dim, dtype=jnp.float32) / half_dim)
    angles = positions.astype(jnp.float32)[..., None] * inverse
    lower_half = values_in[..., :half_dim]
    upper_half = values_in[..., half_dim:]
    return jnp.concatenate(
        [
            lower_half * jnp.cos(angles) - upper_half * jnp.sin(angles),
            upper_half * jnp.cos(angles) + lower_half * jnp.sin(angles),
        ],
        -1,
    )


def rotate_rows(values_in, positions):
    half_dim = values_in.shape[1] // 2
    inverse = ROPE_BASE ** (-jnp.arange(half_dim, dtype=jnp.float32) / half_dim)
    angles = inverse[:, None] * positions.astype(jnp.float32)[None, :]
    lower_half = values_in[:, :half_dim]
    upper_half = values_in[:, half_dim:]
    return jnp.concatenate(
        [
            lower_half * jnp.cos(angles) - upper_half * jnp.sin(angles),
            upper_half * jnp.cos(angles) + lower_half * jnp.sin(angles),
        ],
        1,
    )


def shards(
    tokens,
    attn_gain,
    q_down,
    kv_down,
    rope_down,
    q_latent_gain,
    kv_latent_gain,
    q_up,
    query_gain,
    key_up,
    value_up,
    attn_out,
    cache_latent,
    cache_rope,
    lengths,
    moe_gain,
    route,
    route_weight,
    expert_gate,
    expert_up,
    expert_down,
):
    score_scale = QK ** (-0.5)
    tp_count = lax.axis_size("tp")
    tp_index = lax.axis_index("tp")
    normed = rms_scaled(tokens, attn_gain).astype(jnp.bfloat16)
    q_part = jnp.dot(normed, q_down, preferred_element_type=jnp.float32).astype(jnp.bfloat16)
    kv_part = jnp.dot(normed, kv_down, preferred_element_type=jnp.float32).astype(jnp.bfloat16)
    q_raw, kv_raw = in_one_piece((q_part, kv_part), "tp", 1, 0)
    new_rope = jnp.dot(normed, rope_down, preferred_element_type=jnp.float32).astype(jnp.bfloat16)
    q_lat = rms_scaled(q_raw, q_latent_gain).astype(jnp.bfloat16)
    latent_new = rms_scaled(kv_raw, kv_latent_gain).astype(jnp.bfloat16)
    kv_cols = kv_part.shape[1]
    new_latent = lax.dynamic_slice_in_dim(latent_new, tp_index * kv_cols, kv_cols, 1)
    heads_here = query_gain.shape[0]
    seq_count = tokens.shape[0]
    query_head = rms_scaled(
        jnp.dot(q_lat, q_up, preferred_element_type=jnp.float32).reshape(seq_count, heads_here, QK),
        query_gain,
    )
    query_head = jnp.concatenate(
        [query_head[..., :NOPE], rotate_last(query_head[..., NOPE:], lengths[:, None])], -1
    ).astype(jnp.bfloat16)
    absorbed = jnp.einsum(
        "shn,rhn->shr",
        query_head[..., :NOPE],
        key_up.reshape(-1, heads_here, NOPE),
        preferred_element_type=jnp.float32,
    ).astype(jnp.bfloat16)
    rot_query = query_head[..., NOPE:]
    absorbed_mine, rot_mine = sent_together((absorbed, rot_query), "tp", 0, 1, 2)
    seqs_mine = cache_latent.shape[0]
    first_seq = tp_index * seqs_mine
    len_mine = lax.dynamic_slice_in_dim(lengths, first_seq, seqs_mine, 0)
    latent_mine = lax.dynamic_slice_in_dim(latent_new, first_seq, seqs_mine, 0)
    key_new = rotate_last(
        lax.dynamic_slice_in_dim(new_rope, first_seq, seqs_mine, 0).astype(jnp.float32), len_mine
    ).astype(jnp.bfloat16)
    positions = jnp.arange(cache_latent.shape[1], dtype=jnp.int32)
    rotated_keys = rotate_rows(cache_rope.astype(jnp.float32), positions).astype(jnp.bfloat16)
    scores = (
        jnp.einsum("shr,sjr->shj", absorbed_mine, cache_latent, preferred_element_type=jnp.float32)
        + jnp.einsum("shp,spj->shj", rot_mine, rotated_keys, preferred_element_type=jnp.float32)
    ) * score_scale
    self_score = (
        jnp.einsum("shr,sr->sh", absorbed_mine, latent_mine, preferred_element_type=jnp.float32)
        + jnp.einsum("shp,sp->sh", rot_mine, key_new, preferred_element_type=jnp.float32)
    ) * score_scale
    valid_keys = positions[None, :] < len_mine[:, None]
    masked = jnp.where(valid_keys[:, None, :], scores, -jnp.inf)
    row_max = jnp.maximum(jnp.max(masked, axis=-1), self_score)
    weights = jnp.exp(masked - row_max[..., None])
    self_weight = jnp.exp(self_score - row_max)
    total_weight = jnp.sum(weights, axis=-1) + self_weight
    latent_sum = jnp.einsum(
        "shj,sjr->shr",
        weights.astype(jnp.bfloat16),
        cache_latent,
        preferred_element_type=jnp.float32,
    )
    latent_sum = (
        latent_sum
        + self_weight.astype(jnp.bfloat16).astype(jnp.float32)[..., None]
        * latent_mine.astype(jnp.float32)[:, None, :]
    )
    attended = (latent_sum / total_weight[..., None]).astype(jnp.bfloat16)
    attended_heads = lax.all_to_all(attended, "tp", split_axis=1, concat_axis=0, tiled=True)
    head_values = (
        jnp.einsum(
            "shr,rhv->shv",
            attended_heads,
            value_up.reshape(-1, heads_here, VDIM),
            preferred_element_type=jnp.float32,
        )
        .astype(jnp.bfloat16)
        .reshape(seq_count, heads_here * VDIM)
    )
    head_sum = of_everyone(
        jnp.dot(head_values, attn_out, preferred_element_type=jnp.float32).astype(jnp.bfloat16),
        "tp",
    ).astype(jnp.float32)
    attn_resid = (tokens.astype(jnp.float32) + head_sum).astype(jnp.bfloat16)
    moe_input = rms_scaled(attn_resid, moe_gain).astype(jnp.bfloat16)
    topk_here = route.shape[1]
    experts_all = expert_gate.shape[0] * lax.axis_size(EP)
    group_cap = min(seq_count, max(2, 2 * seq_count * EPG // experts_all))
    capacity = (topk_here * group_cap + EPG - 1) // EPG
    flat_route = route.reshape(-1)
    row_order = jnp.arange(flat_route.shape[0])
    slot_rank = jnp.sum(
        (flat_route[:, None] == flat_route[None, :]) & (row_order[None, :] < row_order[:, None]),
        axis=1,
    )
    slot_index = flat_route * capacity + slot_rank
    model_width = tokens.shape[1]
    quarter_cols = model_width // tp_count
    residual = lax.dynamic_slice_in_dim(attn_resid, tp_index * quarter_cols, quarter_cols, 1)
    own_cols = lax.dynamic_slice_in_dim(moe_input, tp_index * quarter_cols, quarter_cols, 1)
    buffer = jnp.zeros((experts_all * capacity, own_cols.shape[1]), jnp.bfloat16)
    buffer = buffer.at[slot_index].set(jnp.repeat(own_cols, topk_here, axis=0))
    arrived = lax.all_to_all(
        buffer.reshape(experts_all, capacity, own_cols.shape[1]),
        EP,
        split_axis=0,
        concat_axis=1,
        tiled=True,
    )
    piece = gathered_copies(arrived, "tp", 2)
    gate_pre = jnp.einsum("erd,edf->erf", piece, expert_gate, preferred_element_type=jnp.float32)
    up_pre = jnp.einsum("erd,edf->erf", piece, expert_up, preferred_element_type=jnp.float32)
    hidden = (jax.nn.silu(gate_pre) * up_pre).astype(jnp.bfloat16)
    partial_value = jnp.einsum(
        "erf,efd->erd", hidden, expert_down, preferred_element_type=jnp.float32
    )
    reduced = sent_and_summed(partial_value.astype(jnp.bfloat16), "tp", 2).astype(jnp.bfloat16)
    returned = core_and_chips(reduced, (("ep_0", "ep_1"), "ep_2"), (1, 0), 1, 0)
    picked = (
        returned.reshape(-1, quarter_cols)[slot_index]
        .astype(jnp.float32)
        .reshape(seq_count, topk_here, quarter_cols)
    )
    mixed_out = (
        residual.astype(jnp.float32) + jnp.sum(picked * route_weight[..., None], axis=1)
    ).astype(jnp.bfloat16)
    return (mixed_out, new_latent, new_rope)


def solution(mesh):
    torus = Mesh(mesh.devices.reshape(8, 8, 2, mesh.shape["tp"]), ("ep_0", "ep_1", "ep_2", "tp"))
    placed = (
        P(EP, None),
        P(),
        P(None, "tp"),
        P(None, "tp"),
        P(),
        P(),
        P(),
        P(None, "tp"),
        P("tp", None),
        P(None, "tp"),
        P(None, "tp"),
        P("tp", None),
        P(EP_TP, None, None),
        P(EP_TP, None, None),
        P(EP),
        P(),
        P(EP, None),
        P(EP, None),
        P(EP, None, "tp"),
        P(EP, None, "tp"),
        P(EP, "tp", None),
    )
    return jax.shard_map(
        shards,
        mesh=torus,
        in_specs=placed,
        out_specs=(P(EP, "tp"), P(EP, "tp"), P(EP, None)),
        check_vma=False,
    )
```

profile of v0, /device:TPU:1, one launch (start us, length us, event | category | flops | bytes accessed | tf_op | source)
XLA Modules:
  0.0 134.0 jit_solution(6604044920400424537)
XLA Ops:
  0.7 0.8 convert_element_type.133
  1.5 0.9 fusion.20
  2.4 1.2 convolution_convert_fusion.5
  3.6 1.2 convolution_convert_fusion.6
  4.8 9.2 %all_gather.3 = bf16[32,512]{1,0:T(8,128)(2,1)S(1)} all-gather(bf16[32,128]{1,0:T(8,128)(2,1)S(1)} %pad_maximum_fusion.1), channel_id=1, replica_groups=mesh['ep_0'=8,'ep_1'=8,'ep_2'=2,'tp'=4] {'tp'}, dimensions={1}, use_global_device_ids=true | all-gather | bytes 40960 | tf_op jit(solution)/shard_map/all_gather | solution.py:21
  14.2 1.1 fusion.42
  15.6 1.0 copy.103
  18.4 3.3 %all-to-all-start = ((bf16[16,2,544]{2,1,0:T(2,128)(2,1)}), bf16[16,2,544]{2,1,0:T(2,128)(2,1)S(1)}, u32[]{:S(2)}, u32[]{:S(2)}) async-start(bf16[16,2,544]{2,1,0:T(2,128)(2,1)} %copy.104), calls=%async_computation | async-start | bytes 81920 | tf_op jit(solution)/shard_map/all_to_all | solution.py:36
  22.5 1.1 convolution_convert_fusion.4
  28.8 4.2 %all-to-all-start.1 = ((bf16[4,8,512]{2,0,1:T(4,128)(2,1)}), bf16[4,8,512]{2,0,1:T(4,128)(2,1)S(1)}, u32[]{:S(2)}, u32[]{:S(2)}) async-start(bf16[4,8,512]{2,0,1:T(4,128)(2,1)} %copy.106), calls=%async_computation.1 | async-start | bytes 65536 | tf_op jit(solution)/shard_map/all_to_all | solution.py:216
  33.4 3.8 %all-to-all-done.1 = bf16[4,8,512]{2,0,1:T(4,128)(2,1)S(1)} async-done(((bf16[4,8,512]{2,0,1:T(4,128)(2,1)}), bf16[4,8,512]{2,0,1:T(4,128)(2,1)S(1)}, u32[]{:S(2)}, u32[]{:S(2)}) %all-to-all-start.1) | async-done | bytes 32800 | tf_op jit(solution)/shard_map/all_to_all | solution.py:216
  38.4 3.3 %all-to-all-start.2 = ((bf16[4,16,1024]{2,1,0:T(8,128)(2,1)}), bf16[4,16,1024]{2,1,0:T(8,128)(2,1)S(1)}, u32[]{:S(2)}, u32[]{:S(2)}) async-start(bf16[4,16,1024]{2,1,0:T(8,128)(2,1)} %broadcast_in_dim.20), calls=%async_computation.2 | async-start | bytes 262144 | tf_op jit(solution)/shard_map/all_to_all | solution.py:45
  41.7 0.8 dynamic-slice
  42.5 4.0 %all-to-all-done.2 = bf16[4,16,1024]{2,1,0:T(8,128)(2,1)S(1)} async-done(((bf16[4,16,1024]{2,1,0:T(8,128)(2,1)}), bf16[4,16,1024]{2,1,0:T(8,128)(2,1)S(1)}, u32[]{:S(2)}, u32[]{:S(2)}) %all-to-all-start.2) | async-done | bytes 131104 | tf_op jit(solution)/shard_map/all_to_all | solution.py:45
  47.4 1.0 scatter_custom_fusion
  48.4 35.6 %all_to_all.70 = bf16[128,2,256]{2,1,0:T(2,128)(2,1)S(1)} all-to-all(bf16[128,2,256]{2,1,0:T(2,128)(2,1)S(1)} %reshape.308), channel_id=1, replica_groups=mesh['ep_0'=8,'ep_1'=8,'ep_2'=2,'tp'=4] {'ep_0','ep_1','ep_2'}, dimensions={0} | all-to-all | bytes 262144 | tf_op jit(solution)/shard_map/all_to_all | solution.py:250
  84.3 11.6 %all_to_all.71 = bf16[4,1,256,256]{2,3,1,0:T(8,128)(2,1)S(1)} all-to-all(bf16[4,1,256,256]{2,3,1,0:T(8,128)(2,1)S(1)} %broadcast_in_dim.24), channel_id=1, replica_groups=mesh['ep_0'=8,'ep_1'=8,'ep_2'=2,'tp'=4] {'tp'}, dimensions={0} | all-to-all | bytes 1048576 | tf_op jit(solution)/shard_map/all_to_all | solution.py:45
  96.2 1.5 %convolution_convert_fusion = bf16[256,1024]{1,0:T(8,128)(2,1)S(1)} fusion(bf16[256,1024]{0,1:T(8,128)(2,1)S(1)} %bitcast.65, bf16[1,128,1024]{2,1,0:T(8,128)(2,1)S(1)} %copy-done.3, bf16[1,1024,128]{2,1,0:T(8,128)(2,1)} %param.40, f32[256,128]{1,0:T(8,128)S(1)} %fusion.10), kind=kOutput, calls=%fused_computation.2 | convolution fusion | flops 134676480 | bytes 1703936 | tf_op jit(solution)/shard_map/erf,efd->erd/dot_general | solution.py:261
  98.2 10.7 %all_to_all.72 = bf16[4,1,256,256]{3,2,1,0:T(8,128)(2,1)S(1)} all-to-all(bf16[4,1,256,256]{3,2,1,0:T(8,128)(2,1)S(1)} %bitcast.66), channel_id=1, replica_groups=mesh['ep_0'=8,'ep_1'=8,'ep_2'=2,'tp'=4] {'tp'}, dimensions={0} | all-to-all | bytes 1048576 | tf_op jit(solution)/shard_map/all_to_all | solution.py:72
  109.2 5.6 %all_to_all.73 = bf16[64,2,1,2,256]{4,3,0,2,1:T(2,128)(2,1)S(1)} all-to-all(bf16[64,2,1,2,256]{4,3,0,2,1:T(2,128)(2,1)S(1)} %copy.115), channel_id=1, replica_groups=mesh['ep_0'=8,'ep_1'=8,'ep_2'=2,'tp'=4] {'ep_2'}, dimensions={1} | all-to-all | bytes 262144 | tf_op jit(solution)/shard_map/all_to_all | solution.py:80
  115.5 4.6 %all-to-all-start.7 = ((bf16[64,2,1,2,256]{4,3,1,2,0:T(2,128)(2,1)}), bf16[64,2,1,2,256]{4,3,1,2,0:T(2,128)(2,1)S(1)}, u32[]{:S(2)}, u32[]{:S(2)}) async-start(bf16[64,2,1,2,256]{4,3,1,2,0:T(2,128)(2,1)} %copy.116), calls=%async_computation.7 | async-start | bytes 262144 | tf_op jit(solution)/shard_map/all_to_all | solution.py:80
  120.8 10.9 %all-to-all-done.7 = bf16[64,2,1,2,256]{4,3,1,2,0:T(2,128)(2,1)S(1)} async-done(((bf16[64,2,1,2,256]{4,3,1,2,0:T(2,128)(2,1)}), bf16[64,2,1,2,256]{4,3,1,2,0:T(2,128)(2,1)S(1)}, u32[]{:S(2)}, u32[]{:S(2)}) %all-to-all-start.7) | async-done | bytes 131104 | tf_op jit(solution)/shard_map/all_to_all | solution.py:80
  131.8 0.8 gather_fusion
  132.7 1.3 add_convert_fusion.1
  (103 shorter events, 13.5 us)
Async XLA Ops:
  0.6 26.0 %copy-start = (bf16[4,512,512]{2,1,0:T(8,128)(2,1)S(1)}, bf16[4,512,512]{2,1,0:T(8,128)(2,1)}, u32[]{:S(2)}) copy-start(bf16[4,512,512]{2,1,0:T(8,128)(2,1)} %param.33) | copy-start | bytes 6291460
  0.6 25.5 %copy-start.8 = (s32[16,6]{0,1:T(8,128)S(1)}, s32[16,6]{0,1:T(8,128)}, u32[]{:S(2)}) copy-start(s32[16,6]{0,1:T(8,128)} %param.37) | copy-start | bytes 1156
  0.7 25.2 %copy-start.5 = (bf16[4,32,512]{2,1,0:T(8,128)(2,1)S(1)}, bf16[4,32,512]{2,1,0:T(8,128)(2,1)}, u32[]{:S(2)}) copy-start(bf16[4,32,512]{2,1,0:T(8,128)(2,1)} %param.34) | copy-start | bytes 393220
  18.4 7.9 %all-to-all-start = ((bf16[16,2,544]{2,1,0:T(2,128)(2,1)}), bf16[16,2,544]{2,1,0:T(2,128)(2,1)S(1)}, u32[]{:S(2)}, u32[]{:S(2)}) async-start(bf16[16,2,544]{2,1,0:T(2,128)(2,1)} %copy.104), calls=%async_computation | async-start | bytes 81920 | tf_op jit(solution)/shard_map/all_to_all | solution.py:36
  23.6 0.6 copy-start.12
  26.6 6.7 %copy-start.6 = (bf16[512,128]{1,0:T(8,128)(2,1)S(1)}, bf16[512,128]{1,0:T(8,128)(2,1)}, u32[]{:S(2)}) copy-start(bf16[512,128]{1,0:T(8,128)(2,1)} %param.31) | copy-start | bytes 393220
  27.3 10.3 %copy-start.2 = (bf16[128,1024]{1,0:T(8,128)(2,1)S(1)}, bf16[128,1024]{1,0:T(8,128)(2,1)}, u32[]{:S(2)}) copy-start(bf16[128,1024]{1,0:T(8,128)(2,1)} %param.32) | copy-start | bytes 786436
  27.3 19.2 %copy-start.7 = (bf16[16,1024]{1,0:T(8,128)(2,1)S(1)}, bf16[16,1024]{1,0:T(8,128)(2,1)}, u32[]{:S(2)}) copy-start(bf16[16,1024]{1,0:T(8,128)(2,1)} %param.21) | copy-start | bytes 98308
  28.8 8.5 %all-to-all-start.1 = ((bf16[4,8,512]{2,0,1:T(4,128)(2,1)}), bf16[4,8,512]{2,0,1:T(4,128)(2,1)S(1)}, u32[]{:S(2)}, u32[]{:S(2)}) async-start(bf16[4,8,512]{2,0,1:T(4,128)(2,1)} %copy.106), calls=%async_computation.1 | async-start | bytes 65536 | tf_op jit(solution)/shard_map/all_to_all | solution.py:216
  37.5 58.3 %copy-start.1 = (bf16[1,1024,128]{2,1,0:T(8,128)(2,1)S(1)}, bf16[1,1024,128]{2,1,0:T(8,128)(2,1)}, u32[]{:S(2)}) copy-start(bf16[1,1024,128]{2,1,0:T(8,128)(2,1)} %param.39) | copy-start | bytes 786436
  38.4 8.1 %all-to-all-start.2 = ((bf16[4,16,1024]{2,1,0:T(8,128)(2,1)}), bf16[4,16,1024]{2,1,0:T(8,128)(2,1)S(1)}, u32[]{:S(2)}, u32[]{:S(2)}) async-start(bf16[4,16,1024]{2,1,0:T(8,128)(2,1)} %broadcast_in_dim.20), calls=%async_computation.2 | async-start | bytes 262144 | tf_op jit(solution)/shard_map/all_to_all | solution.py:45
  41.7 54.2 %copy-start.10 = (s32[96]{0:T(128)}, s32[96]{0:T(128)S(1)}, u32[]{:S(2)}) copy-start(s32[96]{0:T(128)S(1)} %fusion.65) | copy-start | bytes 1156
  46.5 49.7 %copy-start.3 = (bf16[1,128,1024]{2,1,0:T(8,128)(2,1)S(1)}, bf16[1,128,1024]{2,1,0:T(8,128)(2,1)}, u32[]{:S(2)}) copy-start(bf16[1,128,1024]{2,1,0:T(8,128)(2,1)} %param.41) | copy-start | bytes 786436
  46.7 0.6 copy-start.4
  98.1 22.0 %copy-start.9 = (f32[16,6]{0,1:T(8,128)S(1)}, f32[16,6]{0,1:T(8,128)}, u32[]{:S(2)}) copy-start(f32[16,6]{0,1:T(8,128)} %param.38) | copy-start | bytes 1156
  98.1 22.1 %copy-start.11 = (s32[96]{0:T(128)S(1)}, s32[96]{0:T(128)}, u32[]{:S(2)}) copy-start(s32[96]{0:T(128)} %copy-done.10) | copy-start | bytes 1156
  115.5 16.3 %all-to-all-start.7 = ((bf16[64,2,1,2,256]{4,3,1,2,0:T(2,128)(2,1)}), bf16[64,2,1,2,256]{4,3,1,2,0:T(2,128)(2,1)S(1)}, u32[]{:S(2)}, u32[]{:S(2)}) async-start(bf16[64,2,1,2,256]{4,3,1,2,0:T(2,128)(2,1)} %copy.116), calls=%async_computation.7 | async-start | bytes 262144 | tf_op jit(solution)/shard_map/all_to_all | solution.py:80
where the time goes:
time: 135 us; the launch traced here: 134 us
  blocking collectives  72.7 us (54%)
  waiting for transfers between devices  18.8 us (14%)
  starting transfers between devices  15.4 us (11%)
  local copies, waits for them, and re-layouts  9.89 us (7%)
  matrix products  8.38 us (6%)
  other arithmetic  7.84 us (6%)
    all_to_all x1, blocking collectives, shards(): lax.all_to_all(buffer.reshape(experts_all, capacity, own_cols.shape[1]),...  35.6 us
    all_to_all x1, blocking collectives, sent_to_all(): lax.all_to_all(jnp.broadcast_to(shard[None], (size, *shard.shape)), axis,...  11.6 us
    all_to_all x1, waiting for transfers between devices, exchange_in_order(): lax.all_to_all(parts, axes[k], split_axis=k, concat_axis=k, tiled=True)  10.9 us
    all_to_all x1, blocking collectives, sent_and_summed(): lax.all_to_all(parts, axis, split_axis=0, concat_axis=0, tiled=True)  10.7 us
    all_gather x1, blocking collectives, in_one_piece(): lax.all_gather(both, axis, axis=dim, tiled=True)  9.21 us
    all_to_all x1, blocking collectives, exchange_in_order(): lax.all_to_all(parts, axes[k], split_axis=k, concat_axis=k, tiled=True)  5.59 us
    all_to_all x1, starting transfers between devices, exchange_in_order(): lax.all_to_all(parts, axes[k], split_axis=k, concat_axis=k, tiled=True)  4.62 us
    all_to_all x1, starting transfers between devices, shards(): lax.all_to_all(attended, 'tp', split_axis=1, concat_axis=0, tiled=True)  4.18 us
  transfers between devices with their start and end apart: 4, of which 3 were waited for; matrix products, arithmetic and copies ran while one was open for 4% of the time, Pallas kernels for 0%

commit v1 on v0

--- a/solution.py
+++ b/solution.py
@@ -9,20 +9,15 @@
 QK = 96
 EPG = 8
 EP = ("ep_0", "ep_1", "ep_2")
+CHIPS = ("ep_0", "ep_1")
+CORE = "ep_2"
+GROUP_CAP = 2
+EXTRA = 128
 EP_TP = ("ep_0", "ep_1", "ep_2", "tp")
 
 
 EPS = 1e-06
 ROPE_BASE = 10000.0
-
-
-def in_one_piece(arrays, axis, dim, along):
-    both = jnp.concatenate(arrays, axis=along)
-    filled, at, gathered = (lax.all_gather(both, axis, axis=dim, tiled=True), 0, [])
-    for a in arrays:
-        gathered.append(lax.slice_in_dim(filled, at, at + a.shape[along], axis=along))
-        at += a.shape[along]
-    return tuple(gathered)
 
 
 def sent_together(arrays, axis, split_dim, concat_dim, along):
@@ -71,20 +66,6 @@
     parts = in_blocks(shard, dim, lax.axis_size(axis))
     arrived = lax.all_to_all(parts, axis, split_axis=0, concat_axis=0, tiled=True)
     return arrived.astype(jnp.float32).sum(axis=0)
-
-
-def exchange_in_order(parts, axes, turns):
-    shape = [lax.axis_size(a) for a in axes]
-    parts = parts.reshape(*shape, *parts.shape[1:])
-    for k in turns:
-        parts = lax.all_to_all(parts, axes[k], split_axis=k, concat_axis=k, tiled=True)
-    return parts.reshape(-1, *parts.shape[len(axes) :])
-
-
-def core_and_chips(shard, groups, turns, split_dim, concat_dim):
-    size = lax.axis_size(groups[0]) * lax.axis_size(groups[1])
-    parts = in_blocks(shard, split_dim, size)
-    return in_order(exchange_in_order(parts, groups, turns), concat_dim)
 
 
 def rms_scaled(values_in, gain_vec):
@@ -155,7 +136,8 @@
     normed = rms_scaled(tokens, attn_gain).astype(jnp.bfloat16)
     q_part = jnp.dot(normed, q_down, preferred_element_type=jnp.float32).astype(jnp.bfloat16)
     kv_part = jnp.dot(normed, kv_down, preferred_element_type=jnp.float32).astype(jnp.bfloat16)
-    q_raw, kv_raw = in_one_piece((q_part, kv_part), "tp", 1, 0)
+    both = gathered_copies(jnp.concatenate([q_part, kv_part], axis=0), "tp", 1)
+    q_raw, kv_raw = jnp.split(both, 2, axis=0)
     new_rope = jnp.dot(normed, rope_down, preferred_element_type=jnp.float32).astype(jnp.bfloat16)
     q_lat = rms_scaled(q_raw, q_latent_gain).astype(jnp.bfloat16)
     latent_new = rms_scaled(kv_raw, kv_latent_gain).astype(jnp.bfloat16)
@@ -230,47 +212,56 @@
     ).astype(jnp.float32)
     attn_resid = (tokens.astype(jnp.float32) + head_sum).astype(jnp.bfloat16)
     moe_input = rms_scaled(attn_resid, moe_gain).astype(jnp.bfloat16)
-    topk_here = route.shape[1]
-    experts_all = expert_gate.shape[0] * lax.axis_size(EP)
-    group_cap = min(seq_count, max(2, 2 * seq_count * EPG // experts_all))
-    capacity = (topk_here * group_cap + EPG - 1) // EPG
-    flat_route = route.reshape(-1)
-    row_order = jnp.arange(flat_route.shape[0])
-    slot_rank = jnp.sum(
-        (flat_route[:, None] == flat_route[None, :]) & (row_order[None, :] < row_order[:, None]),
-        axis=1,
-    )
-    slot_index = flat_route * capacity + slot_rank
-    model_width = tokens.shape[1]
-    quarter_cols = model_width // tp_count
+    group_of = route[:, 0] // EPG
+    order = jnp.arange(seq_count, dtype=jnp.int32)
+    earlier = (group_of[:, None] == group_of[None, :]) & (order[None, :] < order[:, None])
+    slot = group_of * GROUP_CAP + jnp.sum(earlier, axis=1, dtype=jnp.int32)
+    chips = lax.axis_size(CHIPS)
+    cores = lax.axis_size(CORE)
+    chips_in_group = EPG // cores
+    slots = chips // chips_in_group * GROUP_CAP
+    placing = (jnp.arange(slots, dtype=jnp.int32)[:, None] == slot[None, :]).astype(jnp.bfloat16)
+    lane = jnp.arange(EXTRA, dtype=jnp.int32)
+    named = (route % EPG)[:, :, None] == lane[None, None, :]
+    weight_cols = jnp.sum(jnp.where(named, route_weight[..., None], 0.0), axis=1).astype(jnp.bfloat16)
+    width = tokens.shape[1]
+    rows = jnp.concatenate([moe_input, weight_cols], axis=1)
+    packed = jnp.dot(placing, rows, preferred_element_type=jnp.float32).astype(jnp.bfloat16)
+    packed = jnp.broadcast_to(
+        packed.reshape(-1, 1, GROUP_CAP, width + EXTRA),
+        (slots // GROUP_CAP, chips_in_group, GROUP_CAP, width + EXTRA),
+    ).reshape(chips, GROUP_CAP, width + EXTRA)
+    arrived = lax.all_to_all(packed, CHIPS, 0, 0, tiled=True).reshape(-1, width + EXTRA)
+    swap = [(i, cores - 1 - i) for i in range(cores)]
+    other = lax.ppermute(arrived, CORE, swap)
+    expert_here = lax.axis_index(EP) % EPG
+    mine = lane == expert_here
+
+    def expert(block):
+        inside = block[:, :width]
+        gate_pre = jnp.dot(inside, expert_gate[0], preferred_element_type=jnp.float32)
+        up_pre = jnp.dot(inside, expert_up[0], preferred_element_type=jnp.float32)
+        hidden = (jax.nn.silu(gate_pre) * up_pre).astype(jnp.bfloat16)
+        scale = jnp.sum(
+            jnp.where(mine, block[:, width:].astype(jnp.float32), 0.0), axis=1, keepdims=True
+        )
+        return jnp.dot(hidden, expert_down[0], preferred_element_type=jnp.float32) * scale
+
+    own = expert(arrived)
+    back = lax.ppermute(expert(other).astype(jnp.bfloat16), CORE, swap)
+    sums = (own + back.astype(jnp.float32)).astype(jnp.bfloat16)
+    returned = lax.all_to_all(
+        sums.reshape(chips, GROUP_CAP, width), CHIPS, 0, 0, tiled=True
+    ).reshape(-1, chips_in_group, GROUP_CAP, width)
+    totals = jnp.sum(returned.astype(jnp.float32), axis=1).astype(jnp.bfloat16)
+    picked = jnp.dot(
+        placing.T, totals.reshape(slots, width), preferred_element_type=jnp.float32
+    ).astype(jnp.bfloat16)
+    quarter_cols = width // tp_count
     residual = lax.dynamic_slice_in_dim(attn_resid, tp_index * quarter_cols, quarter_cols, 1)
-    own_cols = lax.dynamic_slice_in_dim(moe_input, tp_index * quarter_cols, quarter_cols, 1)
-    buffer = jnp.zeros((experts_all * capacity, own_cols.shape[1]), jnp.bfloat16)
-    buffer = buffer.at[slot_index].set(jnp.repeat(own_cols, topk_here, axis=0))
-    arrived = lax.all_to_all(
-        buffer.reshape(experts_all, capacity, own_cols.shape[1]),
-        EP,
-        split_axis=0,
-        concat_axis=1,
-        tiled=True,
-    )
-    piece = gathered_copies(arrived, "tp", 2)
-    gate_pre = jnp.einsum("erd,edf->erf", piece, expert_gate, preferred_element_type=jnp.float32)
-    up_pre = jnp.einsum("erd,edf->erf", piece, expert_up, preferred_element_type=jnp.float32)
-    hidden = (jax.nn.silu(gate_pre) * up_pre).astype(jnp.bfloat16)
-    partial_value = jnp.einsum(
-        "erf,efd->erd", hidden, expert_down, preferred_element_type=jnp.float32
-    )
-    reduced = sent_and_summed(partial_value.astype(jnp.bfloat16), "tp", 2).astype(jnp.bfloat16)
-    returned = core_and_chips(reduced, (("ep_0", "ep_1"), "ep_2"), (1, 0), 1, 0)
-    picked = (
-        returned.reshape(-1, quarter_cols)[slot_index]
-        .astype(jnp.float32)
-        .reshape(seq_count, topk_here, quarter_cols)
-    )
-    mixed_out = (
-        residual.astype(jnp.float32) + jnp.sum(picked * route_weight[..., None], axis=1)
-    ).astype(jnp.bfloat16)
+    mixed_out = (residual.astype(jnp.float32) + sent_and_summed(picked, "tp", 1)).astype(
+        jnp.bfloat16
+    )
     return (mixed_out, new_latent, new_rope)
 
 

time: 135 us -> 123 us (0.911)
  the two profiles are of different devices: /device:TPU:1 before, /device:TPU:8 now
where the time goes in v1:
time: 123 us; the launch traced here: 122 us
  waiting for transfers between devices  38.5 us (31%)
  blocking collectives  29.7 us (24%)
  starting transfers between devices  27.9 us (23%)
  matrix products  9.81 us (8%)
  other arithmetic  8.98 us (7%)
  local copies, waits for them, and re-layouts  6.31 us (5%)
    all_to_all x1, blocking collectives, shards(): lax.all_to_all(packed, CHIPS, 0, 0, tiled=True).reshape(-1, width + EXTRA)  29.7 us
    all_to_all x1, waiting for transfers between devices, shards(): lax.all_to_all(sums.reshape(chips, GROUP_CAP, width), CHIPS, 0, 0, tiled=...  15 us
    all_to_all x2, starting transfers between devices, sent_to_all(): lax.all_to_all(jnp.broadcast_to(shard[None], (size, *shard.shape)), axis,...  7.62 us
    all_to_all x2, waiting for transfers between devices, sent_to_all(): lax.all_to_all(jnp.broadcast_to(shard[None], (size, *shard.shape)), axis,...  5.84 us
    all_to_all x1, waiting for transfers between devices, sent_together(): lax.all_to_all(both, axis, split_axis=split_dim, concat_axis=concat_dim,...  5.4 us
    all_to_all x1, starting transfers between devices, shards(): lax.all_to_all(sums.reshape(chips, GROUP_CAP, width), CHIPS, 0, 0, tiled=...  5.02 us
    all_to_all x1, waiting for transfers between devices, sent_and_summed(): lax.all_to_all(parts, axis, split_axis=0, concat_axis=0, tiled=True)  4.81 us
    all_to_all x1, starting transfers between devices, sent_together(): lax.all_to_all(both, axis, split_axis=split_dim, concat_axis=concat_dim,...  4.79 us
  transfers between devices with their start and end apart: 8, of which 7 were waited for; matrix products, arithmetic and copies ran while one was open for 7% of the time, Pallas kernels for 0%

profile of v1, /device:TPU:8, one launch (start us, length us, event | category | flops | bytes accessed | tf_op | source)
XLA Modules:
  0.0 122.3 jit_solution(9221821594958431730)
XLA Ops:
  0.7 1.0 fusion.31
  1.7 1.2 convolution_convert_fusion.6
  2.9 1.2 convolution_convert_fusion.7
  4.7 4.3 %all-to-all-start = ((bf16[4,32,128]{2,1,0:T(8,128)(2,1)}), bf16[4,32,128]{2,1,0:T(8,128)(2,1)S(1)}, u32[]{:S(2)}, u32[]{:S(2)}) async-start(bf16[4,32,128]{2,1,0:T(8,128)(2,1)} %broadcast_in_dim.37), calls=%async_computation | async-start | bytes 65536 | tf_op jit(solution)/shard_map/all_to_all | solution.py:40
  12.9 0.9 convert_element_type.165
  13.9 1.1 convolution_convert_fusion.5
  15.4 1.0 copy.60
  17.9 4.8 %all-to-all-start.1 = ((bf16[16,2,544]{2,1,0:T(2,128)(2,1)}), bf16[16,2,544]{2,1,0:T(2,128)(2,1)S(1)}, u32[]{:S(2)}, u32[]{:S(2)}) async-start(bf16[16,2,544]{2,1,0:T(2,128)(2,1)} %copy.61), calls=%async_computation.1 | async-start | bytes 81920 | tf_op jit(solution)/shard_map/all_to_all | solution.py:31
  22.8 5.4 %all-to-all-done.1 = bf16[16,2,544]{2,1,0:T(2,128)(2,1)S(1)} async-done(((bf16[16,2,544]{2,1,0:T(2,128)(2,1)}), bf16[16,2,544]{2,1,0:T(2,128)(2,1)S(1)}, u32[]{:S(2)}, u32[]{:S(2)}) %all-to-all-start.1) | async-done | bytes 34848 | tf_op jit(solution)/shard_map/all_to_all | solution.py:31
  30.7 3.3 %all-to-all-start.2 = ((bf16[4,8,512]{2,0,1:T(4,128)(2,1)}), bf16[4,8,512]{2,0,1:T(4,128)(2,1)S(1)}, u32[]{:S(2)}, u32[]{:S(2)}) async-start(bf16[4,8,512]{2,0,1:T(4,128)(2,1)} %copy.64), calls=%async_computation.2 | async-start | bytes 65536 | tf_op jit(solution)/shard_map/all_to_all | solution.py:198
  34.8 4.6 %all-to-all-done.2 = bf16[4,8,512]{2,0,1:T(4,128)(2,1)S(1)} async-done(((bf16[4,8,512]{2,0,1:T(4,128)(2,1)}), bf16[4,8,512]{2,0,1:T(4,128)(2,1)S(1)}, u32[]{:S(2)}, u32[]{:S(2)}) %all-to-all-start.2) | async-done | bytes 32800 | tf_op jit(solution)/shard_map/all_to_all | solution.py:198
  40.5 3.3 %all-to-all-start.3 = ((bf16[4,16,1024]{2,1,0:T(8,128)(2,1)}), bf16[4,16,1024]{2,1,0:T(8,128)(2,1)S(1)}, u32[]{:S(2)}, u32[]{:S(2)}) async-start(bf16[4,16,1024]{2,1,0:T(8,128)(2,1)} %broadcast_in_dim.39), calls=%async_computation.3 | async-start | bytes 262144 | tf_op jit(solution)/shard_map/all_to_all | solution.py:40
  43.9 5.8 %all-to-all-done.3 = bf16[4,16,1024]{2,1,0:T(8,128)(2,1)S(1)} async-done(((bf16[4,16,1024]{2,1,0:T(8,128)(2,1)}), bf16[4,16,1024]{2,1,0:T(8,128)(2,1)S(1)}, u32[]{:S(2)}, u32[]{:S(2)}) %all-to-all-start.3) | async-done | bytes 131104 | tf_op jit(solution)/shard_map/all_to_all | solution.py:40
  50.4 29.7 %all_to_all.61 = bf16[64,2,1152]{2,1,0:T(2,128)(2,1)S(1)} all-to-all(bf16[64,2,1152]{2,1,0:T(2,128)(2,1)S(1)} %bitcast.97), channel_id=1, replica_groups=mesh['ep_0'=8,'ep_1'=8,'ep_2'=2,'tp'=4] {'ep_0','ep_1'}, dimensions={0} | all-to-all | bytes 589824 | tf_op jit(solution)/shard_map/all_to_all | solution.py:234
  80.2 1.9 %collective-permute-start = (bf16[128,1152]{1,0:T(8,128)(2,1)S(1)}, bf16[128,1152]{1,0:T(8,128)(2,1)S(1)}, u32[]{:S(2)}, u32[]{:S(2)}) collective-permute-start(bf16[128,1152]{1,0:T(8,128)(2,1)S(1)} %reshape.304), channel_id=1, source_target_pairs={{0,4},{4,0},{1,5},{5,1},{2,6},{6,2},{3,7},{7,3},{8,12},{12,8},{9,1... | collective-permute-start | bytes 884744 | tf_op jit(solution)/shard_map/ppermute | solution.py:236
  82.1 1.5 %collective-permute-done = bf16[128,1152]{1,0:T(8,128)(2,1)S(1)} collective-permute-done((bf16[128,1152]{1,0:T(8,128)(2,1)S(1)}, bf16[128,1152]{1,0:T(8,128)(2,1)S(1)}, u32[]{:S(2)}, u32[]{:S(2)}) %collective-permute-start) | collective-permute-done | bytes 294944 | tf_op jit(solution)/shard_map/ppermute | solution.py:236
  84.0 2.0 %multiply_convert_fusion = bf16[128,1024]{1,0:T(8,128)(2,1)} fusion(f32[128]{0:T(128)S(1)} %get-tuple-element.6, bf16[1,128,1024]{2,1,0:T(8,128)(2,1)} %param.41, f32[128,128]{1,0:T(8,128)S(1)} %fusion.12, bf16[1,1024,128]{2,1,0:T(8,128)(2,1)S(1)} %copy-done.2, bf16[128,1152]{1,0:T(8,128)(2,1)S(1)} %collective-permute-done), kind=kOutput, calls=%fused_computation.20 | convolution fusion | flops 67469312 | bytes 1114624 | tf_op jit(solution)/shard_map/dot_general | solution.py:248
  86.0 2.0 %collective-permute-start.1 = (bf16[128,1024]{1,0:T(8,128)(2,1)}, bf16[128,1024]{1,0:T(8,128)(2,1)S(1)}, u32[]{:S(2)}, u32[]{:S(2)}) collective-permute-start(bf16[128,1024]{1,0:T(8,128)(2,1)} %multiply_convert_fusion), channel_id=1, source_target_pairs={{0,4},{4,0},{1,5},{5,1},{2,6},{6,2},{3,7},{7,3},{8,12},{12,8},{9,1... | collective-permute-start | bytes 786440 | tf_op jit(solution)/shard_map/ppermute | solution.py:251
  88.3 1.4 %collective-permute-done.1 = bf16[128,1024]{1,0:T(8,128)(2,1)S(1)} collective-permute-done((bf16[128,1024]{1,0:T(8,128)(2,1)}, bf16[128,1024]{1,0:T(8,128)(2,1)S(1)}, u32[]{:S(2)}, u32[]{:S(2)}) %collective-permute-start.1) | collective-permute-done | bytes 262176 | tf_op jit(solution)/shard_map/ppermute | solution.py:251
  89.7 1.3 %add_convert_fusion = bf16[128,1024]{1,0:T(8,128)(2,1)S(1)} fusion(bf16[128,1024]{1,0:T(8,128)(2,1)S(1)} %collective-permute-done.1, bf16[1,128,1024]{2,1,0:T(8,128)(2,1)} %param.41, bf16[1,1024,128]{2,1,0:T(8,128)(2,1)S(1)} %copy-done.3, f32[128]{0:T(128)S(1)} %get-tuple-element.5, bf16[128,1152]{1,0:T(8,128)(2,1)S(1)} %reshape.304, f32[128,128]{1,0:T(8,128)S(1)} %fusion.18), kind=kOutput, calls=%fused_computation.19 | convolution fusion | flops 67731456 | bytes 1376768 | tf_op jit(solution)/shard_map/dot_general | solution.py:248
  91.8 5.0 %all-to-all-start.5 = ((bf16[64,2,1024]{2,1,0:T(2,128)(2,1)}), bf16[64,2,1024]{2,1,0:T(2,128)(2,1)S(1)}, u32[]{:S(2)}, u32[]{:S(2)}) async-start(bf16[64,2,1024]{2,1,0:T(2,128)(2,1)} %reshape.305), calls=%async_computation.5 | async-start | bytes 524288 | tf_op jit(solution)/shard_map/all_to_all | solution.py:253
  96.8 15.0 %all-to-all-done.5 = bf16[64,2,1024]{2,1,0:T(2,128)(2,1)S(1)} async-done(((bf16[64,2,1024]{2,1,0:T(2,128)(2,1)}), bf16[64,2,1024]{2,1,0:T(2,128)(2,1)S(1)}, u32[]{:S(2)}, u32[]{:S(2)}) %all-to-all-start.5) | async-done | bytes 262176 | tf_op jit(solution)/shard_map/all_to_all | solution.py:253
  112.9 3.3 %all-to-all-start.6 = ((bf16[4,16,256]{2,1,0:T(8,128)(2,1)}), bf16[4,16,256]{2,1,0:T(8,128)(2,1)S(1)}, u32[]{:S(2)}, u32[]{:S(2)}) async-start(bf16[4,16,256]{2,1,0:T(8,128)(2,1)} %bitcast.95), calls=%async_computation.6 | async-start | bytes 65536 | tf_op jit(solution)/shard_map/all_to_all | solution.py:67
  116.8 4.8 %all-to-all-done.6 = bf16[4,16,256]{2,1,0:T(8,128)(2,1)S(1)} async-done(((bf16[4,16,256]{2,1,0:T(8,128)(2,1)}), bf16[4,16,256]{2,1,0:T(8,128)(2,1)S(1)}, u32[]{:S(2)}, u32[]{:S(2)}) %all-to-all-start.6) | async-done | bytes 32800 | tf_op jit(solution)/shard_map/all_to_all | solution.py:67
  (100 shorter events, 15.3 us)
Async XLA Ops:
  0.6 27.7 %copy-start = (bf16[4,512,512]{2,1,0:T(8,128)(2,1)S(1)}, bf16[4,512,512]{2,1,0:T(8,128)(2,1)}, u32[]{:S(2)}) copy-start(bf16[4,512,512]{2,1,0:T(8,128)(2,1)} %param.33) | copy-start | bytes 6291460
  0.6 15.9 %copy-start.9 = (f32[512]{0:T(512)S(1)}, f32[512]{0:T(512)}, u32[]{:S(2)}) copy-start(f32[512]{0:T(512)} %param.26) | copy-start | bytes 6148
  0.7 16.0 %copy-start.4 = (bf16[512,192]{0,1:T(8,128)(2,1)S(1)}, bf16[512,192]{0,1:T(8,128)(2,1)}, u32[]{:S(2)}) copy-start(bf16[512,192]{0,1:T(8,128)(2,1)} %param.28) | copy-start | bytes 589828
  0.7 16.2 %copy-start.11 = (f32[2,96]{1,0:T(2,128)S(1)}, f32[2,96]{1,0:T(2,128)}, u32[]{:S(2)}) copy-start(f32[2,96]{1,0:T(2,128)} %param.29) | copy-start | bytes 2308
  0.7 22.1 %copy-start.10 = (f32[512]{0:T(512)S(1)}, f32[512]{0:T(512)}, u32[]{:S(2)}) copy-start(f32[512]{0:T(512)} %param.27) | copy-start | bytes 6148
  4.7 11.6 %all-to-all-start = ((bf16[4,32,128]{2,1,0:T(8,128)(2,1)}), bf16[4,32,128]{2,1,0:T(8,128)(2,1)S(1)}, u32[]{:S(2)}, u32[]{:S(2)}) async-start(bf16[4,32,128]{2,1,0:T(8,128)(2,1)} %broadcast_in_dim.37), calls=%async_computation | async-start | bytes 65536 | tf_op jit(solution)/shard_map/all_to_all | solution.py:40
  14.9 14.3 %copy-start.12 = (bf16[16,32]{1,0:T(8,128)(2,1)}, bf16[16,32]{1,0:T(8,128)(2,1)S(1)}, u32[]{:S(2)}) copy-start(bf16[16,32]{1,0:T(8,128)(2,1)S(1)} %convolution_convert_fusion.5) | copy-start | bytes 3076
  17.9 10.3 %all-to-all-start.1 = ((bf16[16,2,544]{2,1,0:T(2,128)(2,1)}), bf16[16,2,544]{2,1,0:T(2,128)(2,1)S(1)}, u32[]{:S(2)}, u32[]{:S(2)}) async-start(bf16[16,2,544]{2,1,0:T(2,128)(2,1)} %copy.61), calls=%async_computation.1 | async-start | bytes 81920 | tf_op jit(solution)/shard_map/all_to_all | solution.py:31
  28.3 6.4 %copy-start.5 = (bf16[512,128]{1,0:T(8,128)(2,1)S(1)}, bf16[512,128]{1,0:T(8,128)(2,1)}, u32[]{:S(2)}) copy-start(bf16[512,128]{1,0:T(8,128)(2,1)} %param.31) | copy-start | bytes 393220
  29.0 10.7 %copy-start.1 = (bf16[128,1024]{1,0:T(8,128)(2,1)S(1)}, bf16[128,1024]{1,0:T(8,128)(2,1)}, u32[]{:S(2)}) copy-start(bf16[128,1024]{1,0:T(8,128)(2,1)} %param.32) | copy-start | bytes 786436
  29.0 14.9 %copy-start.7 = (f32[16,6]{0,1:T(8,128)S(1)}, f32[16,6]{0,1:T(8,128)}, u32[]{:S(2)}) copy-start(f32[16,6]{0,1:T(8,128)} %param.38) | copy-start | bytes 1156
  29.2 20.6 %copy-start.6 = (bf16[16,1024]{1,0:T(8,128)(2,1)S(1)}, bf16[16,1024]{1,0:T(8,128)(2,1)}, u32[]{:S(2)}) copy-start(bf16[16,1024]{1,0:T(8,128)(2,1)} %param.21) | copy-start | bytes 98308
  29.5 20.5 %copy-start.8 = (f32[1024]{0:T(1024)S(1)}, f32[1024]{0:T(1024)}, u32[]{:S(2)}) copy-start(f32[1024]{0:T(1024)} %param.36) | copy-start | bytes 12292
  30.1 53.6 %copy-start.3 = (bf16[1,1024,128]{2,1,0:T(8,128)(2,1)S(1)}, bf16[1,1024,128]{2,1,0:T(8,128)(2,1)}, u32[]{:S(2)}) copy-start(bf16[1,1024,128]{2,1,0:T(8,128)(2,1)} %param.40) | copy-start | bytes 786436
  30.7 8.7 %all-to-all-start.2 = ((bf16[4,8,512]{2,0,1:T(4,128)(2,1)}), bf16[4,8,512]{2,0,1:T(4,128)(2,1)S(1)}, u32[]{:S(2)}, u32[]{:S(2)}) async-start(bf16[4,8,512]{2,0,1:T(4,128)(2,1)} %copy.64), calls=%async_computation.2 | async-start | bytes 65536 | tf_op jit(solution)/shard_map/all_to_all | solution.py:198
  34.7 49.3 %copy-start.2 = (bf16[1,1024,128]{2,1,0:T(8,128)(2,1)S(1)}, bf16[1,1024,128]{2,1,0:T(8,128)(2,1)}, u32[]{:S(2)}) copy-start(bf16[1,1024,128]{2,1,0:T(8,128)(2,1)} %param.39) | copy-start | bytes 786436
  40.5 9.3 %all-to-all-start.3 = ((bf16[4,16,1024]{2,1,0:T(8,128)(2,1)}), bf16[4,16,1024]{2,1,0:T(8,128)(2,1)S(1)}, u32[]{:S(2)}, u32[]{:S(2)}) async-start(bf16[4,16,1024]{2,1,0:T(8,128)(2,1)} %broadcast_in_dim.39), calls=%async_computation.3 | async-start | bytes 262144 | tf_op jit(solution)/shard_map/all_to_all | solution.py:40
  80.2 3.5 %collective-permute-start = (bf16[128,1152]{1,0:T(8,128)(2,1)S(1)}, bf16[128,1152]{1,0:T(8,128)(2,1)S(1)}, u32[]{:S(2)}, u32[]{:S(2)}) collective-permute-start(bf16[128,1152]{1,0:T(8,128)(2,1)S(1)} %reshape.304), channel_id=1, source_target_pairs={{0,4},{4,0},{1,5},{5,1},{2,6},{6,2},{3,7},{7,3},{8,12},{12,8},{9,1... | collective-permute-start | bytes 884744 | tf_op jit(solution)/shard_map/ppermute | solution.py:236
  86.0 3.6 %collective-permute-start.1 = (bf16[128,1024]{1,0:T(8,128)(2,1)}, bf16[128,1024]{1,0:T(8,128)(2,1)S(1)}, u32[]{:S(2)}, u32[]{:S(2)}) collective-permute-start(bf16[128,1024]{1,0:T(8,128)(2,1)} %multiply_convert_fusion), channel_id=1, source_target_pairs={{0,4},{4,0},{1,5},{5,1},{2,6},{6,2},{3,7},{7,3},{8,12},{12,8},{9,1... | collective-permute-start | bytes 786440 | tf_op jit(solution)/shard_map/ppermute | solution.py:251
  91.8 20.0 %all-to-all-start.5 = ((bf16[64,2,1024]{2,1,0:T(2,128)(2,1)}), bf16[64,2,1024]{2,1,0:T(2,128)(2,1)S(1)}, u32[]{:S(2)}, u32[]{:S(2)}) async-start(bf16[64,2,1024]{2,1,0:T(2,128)(2,1)} %reshape.305), calls=%async_computation.5 | async-start | bytes 524288 | tf_op jit(solution)/shard_map/all_to_all | solution.py:253
  112.9 8.7 %all-to-all-start.6 = ((bf16[4,16,256]{2,1,0:T(8,128)(2,1)}), bf16[4,16,256]{2,1,0:T(8,128)(2,1)S(1)}, u32[]{:S(2)}, u32[]{:S(2)}) async-start(bf16[4,16,256]{2,1,0:T(8,128)(2,1)} %bitcast.95), calls=%async_computation.6 | async-start | bytes 65536 | tf_op jit(solution)/shard_map/all_to_all | solution.py:67

commit v2 on v1

v2 whole, which is shorter than its diff:
```python
import jax
import jax.numpy as jnp
from jax import lax
from jax.experimental import pallas as pl
from jax.sharding import Mesh
from jax.sharding import PartitionSpec as P

NOPE = 64
VDIM = 64
QK = 96
EPG = 8
EP = ("ep_0", "ep_1", "ep_2")
CHIPS = ("ep_0", "ep_1")
CORE = "ep_2"
GROUP_CAP = 2
EXTRA = 128
EP_TP = ("ep_0", "ep_1", "ep_2", "tp")


EPS = 1e-06
ROPE_BASE = 10000.0


def rms_scaled(values_in, gain_vec):
    values_in = values_in.astype(jnp.float32)
    return (
        values_in
        * lax.rsqrt(jnp.mean(values_in * values_in, axis=-1, keepdims=True) + EPS)
        * gain_vec
    )


def rotate_last(values_in, positions):
    half_dim = values_in.shape[-1] // 2
    inverse = ROPE_BASE ** (-jnp.arange(half_dim, dtype=jnp.float32) / half_dim)
    angles = positions.astype(jnp.float32)[..., None] * inverse
    lower_half = values_in[..., :half_dim]
    upper_half = values_in[..., half_dim:]
    return jnp.concatenate(
        [
            lower_half * jnp.cos(angles) - upper_half * jnp.sin(angles),
            upper_half * jnp.cos(angles) + lower_half * jnp.sin(angles),
        ],
        -1,
    )


def rotate_rows(values_in, positions):
    half_dim = values_in.shape[1] // 2
    inverse = ROPE_BASE ** (-jnp.arange(half_dim, dtype=jnp.float32) / half_dim)
    angles = inverse[:, None] * positions.astype(jnp.float32)[None, :]
    lower_half = values_in[:, :half_dim]
    upper_half = values_in[:, half_dim:]
    return jnp.concatenate(
        [
            lower_half * jnp.cos(angles) - upper_half * jnp.sin(angles),
            upper_half * jnp.cos(angles) + lower_half * jnp.sin(angles),
        ],
        1,
    )


F32 = jnp.float32
BF16 = jnp.bfloat16
NEG = -1e30


def dot(a, b):
    return jnp.dot(a, b, preferred_element_type=F32)


def dot_t(a, b):
    return lax.dot_general(a, b, (((1,), (1,)), ((), ())), preferred_element_type=F32)


def run(body, outs, *args, flops=2_000_000):
    moved = sum(a.size * a.dtype.itemsize for a in args)
    return pl.pallas_call(
        body,
        out_shape=outs,
        cost_estimate=pl.CostEstimate(flops=flops, transcendentals=0, bytes_accessed=moved),
    )(*args)


def down_body(tok_ref, gain_ref, q_ref, kv_ref, rope_ref, both_ref, new_rope_ref):
    normed = rms_scaled(tok_ref[...], gain_ref[...]).astype(BF16)
    rows = normed.shape[0]
    q_part = dot(normed, q_ref[...]).astype(BF16)
    kv_part = dot(normed, kv_ref[...]).astype(BF16)
    for i in range(both_ref.shape[0]):
        both_ref[i, :rows, :] = q_part
        both_ref[i, rows:, :] = kv_part
    new_rope_ref[...] = dot(normed, rope_ref[...]).astype(BF16)


def query_body(
    arr_ref, q_gain_ref, kv_gain_ref, q_up_ref, head_gain_ref, key_up_ref, cos_ref, sin_ref,
    send_ref, latent_ref,
):
    peers, both, _ = arr_ref.shape
    rows = both // 2
    rank = key_up_ref.shape[0]
    half = cos_ref.shape[1]
    q_raw = jnp.concatenate([arr_ref[i, :rows, :] for i in range(peers)], axis=1)
    kv_raw = jnp.concatenate([arr_ref[i, rows:, :] for i in range(peers)], axis=1)
    latent_ref[...] = rms_scaled(kv_raw, kv_gain_ref[...]).astype(BF16)
    q_lat = rms_scaled(q_raw, q_gain_ref[...]).astype(BF16)
    query = dot(q_lat, q_up_ref[...])
    each = rows // peers
    for h in range(head_gain_ref.shape[0]):
        one = rms_scaled(query[:, h * QK : (h + 1) * QK], head_gain_ref[h : h + 1, :])
        lower = one[:, NOPE : NOPE + half]
        upper = one[:, NOPE + half :]
        turned = jnp.concatenate(
            [
                lower * cos_ref[...] - upper * sin_ref[...],
                upper * cos_ref[...] + lower * sin_ref[...],
            ],
            axis=1,
        )
        absorbed = dot_t(one[:, :NOPE].astype(BF16), key_up_ref[:, h * NOPE : (h + 1) * NOPE])
        for i in range(peers):
            at = slice(h * each, (h + 1) * each)
            send_ref[i, at, :rank] = absorbed[i * each : (i + 1) * each].astype(BF16)
            send_ref[i, at, rank:] = turned[i * each : (i + 1) * each].astype(BF16)


def attend_body(arr_ref, cache_ref, keys_ref, latent_ref, key_new_ref, len_ref, out_ref):
    seqs, places, rank = cache_ref.shape
    peers, each, _ = arr_ref.shape
    rows = peers * each
    arrived = arr_ref[...].reshape(rows, arr_ref.shape[2])
    absorbed = arrived[:, :rank]
    turned = arrived[:, rank:]
    scale = QK ** (-0.5)
    row_seq = lax.broadcasted_iota(jnp.int32, (rows, 1), 0) % seqs
    scores = jnp.zeros((rows, places), F32)
    for s in range(seqs):
        part = dot_t(absorbed, cache_ref[s]) + dot(turned, keys_ref[s])
        scores = jnp.where(row_seq == s, part, scores)
    spread = rows // seqs
    latent = jnp.concatenate([latent_ref[...].astype(F32)] * spread, axis=0)
    key_new = jnp.concatenate([key_new_ref[...].astype(F32)] * spread, axis=0)
    self_score = (
        jnp.sum(absorbed.astype(F32) * latent, axis=1, keepdims=True)
        + jnp.sum(turned.astype(F32) * key_new, axis=1, keepdims=True)
    ) * scale
    place = lax.broadcasted_iota(jnp.int32, (rows, places), 1)
    valid = place < len_ref[...]
    scores = jnp.where(valid, scores * scale, NEG)
    top = jnp.maximum(jnp.max(scores, axis=1, keepdims=True), self_score)
    weights = jnp.where(valid, jnp.exp(scores - top), 0.0)
    self_weight = jnp.exp(self_score - top)
    total = jnp.sum(weights, axis=1, keepdims=True) + self_weight
    summed = self_weight.astype(BF16).astype(F32) * latent
    for s in range(seqs):
        summed = summed + dot(jnp.where(row_seq == s, weights, 0.0).astype(BF16), cache_ref[s])
    out_ref[...] = (summed / total).astype(BF16).reshape(out_ref.shape)


def heads_body(arr_ref, value_ref, out_w_ref, out_ref):
    peers, each, rank = arr_ref.shape
    rows = peers * each
    heads = value_ref.shape[1] // VDIM
    seqs = each // heads
    values = dot(arr_ref[...].reshape(rows, rank), value_ref[...]).astype(BF16)
    to = lax.broadcasted_iota(jnp.int32, (rows // heads, rows), 0)
    at = lax.broadcasted_iota(jnp.int32, (rows // heads, rows), 1)
    column = lax.broadcasted_iota(jnp.int32, (rows // heads, heads * VDIM), 1)
    picked = jnp.zeros((rows // heads, heads * VDIM), F32)
    for h in range(heads):
        chosen = (at == (to // seqs) * each + h * seqs + to % seqs).astype(BF16)
        picked = jnp.where(column // VDIM == h, dot(chosen, values), picked)
    partial = dot(picked.astype(BF16), out_w_ref[...]).astype(BF16)
    for i in range(out_ref.shape[0]):
        out_ref[i] = partial


def expert_body(rows_ref, mine_ref, gate_ref, up_ref, down_ref, out_ref):
    width = down_ref.shape[1]
    inside = rows_ref[:, :width]
    gate_pre = dot(inside, gate_ref[...])
    up_pre = dot(inside, up_ref[...])
    hidden = (gate_pre / (1.0 + jnp.exp(-gate_pre)) * up_pre).astype(BF16)
    scale = jnp.sum(rows_ref[:, width:].astype(F32) * mine_ref[...], axis=1, keepdims=True)
    out_ref[...] = (dot(hidden, down_ref[...]) * scale).astype(out_ref.dtype)


def shards(
    tokens,
    attn_gain,
    q_down,
    kv_down,
    rope_down,
    q_latent_gain,
    kv_latent_gain,
    q_up,
    query_gain,
    key_up,
    value_up,
    attn_out,
    cache_latent,
    cache_rope,
    lengths,
    moe_gain,
    route,
    route_weight,
    expert_gate,
    expert_up,
    expert_down,
):
    tp_count = lax.axis_size("tp")
    tp_index = lax.axis_index("tp")
    seq_count, width = tokens.shape
    kv_cols = kv_down.shape[1]
    rank = cache_latent.shape[2]
    heads_here = query_gain.shape[0]
    seqs_mine = cache_latent.shape[0]
    first_seq = tp_index * seqs_mine
    both, new_rope = run(
        down_body,
        (
            jax.ShapeDtypeStruct((tp_count, 2 * seq_count, kv_cols), BF16),
            jax.ShapeDtypeStruct((seq_count, rope_down.shape[1]), BF16),
        ),
        tokens,
        attn_gain[None],
        q_down,
        kv_down,
        rope_down,
    )
    latents = lax.all_to_all(both, "tp", 0, 0, tiled=True)
    half_dim = rope_down.shape[1] // 2
    inverse = ROPE_BASE ** (-jnp.arange(half_dim, dtype=F32) / half_dim)
    angles = lengths.astype(F32)[:, None] * inverse
    each = heads_here * seqs_mine
    send, latent_new = run(
        query_body,
        (
            jax.ShapeDtypeStruct((tp_count, each, rank + 2 * half_dim), BF16),
            jax.ShapeDtypeStruct((seq_count, rank), BF16),
        ),
        latents,
        q_latent_gain[None],
        kv_latent_gain[None],
        q_up,
        query_gain,
        key_up,
        jnp.cos(angles),
        jnp.sin(angles),
    )
    queries = lax.all_to_all(send, "tp", 0, 0, tiled=True)
    new_latent = lax.dynamic_slice_in_dim(latent_new, tp_index * kv_cols, kv_cols, 1)
    len_mine = lax.dynamic_slice_in_dim(lengths, first_seq, seqs_mine, 0)
    latent_mine = lax.dynamic_slice_in_dim(latent_new, first_seq, seqs_mine, 0)
    key_new = rotate_last(
        lax.dynamic_slice_in_dim(new_rope, first_seq, seqs_mine, 0).astype(F32), len_mine
    ).astype(BF16)
    positions = jnp.arange(cache_latent.shape[1], dtype=jnp.int32)
    rotated_keys = rotate_rows(cache_rope.astype(F32), positions).astype(BF16)
    attended = run(
        attend_body,
        jax.ShapeDtypeStruct((tp_count, each, rank), BF16),
        queries,
        cache_latent,
        rotated_keys,
        latent_mine,
        key_new,
        jnp.tile(len_mine, tp_count * heads_here)[:, None],
    )
    attended_heads = lax.all_to_all(attended, "tp", 0, 0, tiled=True)
    partials = run(
        heads_body,
        jax.ShapeDtypeStruct((tp_count, seq_count, width), BF16),
        attended_heads,
        value_up,
        attn_out,
    )
    head_sum = lax.all_to_all(partials, "tp", 0, 0, tiled=True).astype(F32).sum(axis=0)
    attn_resid = (tokens.astype(jnp.float32) + head_sum).astype(jnp.bfloat16)
    moe_input = rms_scaled(attn_resid, moe_gain).astype(jnp.bfloat16)
    group_of = route[:, 0] // EPG
    order = jnp.arange(seq_count, dtype=jnp.int32)
    earlier = (group_of[:, None] == group_of[None, :]) & (order[None, :] < order[:, None])
    slot = group_of * GROUP_CAP + jnp.sum(earlier, axis=1, dtype=jnp.int32)
    chips = lax.axis_size(CHIPS)
    cores = lax.axis_size(CORE)
    chips_in_group = EPG // cores
    slots = chips // chips_in_group * GROUP_CAP
    placing = (jnp.arange(slots, dtype=jnp.int32)[:, None] == slot[None, :]).astype(jnp.bfloat16)
    lane = jnp.arange(EXTRA, dtype=jnp.int32)
    named = (route % EPG)[:, :, None] == lane[None, None, :]
    weight_cols = jnp.sum(jnp.where(named, route_weight[..., None], 0.0), axis=1).astype(jnp.bfloat16)
    rows = jnp.concatenate([moe_input, weight_cols], axis=1)
    packed = jnp.dot(placing, rows, preferred_element_type=jnp.float32).astype(jnp.bfloat16)
    packed = jnp.broadcast_to(
        packed.reshape(-1, 1, GROUP_CAP, width + EXTRA),
        (slots // GROUP_CAP, chips_in_group, GROUP_CAP, width + EXTRA),
    ).reshape(chips, GROUP_CAP, width + EXTRA)
    arrived = lax.all_to_all(packed, CHIPS, 0, 0, tiled=True).reshape(-1, width + EXTRA)
    swap = [(i, cores - 1 - i) for i in range(cores)]
    other = lax.ppermute(arrived, CORE, swap)
    mine = (lane == lax.axis_index(EP) % EPG).astype(F32)[None]

    def expert(block, kind):
        return run(
            expert_body,
            jax.ShapeDtypeStruct((block.shape[0], width), kind),
            block,
            mine,
            expert_gate[0],
            expert_up[0],
            expert_down[0],
            flops=100_000_000,
        )

    own = expert(arrived, F32)
    sent_back = lax.ppermute(expert(other, BF16), CORE, swap)
    quarter_cols = width // tp_count
    sums = (own + sent_back.astype(F32)).astype(BF16)
    sums = sums.reshape(chips, GROUP_CAP, tp_count, quarter_cols).swapaxes(1, 2)
    returned = lax.all_to_all(
        sums.reshape(chips * tp_count, GROUP_CAP, quarter_cols), (*CHIPS, "tp"), 0, 0, tiled=True
    ).reshape(-1, chips_in_group * tp_count, GROUP_CAP, quarter_cols)
    totals = jnp.sum(returned.astype(F32), axis=1).reshape(slots, quarter_cols)
    high = totals.astype(BF16)
    picked = jnp.dot(placing.T, high, preferred_element_type=F32)
    residual = lax.dynamic_slice_in_dim(attn_resid, tp_index * quarter_cols, quarter_cols, 1)
    mixed_out = (residual.astype(F32) + picked).astype(BF16)
    return (mixed_out, new_latent, new_rope)


def solution(mesh):
    torus = Mesh(mesh.devices.reshape(8, 8, 2, mesh.shape["tp"]), ("ep_0", "ep_1", "ep_2", "tp"))
    placed = (
        P(EP, None),
        P(),
        P(None, "tp"),
        P(None, "tp"),
        P(),
        P(),
        P(),
        P(None, "tp"),
        P("tp", None),
        P(None, "tp"),
        P(None, "tp"),
        P("tp", None),
        P(EP_TP, None, None),
        P(EP_TP, None, None),
        P(EP),
        P(),
        P(EP, None),
        P(EP, None),
        P(EP, None, "tp"),
        P(EP, None, "tp"),
        P(EP, "tp", None),
    )
    return jax.shard_map(
        shards,
        mesh=torus,
        in_specs=placed,
        out_specs=(P(EP, "tp"), P(EP, "tp"), P(EP, None)),
        check_vma=False,
    )
```

time: 123 us -> 126 us (1.024)
  the two profiles are of different devices: /device:TPU:8 before, /device:TPU:1 now
where the time goes in v2:
time: 126 us; the launch traced here: 125 us
  starting transfers between devices  35.3 us (28%)
  blocking collectives  28.8 us (23%)
  waiting for transfers between devices  24.5 us (19%)
  Pallas kernels  14.7 us (12%)
  other arithmetic  10.5 us (8%)
  local copies, waits for them, and re-layouts  9.75 us (8%)
    all_to_all x1, blocking collectives, shards(): lax.all_to_all(packed, CHIPS, 0, 0, tiled=True).reshape(-1, width + EXTRA)  28.8 us
    pallas_call x6, Pallas kernels, run(): pl.pallas_call(body, out_shape=outs, cost_estimate=pl.CostEstimate(flops=...  14.7 us
    all_to_all x1, waiting for transfers between devices, shards(): lax.all_to_all(sums.reshape(chips * tp_count, GROUP_CAP, quarter_cols), (...  12.5 us
    all_to_all x1, starting transfers between devices, shards(): lax.all_to_all(sums.reshape(chips * tp_count, GROUP_CAP, quarter_cols), (...  9.13 us
    ppermute x1, starting transfers between devices, shards(): other = lax.ppermute(arrived, CORE, swap)  8.24 us
    unnamed x20, local copies, waits for them, and re-layouts  5.11 us
    all_to_all x1, starting transfers between devices, shards(): latents = lax.all_to_all(both, 'tp', 0, 0, tiled=True)  4.83 us
    all_to_all x1, waiting for transfers between devices, shards(): lax.all_to_all(partials, 'tp', 0, 0, tiled=True).astype(F32).sum(axis=0)  4.69 us
  transfers between devices with their start and end apart: 7, of which 5 were waited for; matrix products, arithmetic and copies ran while one was open for 10% of the time, Pallas kernels for 2%

profile of v2, /device:TPU:1, one launch (start us, length us, event | category | flops | bytes accessed | tf_op | source)
XLA Modules:
  0.0 125.3 jit_solution(613299278812342034)
XLA Ops:
  0.6 1.7 %copy.35.rope_ref = bf16[1024,32]{1,0:T(8,128)(2,1)} copy(bf16[1024,32]{0,1:T(8,128)(2,1)} %param.25) | data formatting | bytes 131072 | tf_op args[4]
  2.4 2.0 %shard_map.220 = (bf16[4,32,128]{2,1,0:T(8,128)(2,1)}, bf16[16,32]{1,0:T(8,128)(2,1)}) custom-call(bf16[16,1024]{1,0:T(8,128)(2,1)} %tok_ref.1, f32[1,1024]{1,0:T(1,128)} %bitcast.32, bf16[1024,128]{1,0:T(8,128)(2,1)} %q_ref.1, bf16[1024,128]{1,0:T(8,128)(2,1)} %kv_ref.1, bf16[1024,32]{1,0:T(8,128)(2,1)} %copy.35.rope_ref), custom_call_target="tpu_custom_call" | custom-call | flops 2000000 | bytes 626688 | tf_op jit(solution)/shard_map/pallas_call | solution.py:78
  4.4 4.8 %all-to-all-start = ((bf16[4,32,128]{2,1,0:T(8,128)(2,1)}), bf16[4,32,128]{2,1,0:T(8,128)(2,1)S(1)}, u32[]{:S(2)}, u32[]{:S(2)}) async-start(bf16[4,32,128]{2,1,0:T(8,128)(2,1)} %get-tuple-element.7), calls=%async_computation | async-start | bytes 65536 | tf_op jit(solution)/shard_map/all_to_all | solution.py:232
  14.3 0.9 convert_element_type.88
  19.1 2.2 %shard_map.221 = (bf16[4,8,544]{2,1,0:T(8,128)(2,1)}, bf16[16,512]{1,0:T(8,128)(2,1)}) custom-call(bf16[4,32,128]{2,1,0:T(8,128)(2,1)} %copy-done.4, f32[1,512]{1,0:T(1,128)} %bitcast.33, f32[1,512]{1,0:T(1,128)} %bitcast.34, bf16[512,192]{1,0:T(8,128)(2,1)} %copy.36.q_up_ref, f32[2,96]{1,0:T(2,128)} %head_gain_ref.1, bf16[512,128]{1,0:T(8,128)(2,1)} %key_up_ref.1, ...), custom_call_target="tpu_custom_call" | custom-call | flops 2000000 | bytes 367360 | tf_op jit(solution)/shard_map/pallas_call | solution.py:78
  21.3 4.2 %all-to-all-start.1 = ((bf16[4,8,544]{2,1,0:T(8,128)(2,1)}), bf16[4,8,544]{2,1,0:T(8,128)(2,1)S(1)}, u32[]{:S(2)}, u32[]{:S(2)}) async-start(bf16[4,8,544]{2,1,0:T(8,128)(2,1)} %get-tuple-element.8), calls=%async_computation.1 | async-start | bytes 81920 | tf_op jit(solution)/shard_map/all_to_all | solution.py:252
  25.5 1.3 %constant_dynamic-slice_fusion.1.latent_ref = bf16[4,512]{1,0:T(4,128)(2,1)} fusion(bf16[16,512]{1,0:T(8,128)(2,1)} %get-tuple-element.9, s32[]{:T(128)S(6)} %select_n.43), kind=kLoop, calls=%fused_computation.57 | loop fusion | bytes 8196 | tf_op jit(solution)/shard_map/dynamic_slice | solution.py:255
  26.8 3.0 %all-to-all-done.1.arr_ref = bf16[4,8,544]{2,1,0:T(8,128)(2,1)S(1)} async-done(((bf16[4,8,544]{2,1,0:T(8,128)(2,1)}), bf16[4,8,544]{2,1,0:T(8,128)(2,1)S(1)}, u32[]{:S(2)}, u32[]{:S(2)}) %all-to-all-start.1) | async-done | bytes 34848 | tf_op jit(solution)/shard_map/all_to_all | solution.py:252
  30.5 3.5 %shard_map.222 = bf16[4,8,512]{2,1,0:T(8,128)(2,1)} custom-call(bf16[4,8,544]{2,1,0:T(8,128)(2,1)} %copy-done.3, bf16[4,512,512]{2,1,0:T(8,128)(2,1)} %cache_ref.1, bf16[4,32,512]{2,1,0:T(8,128)(2,1)} %pad_maximum_fusion.keys_ref, bf16[4,512]{1,0:T(4,128)(2,1)} %constant_dynamic-slice_fusion.1.latent_ref, bf16[4,32]{1,0:T(4,128)(2,1)} %pad_maximum_fusion.1.key_new_ref, ...), custom_call_target="tpu_custom_call" | custom-call | flops 2000000 | bytes 2267520 | tf_op jit(solution)/shard_map/pallas_call | solution.py:78
  34.0 3.3 %all-to-all-start.2 = ((bf16[4,8,512]{2,1,0:T(8,128)(2,1)}), bf16[4,8,512]{2,1,0:T(8,128)(2,1)S(1)}, u32[]{:S(2)}, u32[]{:S(2)}) async-start(bf16[4,8,512]{2,1,0:T(8,128)(2,1)} %shard_map.222), calls=%async_computation.2 | async-start | bytes 65536 | tf_op jit(solution)/shard_map/all_to_all | solution.py:271
  37.9 3.6 %all-to-all-done.2.arr_ref = bf16[4,8,512]{2,1,0:T(8,128)(2,1)S(1)} async-done(((bf16[4,8,512]{2,1,0:T(8,128)(2,1)}), bf16[4,8,512]{2,1,0:T(8,128)(2,1)S(1)}, u32[]{:S(2)}, u32[]{:S(2)}) %all-to-all-start.2) | async-done | bytes 32800 | tf_op jit(solution)/shard_map/all_to_all | solution.py:271
  42.1 2.1 %shard_map.223 = bf16[4,16,1024]{2,1,0:T(8,128)(2,1)} custom-call(bf16[4,8,512]{2,1,0:T(8,128)(2,1)} %copy-done.5, bf16[512,128]{1,0:T(8,128)(2,1)} %value_ref.1, bf16[128,1024]{1,0:T(8,128)(2,1)} %out_w_ref.1), custom_call_target="tpu_custom_call" | custom-call | flops 2000000 | bytes 425984 | tf_op jit(solution)/shard_map/pallas_call | solution.py:78
  44.2 3.3 %all-to-all-start.3 = ((bf16[4,16,1024]{2,1,0:T(8,128)(2,1)}), bf16[4,16,1024]{2,1,0:T(8,128)(2,1)S(1)}, u32[]{:S(2)}, u32[]{:S(2)}) async-start(bf16[4,16,1024]{2,1,0:T(8,128)(2,1)} %shard_map.223), calls=%async_computation.3 | async-start | bytes 262144 | tf_op jit(solution)/shard_map/all_to_all | solution.py:279
  47.6 4.7 %all-to-all-done.3 = bf16[4,16,1024]{2,1,0:T(8,128)(2,1)S(1)} async-done(((bf16[4,16,1024]{2,1,0:T(8,128)(2,1)}), bf16[4,16,1024]{2,1,0:T(8,128)(2,1)S(1)}, u32[]{:S(2)}, u32[]{:S(2)}) %all-to-all-start.3) | async-done | bytes 131104 | tf_op jit(solution)/shard_map/all_to_all | solution.py:279
  52.9 28.8 %all_to_all.30 = bf16[64,2,1152]{2,1,0:T(2,128)(2,1)S(1)} all-to-all(bf16[64,2,1152]{2,1,0:T(2,128)(2,1)S(1)} %bitcast.25), channel_id=1, replica_groups=mesh['ep_0'=8,'ep_1'=8,'ep_2'=2,'tp'=4] {'ep_0','ep_1'}, dimensions={0} | all-to-all | bytes 589824 | tf_op jit(solution)/shard_map/all_to_all | solution.py:300
  81.9 8.2 %collective-permute-start = (bf16[128,1152]{1,0:T(8,128)(2,1)S(1)}, bf16[128,1152]{1,0:T(8,128)(2,1)S(1)}, u32[]{:S(2)}, u32[]{:S(2)}) collective-permute-start(bf16[128,1152]{1,0:T(8,128)(2,1)S(1)} %reshape.162.rows_ref), channel_id=1, source_target_pairs={{0,4},{4,0},{1,5},{5,1},{2,6},{6,2},{3,7},{7,3},{8,12},{12,8},{9,1... | collective-permute-start | bytes 884744 | tf_op jit(solution)/shard_map/ppermute | solution.py:302
  92.0 2.4 %shard_map.225 = bf16[128,1024]{1,0:T(8,128)(2,1)} custom-call(bf16[128,1152]{1,0:T(8,128)(2,1)} %copy-done.1, f32[1,128]{1,0:T(1,128)} %compare_convert_fusion.mine_ref, bf16[1024,128]{1,0:T(8,128)(2,1)} %bitcast.26, bf16[1024,128]{1,0:T(8,128)(2,1)} %bitcast.28, bf16[128,1024]{1,0:T(8,128)(2,1)} %bitcast.30), custom_call_target="tpu_custom_call" | custom-call | flops 100000000 | bytes 1081856 | tf_op jit(solution)/shard_map/pallas_call | solution.py:78
  94.4 2.3 %collective-permute-start.1 = (bf16[128,1024]{1,0:T(8,128)(2,1)}, bf16[128,1024]{1,0:T(8,128)(2,1)S(1)}, u32[]{:S(2)}, u32[]{:S(2)}) collective-permute-start(bf16[128,1024]{1,0:T(8,128)(2,1)} %shard_map.225), channel_id=1, source_target_pairs={{0,4},{4,0},{1,5},{5,1},{2,6},{6,2},{3,7},{7,3},{8,12},{12,8},{9,1... | collective-permute-start | bytes 786440 | tf_op jit(solution)/shard_map/ppermute | solution.py:318
  96.7 2.5 %shard_map.224 = f32[128,1024]{1,0:T(8,128)} custom-call(bf16[128,1152]{1,0:T(8,128)(2,1)} %copy-done, f32[1,128]{1,0:T(1,128)} %compare_convert_fusion.mine_ref, bf16[1024,128]{1,0:T(8,128)(2,1)} %bitcast.27, bf16[1024,128]{1,0:T(8,128)(2,1)} %bitcast.29, bf16[128,1024]{1,0:T(8,128)(2,1)} %bitcast.31), custom_call_target="tpu_custom_call" | custom-call | flops 100000000 | bytes 1081856 | tf_op jit(solution)/shard_map/pallas_call | solution.py:78
  99.2 1.1 add_convert_fusion
  100.4 0.9 copy.38
  101.4 9.1 %all-to-all-start.5 = ((bf16[256,2,256]{2,1,0:T(2,128)(2,1)}), bf16[256,2,256]{2,1,0:T(2,128)(2,1)S(1)}, u32[]{:S(2)}, u32[]{:S(2)}) async-start(bf16[256,2,256]{2,1,0:T(2,128)(2,1)} %bitcast.10), calls=%async_computation.5 | async-start | bytes 524288 | tf_op jit(solution)/shard_map/all_to_all | solution.py:322
  110.5 1.3 %constant_dynamic-slice_fusion = bf16[16,128]{1,0:T(8,128)(2,1)} fusion(bf16[16,512]{1,0:T(8,128)(2,1)} %get-tuple-element.9, s32[]{:T(128)S(6)} %select_n.50), kind=kLoop, calls=%fused_computation.56 | loop fusion | bytes 8196 | tf_op jit(solution)/shard_map/dynamic_slice | solution.py:253
  111.8 12.5 %all-to-all-done.5 = bf16[256,2,256]{2,1,0:T(2,128)(2,1)S(1)} async-done(((bf16[256,2,256]{2,1,0:T(2,128)(2,1)}), bf16[256,2,256]{2,1,0:T(2,128)(2,1)S(1)}, u32[]{:S(2)}, u32[]{:S(2)}) %all-to-all-start.5) | async-done | bytes 262176 | tf_op jit(solution)/shard_map/all_to_all | solution.py:322
  (54 shorter events, 14.6 us)
Async XLA Ops:
  0.6 17.0 %copy-start.2 = (bf16[512,192]{0,1:T(8,128)(2,1)S(1)}, bf16[512,192]{0,1:T(8,128)(2,1)}, u32[]{:S(2)}) copy-start(bf16[512,192]{0,1:T(8,128)(2,1)} %param.28) | copy-start | bytes 589828
  4.4 14.0 %all-to-all-start = ((bf16[4,32,128]{2,1,0:T(8,128)(2,1)}), bf16[4,32,128]{2,1,0:T(8,128)(2,1)S(1)}, u32[]{:S(2)}, u32[]{:S(2)}) async-start(bf16[4,32,128]{2,1,0:T(8,128)(2,1)} %get-tuple-element.7), calls=%async_computation | async-start | bytes 65536 | tf_op jit(solution)/shard_map/all_to_all | solution.py:232
  17.6 29.9 %copy-start.7 = (f32[16,6]{0,1:T(8,128)S(1)}, f32[16,6]{0,1:T(8,128)}, u32[]{:S(2)}) copy-start(f32[16,6]{0,1:T(8,128)} %param.38) | copy-start | bytes 1156
  18.4 33.9 %copy-start.6 = (bf16[16,1024]{1,0:T(8,128)(2,1)S(1)}, bf16[16,1024]{1,0:T(8,128)(2,1)}, u32[]{:S(2)}) copy-start(bf16[16,1024]{1,0:T(8,128)(2,1)} %tok_ref.1) | copy-start | bytes 98308
  18.4 34.1 %copy-start.8 = (f32[1024]{0:T(1024)S(1)}, f32[1024]{0:T(1024)}, u32[]{:S(2)}) copy-start(f32[1024]{0:T(1024)} %param.36) | copy-start | bytes 12292
  18.4 0.6 copy-start.4
  21.3 8.6 %all-to-all-start.1 = ((bf16[4,8,544]{2,1,0:T(8,128)(2,1)}), bf16[4,8,544]{2,1,0:T(8,128)(2,1)S(1)}, u32[]{:S(2)}, u32[]{:S(2)}) async-start(bf16[4,8,544]{2,1,0:T(8,128)(2,1)} %get-tuple-element.8), calls=%async_computation.1 | async-start | bytes 81920 | tf_op jit(solution)/shard_map/all_to_all | solution.py:252
  29.9 0.6 copy-start.3
  34.0 7.5 %all-to-all-start.2 = ((bf16[4,8,512]{2,1,0:T(8,128)(2,1)}), bf16[4,8,512]{2,1,0:T(8,128)(2,1)S(1)}, u32[]{:S(2)}, u32[]{:S(2)}) async-start(bf16[4,8,512]{2,1,0:T(8,128)(2,1)} %shard_map.222), calls=%async_computation.2 | async-start | bytes 65536 | tf_op jit(solution)/shard_map/all_to_all | solution.py:271
  41.5 0.6 copy-start.5
  44.2 8.1 %all-to-all-start.3 = ((bf16[4,16,1024]{2,1,0:T(8,128)(2,1)}), bf16[4,16,1024]{2,1,0:T(8,128)(2,1)S(1)}, u32[]{:S(2)}, u32[]{:S(2)}) async-start(bf16[4,16,1024]{2,1,0:T(8,128)(2,1)} %shard_map.223), calls=%async_computation.3 | async-start | bytes 262144 | tf_op jit(solution)/shard_map/all_to_all | solution.py:279
  81.9 14.8 %copy-start = (bf16[128,1152]{1,0:T(8,128)(2,1)}, bf16[128,1152]{1,0:T(8,128)(2,1)S(1)}, u32[]{:S(2)}) copy-start(bf16[128,1152]{1,0:T(8,128)(2,1)S(1)} %reshape.162.rows_ref) | copy-start | bytes 884740
  81.9 9.4 %collective-permute-start = (bf16[128,1152]{1,0:T(8,128)(2,1)S(1)}, bf16[128,1152]{1,0:T(8,128)(2,1)S(1)}, u32[]{:S(2)}, u32[]{:S(2)}) collective-permute-start(bf16[128,1152]{1,0:T(8,128)(2,1)S(1)} %reshape.162.rows_ref), channel_id=1, source_target_pairs={{0,4},{4,0},{1,5},{5,1},{2,6},{6,2},{3,7},{7,3},{8,12},{12,8},{9,1... | collective-permute-start | bytes 884744 | tf_op jit(solution)/shard_map/ppermute | solution.py:302
  91.3 0.7 copy-start.1
  94.4 4.8 %collective-permute-start.1 = (bf16[128,1024]{1,0:T(8,128)(2,1)}, bf16[128,1024]{1,0:T(8,128)(2,1)S(1)}, u32[]{:S(2)}, u32[]{:S(2)}) collective-permute-start(bf16[128,1024]{1,0:T(8,128)(2,1)} %shard_map.225), channel_id=1, source_target_pairs={{0,4},{4,0},{1,5},{5,1},{2,6},{6,2},{3,7},{7,3},{8,12},{12,8},{9,1... | collective-permute-start | bytes 786440 | tf_op jit(solution)/shard_map/ppermute | solution.py:318
  101.4 22.9 %all-to-all-start.5 = ((bf16[256,2,256]{2,1,0:T(2,128)(2,1)}), bf16[256,2,256]{2,1,0:T(2,128)(2,1)S(1)}, u32[]{:S(2)}, u32[]{:S(2)}) async-start(bf16[256,2,256]{2,1,0:T(2,128)(2,1)} %bitcast.10), calls=%async_computation.5 | async-start | bytes 524288 | tf_op jit(solution)/shard_map/all_to_all | solution.py:322

commit v3 on v2

--- a/solution.py
+++ b/solution.py
@@ -1,7 +1,9 @@
 import jax
 import jax.numpy as jnp
+import numpy as np
 from jax import lax
 from jax.experimental import pallas as pl
+from jax.experimental.pallas import tpu as pltpu
 from jax.sharding import Mesh
 from jax.sharding import PartitionSpec as P
 
@@ -19,6 +21,9 @@
 
 EPS = 1e-06
 ROPE_BASE = 10000.0
+F32 = jnp.float32
+BF16 = jnp.bfloat16
+NEG = -1e30
 
 
 def rms_scaled(values_in, gain_vec):
@@ -30,41 +35,6 @@
     )
 
 
-def rotate_last(values_in, positions):
-    half_dim = values_in.shape[-1] // 2
-    inverse = ROPE_BASE ** (-jnp.arange(half_dim, dtype=jnp.float32) / half_dim)
-    angles = positions.astype(jnp.float32)[..., None] * inverse
-    lower_half = values_in[..., :half_dim]
-    upper_half = values_in[..., half_dim:]
-    return jnp.concatenate(
-        [
-            lower_half * jnp.cos(angles) - upper_half * jnp.sin(angles),
-            upper_half * jnp.cos(angles) + lower_half * jnp.sin(angles),
-        ],
-        -1,
-    )
-
-
-def rotate_rows(values_in, positions):
-    half_dim = values_in.shape[1] // 2
-    inverse = ROPE_BASE ** (-jnp.arange(half_dim, dtype=jnp.float32) / half_dim)
-    angles = inverse[:, None] * positions.astype(jnp.float32)[None, :]
-    lower_half = values_in[:, :half_dim]
-    upper_half = values_in[:, half_dim:]
-    return jnp.concatenate(
-        [
-            lower_half * jnp.cos(angles) - upper_half * jnp.sin(angles),
-            upper_half * jnp.cos(angles) + lower_half * jnp.sin(angles),
-        ],
-        1,
-    )
-
-
-F32 = jnp.float32
-BF16 = jnp.bfloat16
-NEG = -1e30
-
-
 def dot(a, b):
     return jnp.dot(a, b, preferred_element_type=F32)
 
@@ -73,24 +43,84 @@
     return lax.dot_general(a, b, (((1,), (1,)), ((), ())), preferred_element_type=F32)
 
 
-def run(body, outs, *args, flops=2_000_000):
+def near(array):
+    return pltpu.with_memory_space_constraint(array, pltpu.VMEM)
+
+
+def far(array):
+    return pltpu.with_memory_space_constraint(array, pltpu.HBM)
+
+
+def run(body, outs, *args, flops=2_000_000, scalars=0):
     moved = sum(a.size * a.dtype.itemsize for a in args)
     return pl.pallas_call(
         body,
-        out_shape=outs,
+        compiler_params=pltpu.CompilerParams(vmem_limit_bytes=16 * 1024 * 1024),
+        in_specs=[pl.BlockSpec(memory_space=pltpu.SMEM)] * scalars
+        + [pl.BlockSpec(memory_space=pltpu.VMEM)] * (len(args) - scalars),
+        out_shape=jax.tree.map(lambda o: pltpu.VMEM(o.shape, o.dtype), outs),
         cost_estimate=pl.CostEstimate(flops=flops, transcendentals=0, bytes_accessed=moved),
     )(*args)
 
 
-def down_body(tok_ref, gain_ref, q_ref, kv_ref, rope_ref, both_ref, new_rope_ref):
+def fetch_body(*refs):
+    count = (len(refs) - 1) // 2
+    sems = refs[-1]
+    copies = [
+        pltpu.make_async_copy(refs[i], refs[count + i], sems.at[i]) for i in range(count)
+    ]
+    for copy in copies:
+        copy.start()
+    for copy in copies:
+        copy.wait()
+
+
+def fetched(*arrays):
+    moved = sum(a.size * a.dtype.itemsize for a in arrays)
+    return pl.pallas_call(
+        fetch_body,
+        compiler_params=pltpu.CompilerParams(vmem_limit_bytes=1024 * 1024),
+        in_specs=[pl.BlockSpec(memory_space=pltpu.HBM)] * len(arrays),
+        out_specs=[pl.BlockSpec(memory_space=pltpu.VMEM)] * len(arrays),
+        out_shape=[pltpu.VMEM(a.shape, a.dtype) for a in arrays],
+        scratch_shapes=[pltpu.SemaphoreType.DMA((len(arrays),))],
+        cost_estimate=pl.CostEstimate(flops=2_000_000, transcendentals=0, bytes_accessed=moved),
+    )(*[far(a) for a in arrays])
+
+
+def down_body(*refs):
+    hbm, (both_ref, new_rope_ref), near_refs, sems = refs[:5], refs[5:7], refs[7:12], refs[12]
+    copies = [pltpu.make_async_copy(hbm[i], near_refs[i], sems.at[i]) for i in range(5)]
+    for copy in copies:
+        copy.start()
+    tok_ref, gain_ref, q_ref, kv_ref, rope_ref = near_refs
+    copies[0].wait()
+    copies[1].wait()
     normed = rms_scaled(tok_ref[...], gain_ref[...]).astype(BF16)
     rows = normed.shape[0]
+    copies[2].wait()
     q_part = dot(normed, q_ref[...]).astype(BF16)
+    copies[3].wait()
     kv_part = dot(normed, kv_ref[...]).astype(BF16)
     for i in range(both_ref.shape[0]):
         both_ref[i, :rows, :] = q_part
         both_ref[i, rows:, :] = kv_part
-    new_rope_ref[...] = dot(normed, rope_ref[...]).astype(BF16)
+    copies[4].wait()
+    new_rope_ref[...] = dot_t(normed, rope_ref[...]).astype(BF16)
+
+
+def down(outs, *args):
+    moved = sum(a.size * a.dtype.itemsize for a in args)
+    return pl.pallas_call(
+        down_body,
+        compiler_params=pltpu.CompilerParams(vmem_limit_bytes=16 * 1024 * 1024),
+        in_specs=[pl.BlockSpec(memory_space=pltpu.HBM)] * len(args),
+        out_specs=[pl.BlockSpec(memory_space=pltpu.VMEM)] * len(outs),
+        out_shape=[pltpu.VMEM(o.shape, o.dtype) for o in outs],
+        scratch_shapes=[pltpu.VMEM(a.shape, a.dtype) for a in args]
+        + [pltpu.SemaphoreType.DMA((len(args),))],
+        cost_estimate=pl.CostEstimate(flops=2_000_000, transcendentals=0, bytes_accessed=moved),
+    )(*[far(a) for a in args])
 
 
 def query_body(
@@ -105,7 +135,7 @@
     kv_raw = jnp.concatenate([arr_ref[i, rows:, :] for i in range(peers)], axis=1)
     latent_ref[...] = rms_scaled(kv_raw, kv_gain_ref[...]).astype(BF16)
     q_lat = rms_scaled(q_raw, q_gain_ref[...]).astype(BF16)
-    query = dot(q_lat, q_up_ref[...])
+    query = dot_t(q_lat, q_up_ref[...])
     each = rows // peers
     for h in range(head_gain_ref.shape[0]):
         one = rms_scaled(query[:, h * QK : (h + 1) * QK], head_gain_ref[h : h + 1, :])
@@ -125,28 +155,69 @@
             send_ref[i, at, rank:] = turned[i * each : (i + 1) * each].astype(BF16)
 
 
-def attend_body(arr_ref, cache_ref, keys_ref, latent_ref, key_new_ref, len_ref, out_ref):
+def keys_body(rope_ref, cos_ref, sin_ref, out_ref):
+    half = cos_ref.shape[0]
+    for s in range(rope_ref.shape[0]):
+        lower = rope_ref[s, :half, :].astype(F32)
+        upper = rope_ref[s, half:, :].astype(F32)
+        out_ref[s, :half, :] = (lower * cos_ref[...] - upper * sin_ref[...]).astype(BF16)
+        out_ref[s, half:, :] = (upper * cos_ref[...] + lower * sin_ref[...]).astype(BF16)
+
+
+def place_body(route_ref, weight_ref, placing_ref, weights_ref):
+    topk, rows = route_ref.shape
+    slots = placing_ref.shape[0]
+    group = route_ref[0:1, :] // EPG
+    first = lax.broadcasted_iota(jnp.int32, (rows, rows), 0)
+    second = lax.broadcasted_iota(jnp.int32, (rows, rows), 1)
+    column = jnp.sum(jnp.where(first == second, group, 0), axis=1, keepdims=True)
+    earlier = jnp.where((column == group) & (first < second), 1, 0)
+    slot = group * GROUP_CAP + jnp.sum(earlier, axis=0, keepdims=True)
+    placing = (lax.broadcasted_iota(jnp.int32, (slots, rows), 0) == slot).astype(BF16)
+    placing_ref[...] = placing
+    lane = lax.broadcasted_iota(jnp.int32, (EXTRA, rows), 0)
+    table = jnp.zeros((EXTRA, rows), F32)
+    for k in range(topk):
+        table = table + jnp.where(route_ref[k : k + 1, :] % EPG == lane, weight_ref[k : k + 1, :], 0.0)
+    weights_ref[...] = dot_t(placing, table.astype(BF16)).astype(BF16)
+
+
+def attend_body(
+    first_ref, arr_ref, cache_ref, keys_ref, latent_ref, rope_ref, cos_ref, sin_ref, len_ref, out_ref
+):
     seqs, places, rank = cache_ref.shape
     peers, each, _ = arr_ref.shape
     rows = peers * each
+    half = cos_ref.shape[1]
     arrived = arr_ref[...].reshape(rows, arr_ref.shape[2])
     absorbed = arrived[:, :rank]
     turned = arrived[:, rank:]
     scale = QK ** (-0.5)
     row_seq = lax.broadcasted_iota(jnp.int32, (rows, 1), 0) % seqs
+    every = latent_ref.shape[0]
+    chosen = lax.broadcasted_iota(jnp.int32, (rows, every), 1) == row_seq + first_ref[0]
+    lengths = jnp.sum(jnp.where(chosen, len_ref[...], 0), axis=1, keepdims=True)
+    chosen = chosen.astype(BF16)
+    latent = dot(chosen, latent_ref[...])
+    lower = rope_ref[:, :half].astype(F32)
+    upper = rope_ref[:, half:].astype(F32)
+    key_new = jnp.concatenate(
+        [
+            lower * cos_ref[...] - upper * sin_ref[...],
+            upper * cos_ref[...] + lower * sin_ref[...],
+        ],
+        axis=1,
+    )
+    key_new = dot(chosen, key_new.astype(BF16))
+    self_score = (
+        jnp.sum(absorbed.astype(F32) * latent, axis=1, keepdims=True)
+        + jnp.sum(turned.astype(F32) * key_new, axis=1, keepdims=True)
+    ) * scale
     scores = jnp.zeros((rows, places), F32)
     for s in range(seqs):
         part = dot_t(absorbed, cache_ref[s]) + dot(turned, keys_ref[s])
         scores = jnp.where(row_seq == s, part, scores)
-    spread = rows // seqs
-    latent = jnp.concatenate([latent_ref[...].astype(F32)] * spread, axis=0)
-    key_new = jnp.concatenate([key_new_ref[...].astype(F32)] * spread, axis=0)
-    self_score = (
-        jnp.sum(absorbed.astype(F32) * latent, axis=1, keepdims=True)
-        + jnp.sum(turned.astype(F32) * key_new, axis=1, keepdims=True)
-    ) * scale
-    place = lax.broadcasted_iota(jnp.int32, (rows, places), 1)
-    valid = place < len_ref[...]
+    valid = lax.broadcasted_iota(jnp.int32, (rows, places), 1) < lengths
     scores = jnp.where(valid, scores * scale, NEG)
     top = jnp.maximum(jnp.max(scores, axis=1, keepdims=True), self_score)
     weights = jnp.where(valid, jnp.exp(scores - top), 0.0)
@@ -216,9 +287,7 @@
     rank = cache_latent.shape[2]
     heads_here = query_gain.shape[0]
     seqs_mine = cache_latent.shape[0]
-    first_seq = tp_index * seqs_mine
-    both, new_rope = run(
-        down_body,
+    both, new_rope = down(
         (
             jax.ShapeDtypeStruct((tp_count, 2 * seq_count, kv_cols), BF16),
             jax.ShapeDtypeStruct((seq_count, rope_down.shape[1]), BF16),
@@ -227,12 +296,32 @@
         attn_gain[None],
         q_down,
         kv_down,
-        rope_down,
+        rope_down.T,
+    )
+    half_dim = rope_down.shape[1] // 2
+    turns = ROPE_BASE ** (-np.arange(half_dim, dtype=np.float32) / np.float32(half_dim))
+    turns = turns.astype(np.float32)[:, None] * np.arange(cache_latent.shape[1], dtype=np.float32)
+    cos_table = jnp.asarray(np.cos(turns.astype(np.float64)).astype(np.float32))
+    sin_table = jnp.asarray(np.sin(turns.astype(np.float64)).astype(np.float32))
+    both, q_up, key_up, cache_latent, lengths = lax.optimization_barrier(
+        (both, q_up, key_up, cache_latent, lengths)
     )
     latents = lax.all_to_all(both, "tp", 0, 0, tiled=True)
-    half_dim = rope_down.shape[1] // 2
+    q_up_t, key_up, q_gain, kv_gain, head_gain, cache, cos_table, sin_table, cache_rope = fetched(
+        q_up.T,
+        key_up,
+        q_latent_gain[None],
+        kv_latent_gain[None],
+        query_gain,
+        cache_latent,
+        cos_table,
+        sin_table,
+        cache_rope,
+    )
     inverse = ROPE_BASE ** (-jnp.arange(half_dim, dtype=F32) / half_dim)
     angles = lengths.astype(F32)[:, None] * inverse
+    cosines = near(jnp.cos(angles))
+    sines = near(jnp.sin(angles))
     each = heads_here * seqs_mine
     send, latent_new = run(
         query_body,
@@ -240,59 +329,65 @@
             jax.ShapeDtypeStruct((tp_count, each, rank + 2 * half_dim), BF16),
             jax.ShapeDtypeStruct((seq_count, rank), BF16),
         ),
-        latents,
-        q_latent_gain[None],
-        kv_latent_gain[None],
-        q_up,
-        query_gain,
-        key_up,
-        jnp.cos(angles),
-        jnp.sin(angles),
-    )
+        near(latents),
+        near(q_gain),
+        near(kv_gain),
+        near(q_up_t),
+        near(head_gain),
+        near(key_up),
+        cosines,
+        sines,
+    )
+    send, cache_rope = lax.optimization_barrier((send, cache_rope))
     queries = lax.all_to_all(send, "tp", 0, 0, tiled=True)
     new_latent = lax.dynamic_slice_in_dim(latent_new, tp_index * kv_cols, kv_cols, 1)
-    len_mine = lax.dynamic_slice_in_dim(lengths, first_seq, seqs_mine, 0)
-    latent_mine = lax.dynamic_slice_in_dim(latent_new, first_seq, seqs_mine, 0)
-    key_new = rotate_last(
-        lax.dynamic_slice_in_dim(new_rope, first_seq, seqs_mine, 0).astype(F32), len_mine
-    ).astype(BF16)
-    positions = jnp.arange(cache_latent.shape[1], dtype=jnp.int32)
-    rotated_keys = rotate_rows(cache_rope.astype(F32), positions).astype(BF16)
+    rotated_keys = run(
+        keys_body,
+        jax.ShapeDtypeStruct(cache_rope.shape, BF16),
+        near(cache_rope),
+        near(cos_table),
+        near(sin_table),
+    )
     attended = run(
         attend_body,
         jax.ShapeDtypeStruct((tp_count, each, rank), BF16),
-        queries,
-        cache_latent,
-        rotated_keys,
-        latent_mine,
-        key_new,
-        jnp.tile(len_mine, tp_count * heads_here)[:, None],
+        (tp_index * seqs_mine)[None].astype(jnp.int32),
+        near(queries),
+        near(cache),
+        near(rotated_keys),
+        near(latent_new),
+        near(new_rope),
+        cosines,
+        sines,
+        near(lengths[None]),
+        scalars=1,
     )
     attended_heads = lax.all_to_all(attended, "tp", 0, 0, tiled=True)
     partials = run(
         heads_body,
         jax.ShapeDtypeStruct((tp_count, seq_count, width), BF16),
-        attended_heads,
-        value_up,
-        attn_out,
+        near(attended_heads),
+        near(value_up),
+        near(attn_out),
     )
     head_sum = lax.all_to_all(partials, "tp", 0, 0, tiled=True).astype(F32).sum(axis=0)
     attn_resid = (tokens.astype(jnp.float32) + head_sum).astype(jnp.bfloat16)
     moe_input = rms_scaled(attn_resid, moe_gain).astype(jnp.bfloat16)
-    group_of = route[:, 0] // EPG
-    order = jnp.arange(seq_count, dtype=jnp.int32)
-    earlier = (group_of[:, None] == group_of[None, :]) & (order[None, :] < order[:, None])
-    slot = group_of * GROUP_CAP + jnp.sum(earlier, axis=1, dtype=jnp.int32)
     chips = lax.axis_size(CHIPS)
     cores = lax.axis_size(CORE)
     chips_in_group = EPG // cores
     slots = chips // chips_in_group * GROUP_CAP
-    placing = (jnp.arange(slots, dtype=jnp.int32)[:, None] == slot[None, :]).astype(jnp.bfloat16)
-    lane = jnp.arange(EXTRA, dtype=jnp.int32)
-    named = (route % EPG)[:, :, None] == lane[None, None, :]
-    weight_cols = jnp.sum(jnp.where(named, route_weight[..., None], 0.0), axis=1).astype(jnp.bfloat16)
-    rows = jnp.concatenate([moe_input, weight_cols], axis=1)
-    packed = jnp.dot(placing, rows, preferred_element_type=jnp.float32).astype(jnp.bfloat16)
+    placing, packed_weights = run(
+        place_body,
+        (
+            jax.ShapeDtypeStruct((slots, seq_count), BF16),
+            jax.ShapeDtypeStruct((slots, EXTRA), BF16),
+        ),
+        near(route.T),
+        near(route_weight.T),
+    )
+    packed = jnp.dot(placing, moe_input, preferred_element_type=F32).astype(BF16)
+    packed = jnp.concatenate([packed, packed_weights], axis=1)
     packed = jnp.broadcast_to(
         packed.reshape(-1, 1, GROUP_CAP, width + EXTRA),
         (slots // GROUP_CAP, chips_in_group, GROUP_CAP, width + EXTRA),
@@ -300,17 +395,18 @@
     arrived = lax.all_to_all(packed, CHIPS, 0, 0, tiled=True).reshape(-1, width + EXTRA)
     swap = [(i, cores - 1 - i) for i in range(cores)]
     other = lax.ppermute(arrived, CORE, swap)
+    lane = jnp.arange(EXTRA, dtype=jnp.int32)
     mine = (lane == lax.axis_index(EP) % EPG).astype(F32)[None]
 
     def expert(block, kind):
         return run(
             expert_body,
             jax.ShapeDtypeStruct((block.shape[0], width), kind),
-            block,
-            mine,
-            expert_gate[0],
-            expert_up[0],
-            expert_down[0],
+            near(block),
+            near(mine),
+            near(expert_gate[0]),
+            near(expert_up[0]),
+            near(expert_down[0]),
             flops=100_000_000,
         )
 

time: 126 us -> 107 us (0.85)
  other arithmetic: 10.5 us -> 1.22 us
  local copies, waits for them, and re-layouts: 9.75 us -> 2.64 us
  blocking collectives: 28.8 us -> 35.7 us
  Pallas kernels: 14.7 us -> 8.78 us
  starting transfers between devices: 35.3 us -> 31.8 us
    all_to_all x0 -> x1, blocking collectives: none -> 6.79 us  [shards(): attended_heads = lax.all_to_all(attended, 'tp', 0, 0, tiled=True)]
    pallas_call x6 -> x9, Pallas kernels: 14.7 us -> 8.78 us  [the longest x7 4.9 us: run(): pl.pallas_call(body, compiler_params=pltpu.CompilerParams(vmem_limit_byte...]
    unnamed x20 -> x21, local copies, waits for them, and re-layouts: 5.11 us -> 0.65 us
    all_to_all x1 -> x0, waiting for transfers between devices: 3.56 us -> none  [shards(): attended_heads = lax.all_to_all(attended, 'tp', 0, 0, tiled=True)]
    all_to_all x1 -> x0, starting transfers between devices: 3.26 us -> none  [shards(): attended_heads = lax.all_to_all(attended, 'tp', 0, 0, tiled=True)]
    convert_element_type x5 -> x0, other arithmetic: 2.42 us -> none  [the longest x1 0.92 us: shards(): rotated_keys = rotate_rows(cache_rope.astype(F32), positions).astype(BF16)]
    all_to_all x1, waiting for transfers between devices: 0.01 us -> 1.53 us  [shards(): latents = lax.all_to_all(both, 'tp', 0, 0, tiled=True)]
    select_n x2 -> x0, other arithmetic: 1.39 us -> none  [the longest x1 0.7 us: shards(): named = (route % EPG)[:, :, None] == lane[None, None, :]]
  transfers between devices with their start and end apart: 7 -> 6, of which waited for: 5 -> 6; matrix products, arithmetic and copies ran while one was open for 10% -> 2% of each run, Pallas kernels for 2% -> 2%
where the time goes in v3:
time: 107 us; the launch traced here: 106 us
  blocking collectives  35.7 us (33%)
  starting transfers between devices  31.8 us (30%)
  waiting for transfers between devices  24.5 us (23%)
  Pallas kernels  8.78 us (8%)
  local copies, waits for them, and re-layouts  2.64 us (2%)
  other arithmetic  1.22 us (1%)
    all_to_all x1, blocking collectives, shards(): lax.all_to_all(packed, CHIPS, 0, 0, tiled=True).reshape(-1, width + EXTRA)  28.9 us
    all_to_all x1, waiting for transfers between devices, shards(): lax.all_to_all(sums.reshape(chips * tp_count, GROUP_CAP, quarter_cols), (...  12.3 us
    all_to_all x1, starting transfers between devices, shards(): lax.all_to_all(sums.reshape(chips * tp_count, GROUP_CAP, quarter_cols), (...  9.15 us
    ppermute x1, starting transfers between devices, shards(): other = lax.ppermute(arrived, CORE, swap)  8.79 us
    all_to_all x1, blocking collectives, shards(): attended_heads = lax.all_to_all(attended, 'tp', 0, 0, tiled=True)  6.79 us
    pallas_call x7, Pallas kernels, run(): pl.pallas_call(body, compiler_params=pltpu.CompilerParams(vmem_limit_byte...  4.9 us
    all_to_all x1, starting transfers between devices, shards(): latents = lax.all_to_all(both, 'tp', 0, 0, tiled=True)  4.84 us
    all_to_all x1, waiting for transfers between devices, shards(): lax.all_to_all(partials, 'tp', 0, 0, tiled=True).astype(F32).sum(axis=0)  4.55 us
  transfers between devices with their start and end apart: 6, of which 6 were waited for; matrix products, arithmetic and copies ran while one was open for 2% of the time, Pallas kernels for 2%

profile of v3, /device:TPU:1, one launch (start us, length us, event | category | flops | bytes accessed | tf_op | source)
XLA Modules:
  0.0 106.5 jit_solution(14325819673171858025)
XLA Ops:
  0.6 2.0 %shard_map.238 = (bf16[4,32,128]{2,1,0:T(8,128)(2,1)}, bf16[16,32]{1,0:T(8,128)(2,1)S(1)}) custom-call(bf16[16,1024]{1,0:T(8,128)(2,1)} %refs_0_.1, f32[1,1024]{1,0:T(1,128)} %bitcast.33, bf16[1024,128]{1,0:T(8,128)(2,1)} %refs_2_.1, bf16[1024,128]{1,0:T(8,128)(2,1)} %refs_3_.1, bf16[32,1024]{1,0:T(8,128)(2,1)} %bitcast.32), custom_call_target="tpu_custom_call" | custom-call | flops 2000000 | bytes 626688 | tf_op jit(solution)/shard_map/pallas_call | solution.py:114
  2.6 4.8 %all-to-all-start = ((bf16[4,32,128]{2,1,0:T(8,128)(2,1)}), bf16[4,32,128]{2,1,0:T(8,128)(2,1)S(1)}, u32[]{:S(2)}, u32[]{:S(2)}) async-start(bf16[4,32,128]{2,1,0:T(8,128)(2,1)} %get-tuple-element.26), calls=%async_computation | async-start | bytes 65536 | tf_op jit(solution)/shard_map/all_to_all | solution.py:309
  7.5 0.7 convert_element_type.56
  8.3 1.9 %shard_map.239 = (bf16[192,512]{1,0:T(8,128)(2,1)S(1)}, bf16[512,128]{1,0:T(8,128)(2,1)S(1)}, f32[1,512]{1,0:T(1,128)S(1)}, f32[1,512]{1,0:T(1,128)S(1)}, f32[2,...) custom-call(bf16[192,512]{1,0:T(8,128)(2,1)} %bitcast.31, ...), custom_call_target="tpu_custom_call" | custom-call | flops 2000000 | bytes 2626304 | tf_op jit(solution)/shard_map/pallas_call | solution.py:80
  10.2 1.5 %all-to-all-done.arr_ref = bf16[4,32,128]{2,1,0:T(8,128)(2,1)S(1)} async-done(((bf16[4,32,128]{2,1,0:T(8,128)(2,1)}), bf16[4,32,128]{2,1,0:T(8,128)(2,1)S(1)}, u32[]{:S(2)}, u32[]{:S(2)}) %all-to-all-start) | async-done | bytes 32800 | tf_op jit(solution)/shard_map/all_to_all | solution.py:309
  11.8 1.2 %shard_map.240 = (bf16[4,8,544]{2,1,0:T(8,128)(2,1)}, bf16[16,512]{1,0:T(8,128)(2,1)S(1)}) custom-call(bf16[4,32,128]{2,1,0:T(8,128)(2,1)S(1)} %all-to-all-done.arr_ref, f32[1,512]{1,0:T(1,128)S(1)} %get-tuple-element.30.q_gain_ref, f32[1,512]{1,0:T(1,128)S(1)} %get-tuple-element.31.kv_gain_ref, bf16[192,512]{1,0:T(8,128)(2,1)S(1)} %get-tuple-element.32.q_up_ref, ...), custom_call_target="tpu_custom_call" | custom-call | flops 2000000 | bytes 367360 | tf_op jit(solution)/shard_map/pallas_call | solution.py:56
  13.0 3.4 %all-to-all-start.1 = ((bf16[4,8,544]{2,1,0:T(8,128)(2,1)}), bf16[4,8,544]{2,1,0:T(8,128)(2,1)S(1)}, u32[]{:S(2)}, u32[]{:S(2)}) async-start(bf16[4,8,544]{2,1,0:T(8,128)(2,1)} %get-tuple-element.38), calls=%async_computation.1 | async-start | bytes 81920 | tf_op jit(solution)/shard_map/all_to_all | solution.py:342
  16.5 4.3 %all-to-all-done.1.arr_ref = bf16[4,8,544]{2,1,0:T(8,128)(2,1)S(1)} async-done(((bf16[4,8,544]{2,1,0:T(8,128)(2,1)}), bf16[4,8,544]{2,1,0:T(8,128)(2,1)S(1)}, u32[]{:S(2)}, u32[]{:S(2)}) %all-to-all-start.1) | async-done | bytes 34848 | tf_op jit(solution)/shard_map/all_to_all | solution.py:342
  20.7 1.4 %shard_map.242 = bf16[4,8,512]{2,1,0:T(8,128)(2,1)S(1)} custom-call(s32[1]{0:T(128)} %bitcast.first_ref, bf16[4,8,544]{2,1,0:T(8,128)(2,1)S(1)} %all-to-all-done.1.arr_ref, bf16[4,512,512]{2,1,0:T(8,128)(2,1)S(1)} %get-tuple-element.39.cache_ref, bf16[4,32,512]{2,1,0:T(8,128)(2,1)S(1)} %shard_map.241.keys_ref, ...), custom_call_target="tpu_custom_call" | custom-call | flops 2000000 | bytes 2282564 | tf_op jit(solution)/shard_map/pallas_call | solution.py:56
  22.2 6.8 %all_to_all.30.arr_ref = bf16[4,8,512]{2,1,0:T(8,128)(2,1)S(1)} all-to-all(bf16[4,8,512]{2,1,0:T(8,128)(2,1)S(1)} %shard_map.242), channel_id=1, replica_groups=mesh['ep_0'=8,'ep_1'=8,'ep_2'=2,'tp'=4] {'tp'}, dimensions={0} | all-to-all | bytes 65536 | tf_op jit(solution)/shard_map/all_to_all | solution.py:365
  29.0 1.0 shard_map.243
  30.0 3.3 %all-to-all-start.3 = ((bf16[4,16,1024]{2,1,0:T(8,128)(2,1)}), bf16[4,16,1024]{2,1,0:T(8,128)(2,1)S(1)}, u32[]{:S(2)}, u32[]{:S(2)}) async-start(bf16[4,16,1024]{2,1,0:T(8,128)(2,1)} %shard_map.243), calls=%async_computation.3 | async-start | bytes 262144 | tf_op jit(solution)/shard_map/all_to_all | solution.py:373
  33.6 4.5 %all-to-all-done.3 = bf16[4,16,1024]{2,1,0:T(8,128)(2,1)S(1)} async-done(((bf16[4,16,1024]{2,1,0:T(8,128)(2,1)}), bf16[4,16,1024]{2,1,0:T(8,128)(2,1)S(1)}, u32[]{:S(2)}, u32[]{:S(2)}) %all-to-all-start.3) | async-done | bytes 131104 | tf_op jit(solution)/shard_map/all_to_all | solution.py:373
  38.8 28.9 %all_to_all.31 = bf16[64,2,1152]{2,1,0:T(2,128)(2,1)S(1)} all-to-all(bf16[64,2,1152]{2,1,0:T(2,128)(2,1)S(1)} %bitcast.30), channel_id=1, replica_groups=mesh['ep_0'=8,'ep_1'=8,'ep_2'=2,'tp'=4] {'ep_0','ep_1'}, dimensions={0} | all-to-all | bytes 589824 | tf_op jit(solution)/shard_map/all_to_all | solution.py:395
  67.7 8.8 %collective-permute-start = (bf16[128,1152]{1,0:T(8,128)(2,1)S(1)}, bf16[128,1152]{1,0:T(8,128)(2,1)S(1)}, u32[]{:S(2)}, u32[]{:S(2)}) collective-permute-start(bf16[128,1152]{1,0:T(8,128)(2,1)S(1)} %reshape.52.rows_ref), channel_id=1, source_target_pairs={{0,4},{4,0},{1,5},{5,1},{2,6},{6,2},{3,7},{7,3},{8,12},{12,8},{9,1... | collective-permute-start | bytes 884744 | tf_op jit(solution)/shard_map/ppermute | solution.py:397
  76.6 1.2 %collective-permute-done.rows_ref = bf16[128,1152]{1,0:T(8,128)(2,1)S(1)} collective-permute-done((bf16[128,1152]{1,0:T(8,128)(2,1)S(1)}, bf16[128,1152]{1,0:T(8,128)(2,1)S(1)}, u32[]{:S(2)}, u32[]{:S(2)}) %collective-permute-start) | collective-permute-done | bytes 294944 | tf_op jit(solution)/shard_map/ppermute | solution.py:397
  78.2 2.3 %collective-permute-start.1 = (bf16[128,1024]{1,0:T(8,128)(2,1)S(1)}, bf16[128,1024]{1,0:T(8,128)(2,1)S(1)}, u32[]{:S(2)}, u32[]{:S(2)}) collective-permute-start(bf16[128,1024]{1,0:T(8,128)(2,1)S(1)} %shard_map.246), channel_id=1, source_target_pairs={{0,4},{4,0},{1,5},{5,1},{2,6},{6,2},{3,7},{7,3},{8,12},{12,8},{9,1... | collective-permute-start | bytes 786440 | tf_op jit(solution)/shard_map/ppermute | solution.py:414
  81.0 0.7 collective-permute-done.1
  81.9 0.9 copy.26
  82.8 9.2 %all-to-all-start.5 = ((bf16[256,2,256]{2,1,0:T(2,128)(2,1)}), bf16[256,2,256]{2,1,0:T(2,128)(2,1)S(1)}, u32[]{:S(2)}, u32[]{:S(2)}) async-start(bf16[256,2,256]{2,1,0:T(2,128)(2,1)} %bitcast.14), calls=%async_computation.5 | async-start | bytes 524288 | tf_op jit(solution)/shard_map/all_to_all | solution.py:418
  91.9 0.6 copy.27
  92.5 0.6 constant_dynamic-slice_fusion
  93.1 12.3 %all-to-all-done.5 = bf16[256,2,256]{2,1,0:T(2,128)(2,1)S(1)} async-done(((bf16[256,2,256]{2,1,0:T(2,128)(2,1)}), bf16[256,2,256]{2,1,0:T(2,128)(2,1)S(1)}, u32[]{:S(2)}, u32[]{:S(2)}) %all-to-all-start.5) | async-done | bytes 262176 | tf_op jit(solution)/shard_map/all_to_all | solution.py:418
  105.7 0.8 fusion
  (39 shorter events, 2.5 us)
Async XLA Ops:
  0.6 20.1 %copy-start.7 = (s32[16]{0:T(128)S(1)}, s32[16]{0:T(128)}, u32[]{:S(2)}) copy-start(s32[16]{0:T(128)} %param.37) | copy-start | bytes 196
  2.6 9.1 %all-to-all-start = ((bf16[4,32,128]{2,1,0:T(8,128)(2,1)}), bf16[4,32,128]{2,1,0:T(8,128)(2,1)S(1)}, u32[]{:S(2)}, u32[]{:S(2)}) async-start(bf16[4,32,128]{2,1,0:T(8,128)(2,1)} %get-tuple-element.26), calls=%async_computation | async-start | bytes 65536 | tf_op jit(solution)/shard_map/all_to_all | solution.py:309
  10.2 18.8 %copy-start.3 = (bf16[128,1024]{1,0:T(8,128)(2,1)S(1)}, bf16[128,1024]{1,0:T(8,128)(2,1)}, u32[]{:S(2)}) copy-start(bf16[128,1024]{1,0:T(8,128)(2,1)} %out_w_ref.1) | copy-start | bytes 786436
  10.2 18.8 %copy-start.4 = (bf16[512,128]{1,0:T(8,128)(2,1)S(1)}, bf16[512,128]{1,0:T(8,128)(2,1)}, u32[]{:S(2)}) copy-start(bf16[512,128]{1,0:T(8,128)(2,1)} %value_ref.1) | copy-start | bytes 393220
  10.2 23.2 %copy-start.5 = (s32[16,6]{0,1:T(8,128)S(1)}, s32[16,6]{0,1:T(8,128)}, u32[]{:S(2)}) copy-start(s32[16,6]{0,1:T(8,128)} %param.39) | copy-start | bytes 1156
  10.2 23.2 %copy-start.6 = (f32[16,6]{0,1:T(8,128)S(1)}, f32[16,6]{0,1:T(8,128)}, u32[]{:S(2)}) copy-start(f32[16,6]{0,1:T(8,128)} %param.40) | copy-start | bytes 1156
  11.8 26.4 %copy-start.8 = (bf16[16,1024]{1,0:T(8,128)(2,1)S(1)}, bf16[16,1024]{1,0:T(8,128)(2,1)}, u32[]{:S(2)}) copy-start(bf16[16,1024]{1,0:T(8,128)(2,1)} %refs_0_.1) | copy-start | bytes 98308
  13.0 25.3 %copy-start.9 = (f32[1024]{0:T(1024)S(1)}, f32[1024]{0:T(1024)}, u32[]{:S(2)}) copy-start(f32[1024]{0:T(1024)} %param.38) | copy-start | bytes 12292
  13.0 7.7 %all-to-all-start.1 = ((bf16[4,8,544]{2,1,0:T(8,128)(2,1)}), bf16[4,8,544]{2,1,0:T(8,128)(2,1)S(1)}, u32[]{:S(2)}, u32[]{:S(2)}) async-start(bf16[4,8,544]{2,1,0:T(8,128)(2,1)} %get-tuple-element.38), calls=%async_computation.1 | async-start | bytes 81920 | tf_op jit(solution)/shard_map/all_to_all | solution.py:342
  22.2 55.6 %copy-start = (bf16[1,1024,128]{2,1,0:T(8,128)(2,1)S(1)}, bf16[1,1024,128]{2,1,0:T(8,128)(2,1)}, u32[]{:S(2)}) copy-start(bf16[1,1024,128]{2,1,0:T(8,128)(2,1)} %param.41) | copy-start | bytes 786436
  22.2 55.6 %copy-start.1 = (bf16[1,1024,128]{2,1,0:T(8,128)(2,1)S(1)}, bf16[1,1024,128]{2,1,0:T(8,128)(2,1)}, u32[]{:S(2)}) copy-start(bf16[1,1024,128]{2,1,0:T(8,128)(2,1)} %param.42) | copy-start | bytes 786436
  22.2 55.6 %copy-start.2 = (bf16[1,128,1024]{2,1,0:T(8,128)(2,1)S(1)}, bf16[1,128,1024]{2,1,0:T(8,128)(2,1)}, u32[]{:S(2)}) copy-start(bf16[1,128,1024]{2,1,0:T(8,128)(2,1)} %param.43) | copy-start | bytes 786436
  30.0 8.1 %all-to-all-start.3 = ((bf16[4,16,1024]{2,1,0:T(8,128)(2,1)}), bf16[4,16,1024]{2,1,0:T(8,128)(2,1)S(1)}, u32[]{:S(2)}, u32[]{:S(2)}) async-start(bf16[4,16,1024]{2,1,0:T(8,128)(2,1)} %shard_map.243), calls=%async_computation.3 | async-start | bytes 262144 | tf_op jit(solution)/shard_map/all_to_all | solution.py:373
  67.7 10.0 %collective-permute-start = (bf16[128,1152]{1,0:T(8,128)(2,1)S(1)}, bf16[128,1152]{1,0:T(8,128)(2,1)S(1)}, u32[]{:S(2)}, u32[]{:S(2)}) collective-permute-start(bf16[128,1152]{1,0:T(8,128)(2,1)S(1)} %reshape.52.rows_ref), channel_id=1, source_target_pairs={{0,4},{4,0},{1,5},{5,1},{2,6},{6,2},{3,7},{7,3},{8,12},{12,8},{9,1... | collective-permute-start | bytes 884744 | tf_op jit(solution)/shard_map/ppermute | solution.py:397
  78.2 3.4 %collective-permute-start.1 = (bf16[128,1024]{1,0:T(8,128)(2,1)S(1)}, bf16[128,1024]{1,0:T(8,128)(2,1)S(1)}, u32[]{:S(2)}, u32[]{:S(2)}) collective-permute-start(bf16[128,1024]{1,0:T(8,128)(2,1)S(1)} %shard_map.246), channel_id=1, source_target_pairs={{0,4},{4,0},{1,5},{5,1},{2,6},{6,2},{3,7},{7,3},{8,12},{12,8},{9,1... | collective-permute-start | bytes 786440 | tf_op jit(solution)/shard_map/ppermute | solution.py:414
  82.8 22.7 %all-to-all-start.5 = ((bf16[256,2,256]{2,1,0:T(2,128)(2,1)}), bf16[256,2,256]{2,1,0:T(2,128)(2,1)S(1)}, u32[]{:S(2)}, u32[]{:S(2)}) async-start(bf16[256,2,256]{2,1,0:T(2,128)(2,1)} %bitcast.14), calls=%async_computation.5 | async-start | bytes 524288 | tf_op jit(solution)/shard_map/all_to_all | solution.py:418

commit v4 on v3

v4 whole, which is shorter than its diff:
```python
import jax
import jax.numpy as jnp
import numpy as np
from jax import lax
from jax.experimental import pallas as pl
from jax.experimental.pallas import tpu as pltpu
from jax.sharding import Mesh
from jax.sharding import PartitionSpec as P

NOPE = 64
VDIM = 64
QK = 96
EPG = 8
EP = ("ep_0", "ep_1", "ep_2")
CHIPS = ("ep_0", "ep_1")
CORE = "ep_2"
GROUP_CAP = 2
EXTRA = 128
EP_TP = ("ep_0", "ep_1", "ep_2", "tp")


EPS = 1e-06
ROPE_BASE = 10000.0
F32 = jnp.float32
BF16 = jnp.bfloat16
NEG = -1e30


def rms_scaled(values_in, gain_vec):
    values_in = values_in.astype(jnp.float32)
    return (
        values_in
        * lax.rsqrt(jnp.mean(values_in * values_in, axis=-1, keepdims=True) + EPS)
        * gain_vec
    )


def dot(a, b):
    return jnp.dot(a, b, preferred_element_type=F32)


def dot_t(a, b):
    return lax.dot_general(a, b, (((1,), (1,)), ((), ())), preferred_element_type=F32)


def near(array):
    return pltpu.with_memory_space_constraint(array, pltpu.VMEM)


def far(array):
    return pltpu.with_memory_space_constraint(array, pltpu.HBM)


def run(body, outs, *args, flops=2_000_000, scalars=0, hbm_in=0, hbm_out=0, sems=0):
    moved = sum(a.size * a.dtype.itemsize for a in args)
    spaces = [pltpu.SMEM] * scalars + [pltpu.HBM] * hbm_in
    spaces += [pltpu.VMEM] * (len(args) - len(spaces))
    kinds = [pltpu.VMEM] * (len(outs) - hbm_out) + [pltpu.HBM] * hbm_out
    place_in = {pltpu.SMEM: lambda a: a, pltpu.HBM: far, pltpu.VMEM: near}
    return pl.pallas_call(
        body,
        compiler_params=pltpu.CompilerParams(vmem_limit_bytes=16 * 1024 * 1024),
        in_specs=[pl.BlockSpec(memory_space=kind) for kind in spaces],
        out_specs=[pl.BlockSpec(memory_space=kind) for kind in kinds],
        out_shape=[kind(o.shape, o.dtype) for kind, o in zip(kinds, outs)],
        scratch_shapes=[pltpu.SemaphoreType.DMA((sems,))] if sems else [],
        cost_estimate=pl.CostEstimate(flops=flops, transcendentals=0, bytes_accessed=moved),
    )(*[place_in[kind](a) for kind, a in zip(spaces, args)])


def place(route_ref, weight_ref, placing_ref, weights_ref):
    topk, rows = route_ref.shape
    slots = placing_ref.shape[0]
    group = route_ref[0:1, :] // EPG
    first = lax.broadcasted_iota(jnp.int32, (rows, rows), 0)
    second = lax.broadcasted_iota(jnp.int32, (rows, rows), 1)
    column = jnp.sum(jnp.where(first == second, group, 0), axis=1, keepdims=True)
    earlier = jnp.where((column == group) & (first < second), 1, 0)
    slot = group * GROUP_CAP + jnp.sum(earlier, axis=0, keepdims=True)
    placing = (lax.broadcasted_iota(jnp.int32, (slots, rows), 0) == slot).astype(BF16)
    placing_ref[...] = placing
    lane = lax.broadcasted_iota(jnp.int32, (EXTRA, rows), 0)
    table = jnp.zeros((EXTRA, rows), F32)
    for k in range(topk):
        table = table + jnp.where(route_ref[k : k + 1, :] % EPG == lane, weight_ref[k : k + 1, :], 0.0)
    weights_ref[...] = dot_t(placing, table.astype(BF16)).astype(BF16)


OWN = 9
MADE = 6


def down_body(*refs):
    count = (len(refs) - MADE - 1) // 2
    hbm, made, last = refs[:count], refs[count : count + MADE], refs[count + MADE : -1]
    sems = refs[-1]
    near_refs = last[count - OWN :] + last[: count - OWN]
    copies = [pltpu.make_async_copy(hbm[i], near_refs[i], sems.at[i]) for i in range(count)]
    for copy in copies:
        copy.start()
    tok_ref, gain_ref, q_ref, kv_ref, rope_ref, len_ref, turn_ref, route_ref, weight_ref = near_refs[
        :OWN
    ]
    both_ref, new_rope_ref, cos_ref, sin_ref, placing_ref, weights_ref = made
    copies[0].wait()
    copies[1].wait()
    normed = rms_scaled(tok_ref[...], gain_ref[...]).astype(BF16)
    rows = normed.shape[0]
    copies[2].wait()
    q_part = dot(normed, q_ref[...]).astype(BF16)
    copies[3].wait()
    kv_part = dot(normed, kv_ref[...]).astype(BF16)
    for i in range(both_ref.shape[0]):
        both_ref[i, :rows, :] = q_part
        both_ref[i, rows:, :] = kv_part
    for i in range(4, OWN):
        copies[i].wait()
    new_rope_ref[...] = dot_t(normed, rope_ref[...]).astype(BF16)
    first = lax.broadcasted_iota(jnp.int32, (rows, rows), 0)
    second = lax.broadcasted_iota(jnp.int32, (rows, rows), 1)
    lengths = jnp.sum(jnp.where(first == second, len_ref[...], 0), axis=1, keepdims=True)
    angles = lengths.astype(F32) * turn_ref[...]
    cos_ref[...] = jnp.cos(angles)
    sin_ref[...] = jnp.sin(angles)
    place(route_ref, weight_ref, placing_ref, weights_ref)
    for copy in copies[OWN:]:
        copy.wait()


def down(made, own, others):
    args = (*own, *others)
    moved = sum(a.size * a.dtype.itemsize for a in args)
    outs = [pltpu.VMEM(o.shape, o.dtype) for o in (*made, *others)]
    return pl.pallas_call(
        down_body,
        compiler_params=pltpu.CompilerParams(vmem_limit_bytes=16 * 1024 * 1024),
        in_specs=[pl.BlockSpec(memory_space=pltpu.HBM)] * len(args),
        out_specs=[pl.BlockSpec(memory_space=pltpu.VMEM)] * len(outs),
        out_shape=outs,
        scratch_shapes=[pltpu.VMEM(a.shape, a.dtype) for a in own]
        + [pltpu.SemaphoreType.DMA((len(args),))],
        cost_estimate=pl.CostEstimate(flops=2_000_000, transcendentals=0, bytes_accessed=moved),
    )(*[far(a) for a in args])


def query_body(
    index_ref, cache_hbm, arr_ref, q_gain_ref, kv_gain_ref, q_up_ref, head_gain_ref, key_up_ref,
    cos_ref, sin_ref, send_ref, latent_ref, mine_ref, cache_ref, sem,
):
    copy = pltpu.make_async_copy(cache_hbm, cache_ref, sem.at[0])
    copy.start()
    peers, both, cols = arr_ref.shape
    rows = both // 2
    rank = key_up_ref.shape[0]
    half = cos_ref.shape[1]
    q_raw = jnp.concatenate([arr_ref[i, :rows, :] for i in range(peers)], axis=1)
    kv_raw = jnp.concatenate([arr_ref[i, rows:, :] for i in range(peers)], axis=1)
    latent = rms_scaled(kv_raw, kv_gain_ref[...]).astype(BF16)
    latent_ref[...] = latent
    mine = latent[:, :cols]
    for i in range(1, peers):
        mine = jnp.where(index_ref[0] == i, latent[:, i * cols : (i + 1) * cols], mine)
    mine_ref[...] = mine
    q_lat = rms_scaled(q_raw, q_gain_ref[...]).astype(BF16)
    query = dot_t(q_lat, q_up_ref[...])
    each = rows // peers
    for h in range(head_gain_ref.shape[0]):
        one = rms_scaled(query[:, h * QK : (h + 1) * QK], head_gain_ref[h : h + 1, :])
        lower = one[:, NOPE : NOPE + half]
        upper = one[:, NOPE + half :]
        turned = jnp.concatenate(
            [
                lower * cos_ref[...] - upper * sin_ref[...],
                upper * cos_ref[...] + lower * sin_ref[...],
            ],
            axis=1,
        )
        absorbed = dot_t(one[:, :NOPE].astype(BF16), key_up_ref[:, h * NOPE : (h + 1) * NOPE])
        for i in range(peers):
            at = slice(h * each, (h + 1) * each)
            send_ref[i, at, :rank] = absorbed[i * each : (i + 1) * each].astype(BF16)
            send_ref[i, at, rank:] = turned[i * each : (i + 1) * each].astype(BF16)
    copy.wait()


def attend_body(
    index_ref, arr_ref, cache_ref, keys_ref, cos_table_ref, sin_table_ref, latent_ref, mine_ref,
    rope_ref, cos_ref, sin_ref, len_ref, out_ref, latent_out, rope_out, sems,
):
    copies = [
        pltpu.make_async_copy(mine_ref, latent_out, sems.at[0]),
        pltpu.make_async_copy(rope_ref, rope_out, sems.at[1]),
    ]
    for copy in copies:
        copy.start()
    seqs, places, rank = cache_ref.shape
    peers, each, _ = arr_ref.shape
    rows = peers * each
    half = cos_ref.shape[1]
    arrived = arr_ref[...].reshape(rows, arr_ref.shape[2])
    absorbed = arrived[:, :rank]
    turned = arrived[:, rank:]
    scale = QK ** (-0.5)
    row_seq = lax.broadcasted_iota(jnp.int32, (rows, 1), 0) % seqs
    every = latent_ref.shape[0]
    chosen = lax.broadcasted_iota(jnp.int32, (rows, every), 1) == row_seq + index_ref[0] * seqs
    lengths = jnp.sum(jnp.where(chosen, len_ref[...], 0), axis=1, keepdims=True)
    chosen = chosen.astype(BF16)
    latent = dot(chosen, latent_ref[...])
    lower = rope_ref[:, :half].astype(F32)
    upper = rope_ref[:, half:].astype(F32)
    key_new = jnp.concatenate(
        [
            lower * cos_ref[...] - upper * sin_ref[...],
            upper * cos_ref[...] + lower * sin_ref[...],
        ],
        axis=1,
    )
    key_new = dot(chosen, key_new.astype(BF16))
    self_score = (
        jnp.sum(absorbed.astype(F32) * latent, axis=1, keepdims=True)
        + jnp.sum(turned.astype(F32) * key_new, axis=1, keepdims=True)
    ) * scale
    scores = jnp.zeros((rows, places), F32)
    for s in range(seqs):
        below = keys_ref[s, :half, :].astype(F32)
        above = keys_ref[s, half:, :].astype(F32)
        keys = jnp.concatenate(
            [
                below * cos_table_ref[...] - above * sin_table_ref[...],
                above * cos_table_ref[...] + below * sin_table_ref[...],
            ],
            axis=0,
        ).astype(BF16)
        part = dot_t(absorbed, cache_ref[s]) + dot(turned, keys)
        scores = jnp.where(row_seq == s, part, scores)
    valid = lax.broadcasted_iota(jnp.int32, (rows, places), 1) < lengths
    scores = jnp.where(valid, scores * scale, NEG)
    top = jnp.maximum(jnp.max(scores, axis=1, keepdims=True), self_score)
    weights = jnp.where(valid, jnp.exp(scores - top), 0.0)
    self_weight = jnp.exp(self_score - top)
    total = jnp.sum(weights, axis=1, keepdims=True) + self_weight
    summed = self_weight.astype(BF16).astype(F32) * latent
    for s in range(seqs):
        summed = summed + dot(jnp.where(row_seq == s, weights, 0.0).astype(BF16), cache_ref[s])
    out_ref[...] = (summed / total).astype(BF16).reshape(out_ref.shape)
    for copy in copies:
        copy.wait()


def heads_body(arr_ref, value_ref, out_w_ref, out_ref):
    peers, each, rank = arr_ref.shape
    rows = peers * each
    heads = value_ref.shape[1] // VDIM
    seqs = each // heads
    values = dot(arr_ref[...].reshape(rows, rank), value_ref[...]).astype(BF16)
    to = lax.broadcasted_iota(jnp.int32, (rows // heads, rows), 0)
    at = lax.broadcasted_iota(jnp.int32, (rows // heads, rows), 1)
    column = lax.broadcasted_iota(jnp.int32, (rows // heads, heads * VDIM), 1)
    picked = jnp.zeros((rows // heads, heads * VDIM), F32)
    for h in range(heads):
        chosen = (at == (to // seqs) * each + h * seqs + to % seqs).astype(BF16)
        picked = jnp.where(column // VDIM == h, dot(chosen, values), picked)
    partial = dot(picked.astype(BF16), out_w_ref[...]).astype(BF16)
    for i in range(out_ref.shape[0]):
        out_ref[i] = partial


def expert_body(rows_ref, mine_ref, gate_ref, up_ref, down_ref, out_ref):
    width = down_ref.shape[1]
    inside = rows_ref[:, :width]
    gate_pre = dot(inside, gate_ref[...])
    up_pre = dot(inside, up_ref[...])
    hidden = (gate_pre / (1.0 + jnp.exp(-gate_pre)) * up_pre).astype(BF16)
    scale = jnp.sum(rows_ref[:, width:].astype(F32) * mine_ref[...], axis=1, keepdims=True)
    out_ref[...] = (dot(hidden, down_ref[...]) * scale).astype(out_ref.dtype)


def shards(
    tokens,
    attn_gain,
    q_down,
    kv_down,
    rope_down,
    q_latent_gain,
    kv_latent_gain,
    q_up,
    query_gain,
    key_up,
    value_up,
    attn_out,
    cache_latent,
    cache_rope,
    lengths,
    moe_gain,
    route,
    route_weight,
    expert_gate,
    expert_up,
    expert_down,
):
    tp_count = lax.axis_size("tp")
    tp_index = lax.axis_index("tp")
    seq_count, width = tokens.shape
    kv_cols = kv_down.shape[1]
    rank = cache_latent.shape[2]
    heads_here = query_gain.shape[0]
    seqs_mine = cache_latent.shape[0]
    index = tp_index.astype(jnp.int32)[None]
    half_dim = rope_down.shape[1] // 2
    each = heads_here * seqs_mine
    chips = lax.axis_size(CHIPS)
    cores = lax.axis_size(CORE)
    chips_in_group = EPG // cores
    slots = chips // chips_in_group * GROUP_CAP
    turns = ROPE_BASE ** (-np.arange(half_dim, dtype=np.float32) / np.float32(half_dim))
    turns = turns.astype(np.float32)
    angles = turns[:, None] * np.arange(cache_latent.shape[1], dtype=np.float32)
    cos_table = jnp.asarray(np.cos(angles.astype(np.float64)).astype(np.float32))
    sin_table = jnp.asarray(np.sin(angles.astype(np.float64)).astype(np.float32))
    (
        both, new_rope, cosines, sines, placing, packed_weights,
        q_up_t, key_near, q_gain, kv_gain, head_gain, cos_table, sin_table, keys, lens,
    ) = down(
        (
            jax.ShapeDtypeStruct((tp_count, 2 * seq_count, kv_cols), BF16),
            jax.ShapeDtypeStruct((seq_count, rope_down.shape[1]), BF16),
            jax.ShapeDtypeStruct((seq_count, half_dim), F32),
            jax.ShapeDtypeStruct((seq_count, half_dim), F32),
            jax.ShapeDtypeStruct((slots, seq_count), BF16),
            jax.ShapeDtypeStruct((slots, EXTRA), BF16),
        ),
        (
            tokens,
            attn_gain[None],
            q_down,
            kv_down,
            rope_down.T,
            lengths[None],
            jnp.asarray(turns[None]),
            route.T,
            route_weight.T,
        ),
        (
            q_up.T,
            key_up,
            q_latent_gain[None],
            kv_latent_gain[None],
            query_gain,
            cos_table,
            sin_table,
            cache_rope,
            lengths[None],
        ),
    )
    both, index = lax.optimization_barrier((both, index))
    latents = lax.all_to_all(both, "tp", 0, 0, tiled=True)
    send, latent_new, mine_new, cache = run(
        query_body,
        (
            jax.ShapeDtypeStruct((tp_count, each, rank + 2 * half_dim), BF16),
            jax.ShapeDtypeStruct((seq_count, rank), BF16),
            jax.ShapeDtypeStruct((seq_count, kv_cols), BF16),
            jax.ShapeDtypeStruct(cache_latent.shape, BF16),
        ),
        index,
        cache_latent,
        latents,
        q_gain,
        kv_gain,
        q_up_t,
        head_gain,
        key_near,
        cosines,
        sines,
        scalars=1,
        hbm_in=1,
        sems=1,
    )
    queries = lax.all_to_all(send, "tp", 0, 0, tiled=True)
    attended, new_latent, new_rope = run(
        attend_body,
        (
            jax.ShapeDtypeStruct((tp_count, each, rank), BF16),
            jax.ShapeDtypeStruct((seq_count, kv_cols), BF16),
            jax.ShapeDtypeStruct(new_rope.shape, BF16),
        ),
        index,
        queries,
        cache,
        keys,
        cos_table,
        sin_table,
        latent_new,
        mine_new,
        new_rope,
        cosines,
        sines,
        lens,
        scalars=1,
        hbm_out=2,
        sems=2,
    )
    attended_heads = lax.all_to_all(attended, "tp", 0, 0, tiled=True)
    (partials,) = run(
        heads_body,
        (jax.ShapeDtypeStruct((tp_count, seq_count, width), BF16),),
        attended_heads,
        value_up,
        attn_out,
    )
    head_sum = lax.all_to_all(partials, "tp", 0, 0, tiled=True).astype(F32).sum(axis=0)
    attn_resid = (tokens.astype(jnp.float32) + head_sum).astype(jnp.bfloat16)
    moe_input = rms_scaled(attn_resid, moe_gain).astype(jnp.bfloat16)
    packed = jnp.dot(placing, moe_input, preferred_element_type=F32).astype(BF16)
    packed = jnp.concatenate([packed, packed_weights], axis=1)
    packed = jnp.broadcast_to(
        packed.reshape(-1, 1, GROUP_CAP, width + EXTRA),
        (slots // GROUP_CAP, chips_in_group, GROUP_CAP, width + EXTRA),
    ).reshape(chips, GROUP_CAP, width + EXTRA)
    arrived = lax.all_to_all(packed, CHIPS, 0, 0, tiled=True).reshape(-1, width + EXTRA)
    swap = [(i, cores - 1 - i) for i in range(cores)]
    other = lax.ppermute(arrived, CORE, swap)
    lane = jnp.arange(EXTRA, dtype=jnp.int32)
    mine = (lane == lax.axis_index(EP) % EPG).astype(F32)[None]

    def expert(block, kind):
        return run(
            expert_body,
            (jax.ShapeDtypeStruct((block.shape[0], width), kind),),
            block,
            mine,
            expert_gate[0],
            expert_up[0],
            expert_down[0],
            flops=100_000_000,
        )[0]

    own = expert(arrived, F32)
    sent_back = lax.ppermute(expert(other, BF16), CORE, swap)
    quarter_cols = width // tp_count
    sums = (own + sent_back.astype(F32)).astype(BF16)
    sums, first_col = lax.optimization_barrier((sums, tp_index * quarter_cols))
    sums = sums.reshape(chips, GROUP_CAP, tp_count, quarter_cols).swapaxes(1, 2)
    returned = lax.all_to_all(
        sums.reshape(chips * tp_count, GROUP_CAP, quarter_cols), (*CHIPS, "tp"), 0, 0, tiled=True
    ).reshape(-1, chips_in_group * tp_count, GROUP_CAP, quarter_cols)
    totals = jnp.sum(returned.astype(F32), axis=1).reshape(slots, quarter_cols)
    high = totals.astype(BF16)
    picked = jnp.dot(placing.T, high, preferred_element_type=F32)
    residual = lax.dynamic_slice_in_dim(
        attn_resid, first_col, quarter_cols, 1, allow_negative_indices=False
    )
    mixed_out = (residual.astype(F32) + picked).astype(BF16)
    return (mixed_out, new_latent, new_rope)


def solution(mesh):
    torus = Mesh(mesh.devices.reshape(8, 8, 2, mesh.shape["tp"]), ("ep_0", "ep_1", "ep_2", "tp"))
    placed = (
        P(EP, None),
        P(),
        P(None, "tp"),
        P(None, "tp"),
        P(),
        P(),
        P(),
        P(None, "tp"),
        P("tp", None),
        P(None, "tp"),
        P(None, "tp"),
        P("tp", None),
        P(EP_TP, None, None),
        P(EP_TP, None, None),
        P(EP),
        P(),
        P(EP, None),
        P(EP, None),
        P(EP, None, "tp"),
        P(EP, None, "tp"),
        P(EP, "tp", None),
    )
    return jax.shard_map(
        shards,
        mesh=torus,
        in_specs=placed,
        out_specs=(P(EP, "tp"), P(EP, "tp"), P(EP, None)),
        check_vma=False,
    )
```

time: 107 us -> 104 us (0.972)
  blocking collectives: 35.7 us -> 81.2 us
  waiting for transfers between devices: 24.5 us -> 1.84 us
  starting transfers between devices: 31.8 us -> 11.1 us
  Pallas kernels: 8.78 us -> 6.11 us
  local copies, waits for them, and re-layouts: 2.64 us -> 0.74 us
    all_to_all x0 -> x4, blocking collectives: none -> 45.8 us  [the longest x1 22.7 us: shards(): lax.all_to_all(sums.reshape(chips * tp_count, GROUP_CAP, quarter_cols), (...]
    all_to_all x4 -> x0, waiting for transfers between devices: 22.7 us -> none  [the longest x1 12.3 us: shards(): lax.all_to_all(sums.reshape(chips * tp_count, GROUP_CAP, quarter_cols), (...]
    all_to_all x4 -> x0, starting transfers between devices: 20.7 us -> none  [the longest x1 9.15 us: shards(): lax.all_to_all(sums.reshape(chips * tp_count, GROUP_CAP, quarter_cols), (...]
    pallas_call x1 -> x0, Pallas kernels: 1.92 us -> none  [fetched(): pl.pallas_call(fetch_body, compiler_params=pltpu.CompilerParams(vmem_limi...]
    pallas_call x7 -> x5, Pallas kernels: 4.9 us -> 4.39 us  [run(): pl.pallas_call(body, compiler_params=pltpu.CompilerParams(vmem_limit_byte...]
  transfers between devices with their start and end apart: 6 -> 2, of which waited for: 6 -> 2; matrix products, arithmetic and copies ran while one was open for 2% -> 0% of each run, Pallas kernels for 2% -> 0%
where the time goes in v4:
time: 104 us; the launch traced here: 103 us
  blocking collectives  81.2 us (78%)
  starting transfers between devices  11.1 us (11%)
  Pallas kernels  6.11 us (6%)
  waiting for transfers between devices  1.84 us (2%)
    all_to_all x1, blocking collectives, shards(): lax.all_to_all(packed, CHIPS, 0, 0, tiled=True).reshape(-1, width + EXTRA)  28.7 us
    all_to_all x1, blocking collectives, shards(): lax.all_to_all(sums.reshape(chips * tp_count, GROUP_CAP, quarter_cols), (...  22.7 us
    all_to_all x1, blocking collectives, shards(): latents = lax.all_to_all(both, 'tp', 0, 0, tiled=True)  8.93 us
    ppermute x1, starting transfers between devices, shards(): other = lax.ppermute(arrived, CORE, swap)  8.81 us
    all_to_all x1, blocking collectives, shards(): lax.all_to_all(partials, 'tp', 0, 0, tiled=True).astype(F32).sum(axis=0)  7.39 us
    all_to_all x1, blocking collectives, shards(): attended_heads = lax.all_to_all(attended, 'tp', 0, 0, tiled=True)  6.79 us
    all_to_all x1, blocking collectives, shards(): queries = lax.all_to_all(send, 'tp', 0, 0, tiled=True)  6.7 us
    pallas_call x5, Pallas kernels, run(): pl.pallas_call(body, compiler_params=pltpu.CompilerParams(vmem_limit_byte...  4.39 us
  transfers between devices with their start and end apart: 2, of which 2 were waited for; matrix products, arithmetic and copies ran while one was open for 0% of the time, Pallas kernels for 0%

profile of v4, /device:TPU:1, one launch (start us, length us, event | category | flops | bytes accessed | tf_op | source)
XLA Modules:
  0.0 103.3 jit_solution(16074709134634701183)
XLA Ops:
  0.6 1.7 %shard_map.247 = (bf16[4,32,128]{2,1,0:T(8,128)(2,1)S(1)}, bf16[16,32]{1,0:T(8,128)(2,1)S(1)}, f32[16,16]{1,0:T(8,128)S(1)}, f32[16,16]{1,0:T(8,128)S(1)}, bf16[...) custom-call(bf16[16,1024]{1,0:T(8,128)(2,1)} %refs_0_.1, ...), custom_call_target="tpu_custom_call" | custom-call | flops 2000000 | bytes 1156800 | tf_op jit(solution)/shard_map/pallas_call | solution.py:134
  2.4 8.9 %all_to_all.30.arr_ref = bf16[4,32,128]{2,1,0:T(8,128)(2,1)S(1)} all-to-all(bf16[4,32,128]{2,1,0:T(8,128)(2,1)S(1)} %get-tuple-element.31), channel_id=1, replica_groups=mesh['ep_0'=8,'ep_1'=8,'ep_2'=2,'tp'=4] {'tp'}, dimensions={0} | all-to-all | bytes 65536 | tf_op jit(solution)/shard_map/all_to_all | solution.py:357
  11.3 1.7 %shard_map.248 = (bf16[4,8,544]{2,1,0:T(8,128)(2,1)S(1)}, bf16[16,512]{1,0:T(8,128)(2,1)S(1)}, bf16[16,128]{1,0:T(8,128)(2,1)S(1)}, bf16[4,512,512]{2,1,0:T(8,128)(2,1)S(1)}) custom-call(s32[1]{0:T(128)} %bitcast.8.index_ref, bf16[4,512,512]{2,1,0:T(8,128)(2,1)} %cache_hbm.1, bf16[4,32,128]{2,1,0:T(8,128)(2,1)S(1)} %all_to_all.30.arr_ref, ...), custom_call_target="tpu_custom_call" | custom-call | flops 2000000 | bytes 2464516 | tf_op jit(solution)/shard_map/pallas_call | solution.py:60
  13.0 6.7 %all_to_all.31.arr_ref = bf16[4,8,544]{2,1,0:T(8,128)(2,1)S(1)} all-to-all(bf16[4,8,544]{2,1,0:T(8,128)(2,1)S(1)} %get-tuple-element.39), channel_id=1, replica_groups=mesh['ep_0'=8,'ep_1'=8,'ep_2'=2,'tp'=4] {'tp'}, dimensions={0} | all-to-all | bytes 69632 | tf_op jit(solution)/shard_map/all_to_all | solution.py:380
  19.7 1.4 %shard_map.249 = (bf16[4,8,512]{2,1,0:T(8,128)(2,1)S(1)}, bf16[16,128]{1,0:T(8,128)(2,1)}, bf16[16,32]{1,0:T(8,128)(2,1)}) custom-call(s32[1]{0:T(128)} %bitcast.8.index_ref, bf16[4,8,544]{2,1,0:T(8,128)(2,1)S(1)} %all_to_all.31.arr_ref, bf16[4,512,512]{2,1,0:T(8,128)(2,1)S(1)} %get-tuple-element.40.cache_ref, ...), custom_call_target="tpu_custom_call" | custom-call | flops 2000000 | bytes 2352196 | tf_op jit(solution)/shard_map/pallas_call | solution.py:60
  21.2 6.8 %all_to_all.32.arr_ref = bf16[4,8,512]{2,1,0:T(8,128)(2,1)S(1)} all-to-all(bf16[4,8,512]{2,1,0:T(8,128)(2,1)S(1)} %get-tuple-element.48), channel_id=1, replica_groups=mesh['ep_0'=8,'ep_1'=8,'ep_2'=2,'tp'=4] {'tp'}, dimensions={0} | all-to-all | bytes 65536 | tf_op jit(solution)/shard_map/all_to_all | solution.py:404
  28.0 0.4 shard_map.250
  28.4 7.4 %all_to_all.33 = bf16[4,16,1024]{2,1,0:T(8,128)(2,1)S(1)} all-to-all(bf16[4,16,1024]{2,1,0:T(8,128)(2,1)S(1)} %shard_map.250), channel_id=1, replica_groups=mesh['ep_0'=8,'ep_1'=8,'ep_2'=2,'tp'=4] {'tp'}, dimensions={0} | all-to-all | bytes 262144 | tf_op jit(solution)/shard_map/all_to_all | solution.py:412
  35.8 0.1 fusion.1
  35.9 0.2 convolution_convert_fusion
  36.2 0.2 broadcast_in_dim.32
  36.4 28.7 %all_to_all.34 = bf16[64,2,1152]{2,1,0:T(2,128)(2,1)S(1)} all-to-all(bf16[64,2,1152]{2,1,0:T(2,128)(2,1)S(1)} %bitcast.27), channel_id=1, replica_groups=mesh['ep_0'=8,'ep_1'=8,'ep_2'=2,'tp'=4] {'ep_0','ep_1'}, dimensions={0} | all-to-all | bytes 589824 | tf_op jit(solution)/shard_map/all_to_all | solution.py:421
  65.0 0.1 reshape.45.rows_ref
  65.2 8.8 %collective-permute-start = (bf16[128,1152]{1,0:T(8,128)(2,1)S(1)}, bf16[128,1152]{1,0:T(8,128)(2,1)S(1)}, u32[]{:S(2)}, u32[]{:S(2)}) collective-permute-start(bf16[128,1152]{1,0:T(8,128)(2,1)S(1)} %reshape.45.rows_ref), channel_id=1, source_target_pairs={{0,4},{4,0},{1,5},{5,1},{2,6},{6,2},{3,7},{7,3},{8,12},{12,8},{9,1... | collective-permute-start | bytes 884744 | tf_op jit(solution)/shard_map/ppermute | solution.py:423
  74.0 1.2 %collective-permute-done.rows_ref = bf16[128,1152]{1,0:T(8,128)(2,1)S(1)} collective-permute-done((bf16[128,1152]{1,0:T(8,128)(2,1)S(1)}, bf16[128,1152]{1,0:T(8,128)(2,1)S(1)}, u32[]{:S(2)}, u32[]{:S(2)}) %collective-permute-start) | collective-permute-done | bytes 294944 | tf_op jit(solution)/shard_map/ppermute | solution.py:423
  75.2 0.5 shard_map.252
  75.6 2.3 %collective-permute-start.1 = (bf16[128,1024]{1,0:T(8,128)(2,1)S(1)}, bf16[128,1024]{1,0:T(8,128)(2,1)S(1)}, u32[]{:S(2)}, u32[]{:S(2)}) collective-permute-start(bf16[128,1024]{1,0:T(8,128)(2,1)S(1)} %shard_map.252), channel_id=1, source_target_pairs={{0,4},{4,0},{1,5},{5,1},{2,6},{6,2},{3,7},{7,3},{8,12},{12,8},{9,1... | collective-permute-start | bytes 786440 | tf_op jit(solution)/shard_map/ppermute | solution.py:440
  77.9 0.5 shard_map.251
  78.4 0.7 collective-permute-done.1
  79.1 0.2 reshape.46
  79.3 0.2 copy.27
  79.5 22.7 %all_to_all.35 = bf16[256,2,256]{2,1,0:T(2,128)(2,1)S(1)} all-to-all(bf16[256,2,256]{2,1,0:T(2,128)(2,1)S(1)} %bitcast.28), channel_id=1, replica_groups=mesh['ep_0'=8,'ep_1'=8,'ep_2'=2,'tp'=4] {'ep_0','ep_1','tp'}, dimensions={0} | all-to-all | bytes 524288 | tf_op jit(solution)/shard_map/all_to_all | solution.py:445
  102.3 0.2 bitcast_reduce_fusion
  102.5 0.8 fusion
  (21 shorter events, 0.2 us)
Async XLA Ops:
  11.3 16.7 %copy-start.3 = (bf16[128,1024]{1,0:T(8,128)(2,1)S(1)}, bf16[128,1024]{1,0:T(8,128)(2,1)}, u32[]{:S(2)}) copy-start(bf16[128,1024]{1,0:T(8,128)(2,1)} %out_w_ref.1) | copy-start | bytes 786436
  11.3 16.7 %copy-start.4 = (bf16[512,128]{1,0:T(8,128)(2,1)S(1)}, bf16[512,128]{1,0:T(8,128)(2,1)}, u32[]{:S(2)}) copy-start(bf16[512,128]{1,0:T(8,128)(2,1)} %value_ref.1) | copy-start | bytes 393220
  13.0 22.8 %copy-start.5 = (bf16[16,1024]{1,0:T(8,128)(2,1)S(1)}, bf16[16,1024]{1,0:T(8,128)(2,1)}, u32[]{:S(2)}) copy-start(bf16[16,1024]{1,0:T(8,128)(2,1)} %refs_0_.1) | copy-start | bytes 98308
  13.0 22.9 %copy-start.6 = (f32[1024]{0:T(1024)S(1)}, f32[1024]{0:T(1024)}, u32[]{:S(2)}) copy-start(f32[1024]{0:T(1024)} %param.39) | copy-start | bytes 12292
  21.1 54.0 %copy-start = (bf16[1,1024,128]{2,1,0:T(8,128)(2,1)S(1)}, bf16[1,1024,128]{2,1,0:T(8,128)(2,1)}, u32[]{:S(2)}) copy-start(bf16[1,1024,128]{2,1,0:T(8,128)(2,1)} %param.42) | copy-start | bytes 786436
  21.2 54.0 %copy-start.1 = (bf16[1,1024,128]{2,1,0:T(8,128)(2,1)S(1)}, bf16[1,1024,128]{2,1,0:T(8,128)(2,1)}, u32[]{:S(2)}) copy-start(bf16[1,1024,128]{2,1,0:T(8,128)(2,1)} %param.43) | copy-start | bytes 786436
  21.2 54.0 %copy-start.2 = (bf16[1,128,1024]{2,1,0:T(8,128)(2,1)S(1)}, bf16[1,128,1024]{2,1,0:T(8,128)(2,1)}, u32[]{:S(2)}) copy-start(bf16[1,128,1024]{2,1,0:T(8,128)(2,1)} %param.44) | copy-start | bytes 786436
  65.2 10.0 %collective-permute-start = (bf16[128,1152]{1,0:T(8,128)(2,1)S(1)}, bf16[128,1152]{1,0:T(8,128)(2,1)S(1)}, u32[]{:S(2)}, u32[]{:S(2)}) collective-permute-start(bf16[128,1152]{1,0:T(8,128)(2,1)S(1)} %reshape.45.rows_ref), channel_id=1, source_target_pairs={{0,4},{4,0},{1,5},{5,1},{2,6},{6,2},{3,7},{7,3},{8,12},{12,8},{9,1... | collective-permute-start | bytes 884744 | tf_op jit(solution)/shard_map/ppermute | solution.py:423
  75.6 3.4 %collective-permute-start.1 = (bf16[128,1024]{1,0:T(8,128)(2,1)S(1)}, bf16[128,1024]{1,0:T(8,128)(2,1)S(1)}, u32[]{:S(2)}, u32[]{:S(2)}) collective-permute-start(bf16[128,1024]{1,0:T(8,128)(2,1)S(1)} %shard_map.252), channel_id=1, source_target_pairs={{0,4},{4,0},{1,5},{5,1},{2,6},{6,2},{3,7},{7,3},{8,12},{12,8},{9,1... | collective-permute-start | bytes 786440 | tf_op jit(solution)/shard_map/ppermute | solution.py:440

commit v5 on v4

--- a/solution.py
+++ b/solution.py
@@ -184,13 +184,25 @@
 
 
 def attend_body(
-    index_ref, arr_ref, cache_ref, keys_ref, cos_table_ref, sin_table_ref, latent_ref, mine_ref,
-    rope_ref, cos_ref, sin_ref, len_ref, out_ref, latent_out, rope_out, sems,
+    index_ref, gate_hbm, up_hbm, down_hbm, arr_ref, cache_ref, keys_ref, cos_table_ref, sin_table_ref, latent_ref, mine_ref,
+    rope_ref, cos_ref, sin_ref, len_ref, out_ref, packed_ref, latent_out, rope_out, sems,
 ):
+    width, units = gate_hbm.shape
     copies = [
         pltpu.make_async_copy(mine_ref, latent_out, sems.at[0]),
         pltpu.make_async_copy(rope_ref, rope_out, sems.at[1]),
+        pltpu.make_async_copy(gate_hbm, packed_ref.at[:width], sems.at[2]),
+        pltpu.make_async_copy(up_hbm, packed_ref.at[width : 2 * width], sems.at[3]),
     ]
+    for j in range(width // units):
+        at = 2 * width + j * units
+        copies.append(
+            pltpu.make_async_copy(
+                down_hbm.at[:, j * units : (j + 1) * units],
+                packed_ref.at[at : at + units],
+                sems.at[4 + j],
+            )
+        )
     for copy in copies:
         copy.start()
     seqs, places, rank = cache_ref.shape
@@ -266,14 +278,25 @@
         out_ref[i] = partial
 
 
-def expert_body(rows_ref, mine_ref, gate_ref, up_ref, down_ref, out_ref):
-    width = down_ref.shape[1]
+def experts_body(index_ref, rows_ref, own_ref, other_ref, out_ref):
+    width = out_ref.shape[1]
+    units = own_ref.shape[1]
     inside = rows_ref[:, :width]
-    gate_pre = dot(inside, gate_ref[...])
-    up_pre = dot(inside, up_ref[...])
-    hidden = (gate_pre / (1.0 + jnp.exp(-gate_pre)) * up_pre).astype(BF16)
-    scale = jnp.sum(rows_ref[:, width:].astype(F32) * mine_ref[...], axis=1, keepdims=True)
-    out_ref[...] = (dot(hidden, down_ref[...]) * scale).astype(out_ref.dtype)
+    extra = rows_ref[:, width:].astype(F32)
+    lane = lax.broadcasted_iota(jnp.int32, extra.shape, 1)
+    here = index_ref[0]
+    there = here + 1 - 2 * (here % 2)
+    hidden, scales = [], []
+    for weights_ref, place_in in ((own_ref, here), (other_ref, there)):
+        gate_pre = dot(inside, weights_ref[:width, :])
+        up_pre = dot(inside, weights_ref[width : 2 * width, :])
+        hidden.append((gate_pre / (1.0 + jnp.exp(-gate_pre)) * up_pre).astype(BF16))
+        scales.append(jnp.sum(jnp.where(lane == place_in, extra, 0.0), axis=1, keepdims=True))
+    for j in range(width // units):
+        at = 2 * width + j * units
+        summed = dot(hidden[0], own_ref[at : at + units, :]) * scales[0]
+        summed = summed + dot(hidden[1], other_ref[at : at + units, :]) * scales[1]
+        out_ref[:, j * units : (j + 1) * units] = summed.astype(BF16)
 
 
 def shards(
@@ -353,7 +376,12 @@
             lengths[None],
         ),
     )
-    both, index = lax.optimization_barrier((both, index))
+    expert_here = (lax.axis_index(EP) % EPG).astype(jnp.int32)[None]
+    quarter_cols = width // tp_count
+    first_col = (tp_index * quarter_cols).astype(jnp.int32)
+    both, index, expert_here, first_col = lax.optimization_barrier(
+        (both, index, expert_here, first_col)
+    )
     latents = lax.all_to_all(both, "tp", 0, 0, tiled=True)
     send, latent_new, mine_new, cache = run(
         query_body,
@@ -378,14 +406,19 @@
         sems=1,
     )
     queries = lax.all_to_all(send, "tp", 0, 0, tiled=True)
-    attended, new_latent, new_rope = run(
+    units = expert_gate.shape[2]
+    attended, own_weights, new_latent, new_rope = run(
         attend_body,
         (
             jax.ShapeDtypeStruct((tp_count, each, rank), BF16),
+            jax.ShapeDtypeStruct((3 * width, units), BF16),
             jax.ShapeDtypeStruct((seq_count, kv_cols), BF16),
             jax.ShapeDtypeStruct(new_rope.shape, BF16),
         ),
         index,
+        expert_gate[0],
+        expert_up[0],
+        expert_down[0],
         queries,
         cache,
         keys,
@@ -398,9 +431,12 @@
         sines,
         lens,
         scalars=1,
+        hbm_in=3,
         hbm_out=2,
-        sems=2,
-    )
+        sems=4 + width // units,
+    )
+    swap = [(i, cores - 1 - i) for i in range(cores)]
+    other_weights = lax.ppermute(own_weights, CORE, swap)
     attended_heads = lax.all_to_all(attended, "tp", 0, 0, tiled=True)
     (partials,) = run(
         heads_body,
@@ -419,28 +455,16 @@
         (slots // GROUP_CAP, chips_in_group, GROUP_CAP, width + EXTRA),
     ).reshape(chips, GROUP_CAP, width + EXTRA)
     arrived = lax.all_to_all(packed, CHIPS, 0, 0, tiled=True).reshape(-1, width + EXTRA)
-    swap = [(i, cores - 1 - i) for i in range(cores)]
-    other = lax.ppermute(arrived, CORE, swap)
-    lane = jnp.arange(EXTRA, dtype=jnp.int32)
-    mine = (lane == lax.axis_index(EP) % EPG).astype(F32)[None]
-
-    def expert(block, kind):
-        return run(
-            expert_body,
-            (jax.ShapeDtypeStruct((block.shape[0], width), kind),),
-            block,
-            mine,
-            expert_gate[0],
-            expert_up[0],
-            expert_down[0],
-            flops=100_000_000,
-        )[0]
-
-    own = expert(arrived, F32)
-    sent_back = lax.ppermute(expert(other, BF16), CORE, swap)
-    quarter_cols = width // tp_count
-    sums = (own + sent_back.astype(F32)).astype(BF16)
-    sums, first_col = lax.optimization_barrier((sums, tp_index * quarter_cols))
+    (sums,) = run(
+        experts_body,
+        (jax.ShapeDtypeStruct((arrived.shape[0], width), BF16),),
+        expert_here,
+        arrived,
+        own_weights,
+        other_weights,
+        flops=100_000_000,
+        scalars=1,
+    )
     sums = sums.reshape(chips, GROUP_CAP, tp_count, quarter_cols).swapaxes(1, 2)
     returned = lax.all_to_all(
         sums.reshape(chips * tp_count, GROUP_CAP, quarter_cols), (*CHIPS, "tp"), 0, 0, tiled=True

time: 104 us -> 98.4 us (0.946)
  blocking collectives: 81.2 us -> 73.6 us
  starting transfers between devices: 11.1 us -> 13.2 us
  waiting for transfers between devices: 1.84 us -> 0.01 us
  Pallas kernels: 6.11 us -> 7.32 us
    all_to_all x1 -> x0, blocking collectives: 7.39 us -> none  [shards(): lax.all_to_all(partials, 'tp', 0, 0, tiled=True).astype(F32).sum(axis=0)]
    all_to_all x1, blocking collectives: 28.7 us -> 25.2 us  [shards(): lax.all_to_all(packed, CHIPS, 0, 0, tiled=True).reshape(-1, width + EXTRA)]
    all_to_all x0 -> x1, starting transfers between devices: none -> 3.32 us  [shards(): lax.all_to_all(partials, 'tp', 0, 0, tiled=True).astype(F32).sum(axis=0)]
    all_to_all x1, blocking collectives: 22.7 us -> 26 us  [shards(): lax.all_to_all(sums.reshape(chips * tp_count, GROUP_CAP, quarter_cols), (...]
    ppermute x2 -> x1, waiting for transfers between devices: 1.84 us -> 0.01 us  [shards(): other_weights = lax.ppermute(own_weights, CORE, swap)]
    pallas_call x5 -> x4, Pallas kernels: 4.39 us -> 5.6 us  [run(): pl.pallas_call(body, compiler_params=pltpu.CompilerParams(vmem_limit_byte...]
    ppermute x2 -> x1, starting transfers between devices: 11.1 us -> 9.92 us  [shards(): other_weights = lax.ppermute(own_weights, CORE, swap)]
  transfers between devices with their start and end apart: 2 -> 2, of which waited for: 2 -> 0; matrix products, arithmetic and copies ran while one was open for 0% -> 1% of each run, Pallas kernels for 0% -> 0%
where the time goes in v5:
time: 98.4 us; the launch traced here: 97.1 us
  blocking collectives  73.6 us (75%)
  starting transfers between devices  13.2 us (13%)
  Pallas kernels  7.32 us (7%)
    all_to_all x1, blocking collectives, shards(): lax.all_to_all(sums.reshape(chips * tp_count, GROUP_CAP, quarter_cols), (...  26 us
    all_to_all x1, blocking collectives, shards(): lax.all_to_all(packed, CHIPS, 0, 0, tiled=True).reshape(-1, width + EXTRA)  25.2 us
    ppermute x1, starting transfers between devices, shards(): other_weights = lax.ppermute(own_weights, CORE, swap)  9.92 us
    all_to_all x1, blocking collectives, shards(): latents = lax.all_to_all(both, 'tp', 0, 0, tiled=True)  8.93 us
    all_to_all x1, blocking collectives, shards(): queries = lax.all_to_all(send, 'tp', 0, 0, tiled=True)  6.83 us
    all_to_all x1, blocking collectives, shards(): attended_heads = lax.all_to_all(attended, 'tp', 0, 0, tiled=True)  6.65 us
    pallas_call x4, Pallas kernels, run(): pl.pallas_call(body, compiler_params=pltpu.CompilerParams(vmem_limit_byte...  5.6 us
    all_to_all x1, starting transfers between devices, shards(): lax.all_to_all(partials, 'tp', 0, 0, tiled=True).astype(F32).sum(axis=0)  3.32 us
  transfers between devices with their start and end apart: 2, of which 0 were waited for; matrix products, arithmetic and copies ran while one was open for 1% of the time, Pallas kernels for 0%

profile of v5, /device:TPU:1, one launch (start us, length us, event | category | flops | bytes accessed | tf_op | source)
XLA Modules:
  0.0 97.1 jit_solution(17388655436790350870)
XLA Ops:
  0.7 1.7 %shard_map.247 = (bf16[4,32,128]{2,1,0:T(8,128)(2,1)S(1)}, bf16[16,32]{1,0:T(8,128)(2,1)S(1)}, f32[16,16]{1,0:T(8,128)S(1)}, f32[16,16]{1,0:T(8,128)S(1)}, bf16[...) custom-call(bf16[16,1024]{1,0:T(8,128)(2,1)} %refs_0_.1, ...), custom_call_target="tpu_custom_call" | custom-call | flops 2000000 | bytes 1156800 | tf_op jit(solution)/shard_map/pallas_call | solution.py:134
  2.4 8.9 %all_to_all.30.arr_ref = bf16[4,32,128]{2,1,0:T(8,128)(2,1)S(1)} all-to-all(bf16[4,32,128]{2,1,0:T(8,128)(2,1)S(1)} %get-tuple-element.32), channel_id=1, replica_groups=mesh['ep_0'=8,'ep_1'=8,'ep_2'=2,'tp'=4] {'tp'}, dimensions={0} | all-to-all | bytes 65536 | tf_op jit(solution)/shard_map/all_to_all | solution.py:385
  11.3 1.6 %shard_map.248 = (bf16[4,8,544]{2,1,0:T(8,128)(2,1)S(1)}, bf16[16,512]{1,0:T(8,128)(2,1)S(1)}, bf16[16,128]{1,0:T(8,128)(2,1)S(1)}, bf16[4,512,512]{2,1,0:T(8,128)(2,1)S(1)}) custom-call(s32[1]{0:T(128)} %bitcast.8.index_ref, bf16[4,512,512]{2,1,0:T(8,128)(2,1)} %cache_hbm.1, bf16[4,32,128]{2,1,0:T(8,128)(2,1)S(1)} %all_to_all.30.arr_ref, ...), custom_call_target="tpu_custom_call" | custom-call | flops 2000000 | bytes 2464516 | tf_op jit(solution)/shard_map/pallas_call | solution.py:60
  12.9 0.0 copy-start
  12.9 0.0 copy-start.1
  12.9 6.8 %all_to_all.31.arr_ref = bf16[4,8,544]{2,1,0:T(8,128)(2,1)S(1)} all-to-all(bf16[4,8,544]{2,1,0:T(8,128)(2,1)S(1)} %get-tuple-element.40), channel_id=1, replica_groups=mesh['ep_0'=8,'ep_1'=8,'ep_2'=2,'tp'=4] {'tp'}, dimensions={0} | all-to-all | bytes 69632 | tf_op jit(solution)/shard_map/all_to_all | solution.py:408
  19.8 2.3 %shard_map.249 = (bf16[4,8,512]{2,1,0:T(8,128)(2,1)S(1)}, bf16[3072,128]{1,0:T(8,128)(2,1)S(1)}, bf16[16,128]{1,0:T(8,128)(2,1)}, bf16[16,32]{1,0:T(8,128)(2,1)}) custom-call(s32[1]{0:T(128)} %bitcast.8.index_ref, bf16[1024,128]{1,0:T(8,128)(2,1)} %bitcast.24, bf16[1024,128]{1,0:T(8,128)(2,1)} %bitcast.25, bf16[128,1024]{1,0:T(8,128)(2,1)} %bitcast.26, ...), custom_call_target="tpu_custom_call" | custom-call | flops 2000000 | bytes 3138628 | tf_op jit(solution)/shard_map/pallas_call | solution.py:60
  22.1 6.7 %all_to_all.32.arr_ref = bf16[4,8,512]{2,1,0:T(8,128)(2,1)S(1)} all-to-all(bf16[4,8,512]{2,1,0:T(8,128)(2,1)S(1)} %get-tuple-element.49), channel_id=1, replica_groups=mesh['ep_0'=8,'ep_1'=8,'ep_2'=2,'tp'=4] {'tp'}, dimensions={0} | all-to-all | bytes 65536 | tf_op jit(solution)/shard_map/all_to_all | solution.py:440
  28.7 1.0 %shard_map.250 = bf16[4,16,1024]{2,1,0:T(8,128)(2,1)} custom-call(bf16[4,8,512]{2,1,0:T(8,128)(2,1)S(1)} %all_to_all.32.arr_ref, bf16[512,128]{1,0:T(8,128)(2,1)S(1)} %copy-done.1, bf16[128,1024]{1,0:T(8,128)(2,1)S(1)} %copy-done), custom_call_target="tpu_custom_call" | custom-call | flops 2000000 | bytes 425984 | tf_op jit(solution)/shard_map/pallas_call | solution.py:60
  29.8 3.3 %all-to-all-start.3 = ((bf16[4,16,1024]{2,1,0:T(8,128)(2,1)}), bf16[4,16,1024]{2,1,0:T(8,128)(2,1)S(1)}, u32[]{:S(2)}, u32[]{:S(2)}) async-start(bf16[4,16,1024]{2,1,0:T(8,128)(2,1)} %shard_map.250), calls=%async_computation.3 | async-start | bytes 262144 | tf_op jit(solution)/shard_map/all_to_all | solution.py:448
  33.1 9.9 %collective-permute-start = (bf16[3072,128]{1,0:T(8,128)(2,1)S(1)}, bf16[3072,128]{1,0:T(8,128)(2,1)S(1)}, u32[]{:S(2)}, u32[]{:S(2)}) collective-permute-start(bf16[3072,128]{1,0:T(8,128)(2,1)S(1)} %get-tuple-element.54.own_ref), channel_id=1, source_target_pairs={{0,4},{4,0},{1,5},{5,1},{2,6},{6,2},{3,7},{7,3},{8,12},{12,8},{9,1... | collective-permute-start | bytes 2359304 | tf_op jit(solution)/shard_map/ppermute | solution.py:439
  43.0 0.0 all-to-all-done.3
  43.1 0.1 fusion.1
  43.2 0.2 convolution_convert_fusion
  43.5 0.2 broadcast_in_dim.35
  43.7 25.2 %all_to_all.33 = bf16[64,2,1152]{2,1,0:T(2,128)(2,1)S(1)} all-to-all(bf16[64,2,1152]{2,1,0:T(2,128)(2,1)S(1)} %bitcast.22), channel_id=1, replica_groups=mesh['ep_0'=8,'ep_1'=8,'ep_2'=2,'tp'=4] {'ep_0','ep_1'}, dimensions={0} | all-to-all | bytes 589824 | tf_op jit(solution)/shard_map/all_to_all | solution.py:457
  68.9 0.1 reshape.35.rows_ref
  69.0 0.0 collective-permute-done.other_ref
  69.0 0.7 shard_map.251
  69.7 0.2 reshape.36
  69.9 0.2 copy.27
  70.1 26.0 %all_to_all.34 = bf16[256,2,256]{2,1,0:T(2,128)(2,1)S(1)} all-to-all(bf16[256,2,256]{2,1,0:T(2,128)(2,1)S(1)} %bitcast.23), channel_id=1, replica_groups=mesh['ep_0'=8,'ep_1'=8,'ep_2'=2,'tp'=4] {'ep_0','ep_1','tp'}, dimensions={0} | all-to-all | bytes 524288 | tf_op jit(solution)/shard_map/all_to_all | solution.py:469
  96.1 0.2 bitcast_reduce_fusion
  96.3 0.8 fusion
  (11 shorter events, 0.1 us)
Async XLA Ops:
  12.9 15.8 %copy-start = (bf16[128,1024]{1,0:T(8,128)(2,1)S(1)}, bf16[128,1024]{1,0:T(8,128)(2,1)}, u32[]{:S(2)}) copy-start(bf16[128,1024]{1,0:T(8,128)(2,1)} %out_w_ref.1) | copy-start | bytes 786436
  12.9 15.8 %copy-start.1 = (bf16[512,128]{1,0:T(8,128)(2,1)S(1)}, bf16[512,128]{1,0:T(8,128)(2,1)}, u32[]{:S(2)}) copy-start(bf16[512,128]{1,0:T(8,128)(2,1)} %value_ref.1) | copy-start | bytes 393220
  19.8 23.3 %copy-start.2 = (bf16[16,1024]{1,0:T(8,128)(2,1)S(1)}, bf16[16,1024]{1,0:T(8,128)(2,1)}, u32[]{:S(2)}) copy-start(bf16[16,1024]{1,0:T(8,128)(2,1)} %refs_0_.1) | copy-start | bytes 98308
  19.8 23.4 %copy-start.3 = (f32[1024]{0:T(1024)S(1)}, f32[1024]{0:T(1024)}, u32[]{:S(2)}) copy-start(f32[1024]{0:T(1024)} %param.39) | copy-start | bytes 12292
  29.8 13.3 %all-to-all-start.3 = ((bf16[4,16,1024]{2,1,0:T(8,128)(2,1)}), bf16[4,16,1024]{2,1,0:T(8,128)(2,1)S(1)}, u32[]{:S(2)}, u32[]{:S(2)}) async-start(bf16[4,16,1024]{2,1,0:T(8,128)(2,1)} %shard_map.250), calls=%async_computation.3 | async-start | bytes 262144 | tf_op jit(solution)/shard_map/all_to_all | solution.py:448
  33.1 35.9 %collective-permute-start = (bf16[3072,128]{1,0:T(8,128)(2,1)S(1)}, bf16[3072,128]{1,0:T(8,128)(2,1)S(1)}, u32[]{:S(2)}, u32[]{:S(2)}) collective-permute-start(bf16[3072,128]{1,0:T(8,128)(2,1)S(1)} %get-tuple-element.54.own_ref), channel_id=1, source_target_pairs={{0,4},{4,0},{1,5},{5,1},{2,6},{6,2},{3,7},{7,3},{8,12},{12,8},{9,1... | collective-permute-start | bytes 2359304 | tf_op jit(solution)/shard_map/ppermute | solution.py:439

commit v6 on v5

--- a/solution.py
+++ b/solution.py
@@ -12,7 +12,7 @@
 QK = 96
 EPG = 8
 EP = ("ep_0", "ep_1", "ep_2")
-CHIPS = ("ep_0", "ep_1")
+CHIPS = ("ep_1", "ep_0")
 CORE = "ep_2"
 GROUP_CAP = 2
 EXTRA = 128
@@ -51,7 +51,7 @@
     return pltpu.with_memory_space_constraint(array, pltpu.HBM)
 
 
-def run(body, outs, *args, flops=2_000_000, scalars=0, hbm_in=0, hbm_out=0, sems=0):
+def run(body, outs, *args, flops=2_000_000, scalars=0, hbm_in=0, hbm_out=0, sems=0, scratch=()):
     moved = sum(a.size * a.dtype.itemsize for a in args)
     spaces = [pltpu.SMEM] * scalars + [pltpu.HBM] * hbm_in
     spaces += [pltpu.VMEM] * (len(args) - len(spaces))
@@ -63,15 +63,16 @@
         in_specs=[pl.BlockSpec(memory_space=kind) for kind in spaces],
         out_specs=[pl.BlockSpec(memory_space=kind) for kind in kinds],
         out_shape=[kind(o.shape, o.dtype) for kind, o in zip(kinds, outs)],
-        scratch_shapes=[pltpu.SemaphoreType.DMA((sems,))] if sems else [],
+        scratch_shapes=[*scratch] + ([pltpu.SemaphoreType.DMA((sems,))] if sems else []),
         cost_estimate=pl.CostEstimate(flops=flops, transcendentals=0, bytes_accessed=moved),
     )(*[place_in[kind](a) for kind, a in zip(spaces, args)])
 
 
-def place(route_ref, weight_ref, placing_ref, weights_ref):
+def place(route_ref, weight_ref, placing_ref, turned_ref, weights_ref, parts):
     topk, rows = route_ref.shape
     slots = placing_ref.shape[0]
     group = route_ref[0:1, :] // EPG
+    group = group % parts * (slots // GROUP_CAP // parts) + group // parts
     first = lax.broadcasted_iota(jnp.int32, (rows, rows), 0)
     second = lax.broadcasted_iota(jnp.int32, (rows, rows), 1)
     column = jnp.sum(jnp.where(first == second, group, 0), axis=1, keepdims=True)
@@ -79,6 +80,10 @@
     slot = group * GROUP_CAP + jnp.sum(earlier, axis=0, keepdims=True)
     placing = (lax.broadcasted_iota(jnp.int32, (slots, rows), 0) == slot).astype(BF16)
     placing_ref[...] = placing
+    slot_column = jnp.sum(jnp.where(first == second, slot, 0), axis=1, keepdims=True)
+    turned_ref[...] = (
+        lax.broadcasted_iota(jnp.int32, (rows, slots), 1) == slot_column
+    ).astype(BF16)
     lane = lax.broadcasted_iota(jnp.int32, (EXTRA, rows), 0)
     table = jnp.zeros((EXTRA, rows), F32)
     for k in range(topk):
@@ -87,10 +92,10 @@
 
 
 OWN = 9
-MADE = 6
-
-
-def down_body(*refs):
+MADE = 7
+
+
+def down_body(parts, *refs):
     count = (len(refs) - MADE - 1) // 2
     hbm, made, last = refs[:count], refs[count : count + MADE], refs[count + MADE : -1]
     sems = refs[-1]
@@ -101,7 +106,7 @@
     tok_ref, gain_ref, q_ref, kv_ref, rope_ref, len_ref, turn_ref, route_ref, weight_ref = near_refs[
         :OWN
     ]
-    both_ref, new_rope_ref, cos_ref, sin_ref, placing_ref, weights_ref = made
+    both_ref, new_rope_ref, cos_ref, sin_ref, placing_ref, turned_ref, weights_ref = made
     copies[0].wait()
     copies[1].wait()
     normed = rms_scaled(tok_ref[...], gain_ref[...]).astype(BF16)
@@ -122,17 +127,17 @@
     angles = lengths.astype(F32) * turn_ref[...]
     cos_ref[...] = jnp.cos(angles)
     sin_ref[...] = jnp.sin(angles)
-    place(route_ref, weight_ref, placing_ref, weights_ref)
+    place(route_ref, weight_ref, placing_ref, turned_ref, weights_ref, parts)
     for copy in copies[OWN:]:
         copy.wait()
 
 
-def down(made, own, others):
+def down(made, own, others, parts):
     args = (*own, *others)
     moved = sum(a.size * a.dtype.itemsize for a in args)
     outs = [pltpu.VMEM(o.shape, o.dtype) for o in (*made, *others)]
     return pl.pallas_call(
-        down_body,
+        lambda *refs: down_body(parts, *refs),
         compiler_params=pltpu.CompilerParams(vmem_limit_bytes=16 * 1024 * 1024),
         in_specs=[pl.BlockSpec(memory_space=pltpu.HBM)] * len(args),
         out_specs=[pl.BlockSpec(memory_space=pltpu.VMEM)] * len(outs),
@@ -184,25 +189,13 @@
 
 
 def attend_body(
-    index_ref, gate_hbm, up_hbm, down_hbm, arr_ref, cache_ref, keys_ref, cos_table_ref, sin_table_ref, latent_ref, mine_ref,
-    rope_ref, cos_ref, sin_ref, len_ref, out_ref, packed_ref, latent_out, rope_out, sems,
+    index_ref, arr_ref, cache_ref, keys_ref, cos_table_ref, sin_table_ref, latent_ref, mine_ref,
+    rope_ref, cos_ref, sin_ref, len_ref, out_ref, latent_out, rope_out, sems,
 ):
-    width, units = gate_hbm.shape
     copies = [
         pltpu.make_async_copy(mine_ref, latent_out, sems.at[0]),
         pltpu.make_async_copy(rope_ref, rope_out, sems.at[1]),
-        pltpu.make_async_copy(gate_hbm, packed_ref.at[:width], sems.at[2]),
-        pltpu.make_async_copy(up_hbm, packed_ref.at[width : 2 * width], sems.at[3]),
     ]
-    for j in range(width // units):
-        at = 2 * width + j * units
-        copies.append(
-            pltpu.make_async_copy(
-                down_hbm.at[:, j * units : (j + 1) * units],
-                packed_ref.at[at : at + units],
-                sems.at[4 + j],
-            )
-        )
     for copy in copies:
         copy.start()
     seqs, places, rank = cache_ref.shape
@@ -260,6 +253,27 @@
         copy.wait()
 
 
+def weights_body(gate_ref, up_ref, down_ref, out_ref):
+    width, units = gate_ref.shape
+    out_ref[:width, :] = gate_ref[...]
+    out_ref[width : 2 * width, :] = up_ref[...]
+    for j in range(width // units):
+        at = 2 * width + j * units
+        out_ref[at : at + units, :] = down_ref[:, j * units : (j + 1) * units]
+
+
+def moe_body(arr_ref, tok_ref, gain_ref, placing_ref, weights_ref, resid_ref, out_ref):
+    head_sum = arr_ref[0].astype(F32)
+    for i in range(1, arr_ref.shape[0]):
+        head_sum = head_sum + arr_ref[i].astype(F32)
+    resid = (tok_ref[...].astype(F32) + head_sum).astype(BF16)
+    resid_ref[...] = resid
+    width = resid.shape[1]
+    moe_input = rms_scaled(resid, gain_ref[...]).astype(BF16)
+    out_ref[:, :width] = dot(placing_ref[...], moe_input).astype(BF16)
+    out_ref[:, width:] = weights_ref[...]
+
+
 def heads_body(arr_ref, value_ref, out_w_ref, out_ref):
     peers, each, rank = arr_ref.shape
     rows = peers * each
@@ -279,7 +293,8 @@
 
 
 def experts_body(index_ref, rows_ref, own_ref, other_ref, out_ref):
-    width = out_ref.shape[1]
+    chips, quarters, cap, quarter = out_ref.shape
+    width = quarters * quarter
     units = own_ref.shape[1]
     inside = rows_ref[:, :width]
     extra = rows_ref[:, width:].astype(F32)
@@ -292,11 +307,33 @@
         up_pre = dot(inside, weights_ref[width : 2 * width, :])
         hidden.append((gate_pre / (1.0 + jnp.exp(-gate_pre)) * up_pre).astype(BF16))
         scales.append(jnp.sum(jnp.where(lane == place_in, extra, 0.0), axis=1, keepdims=True))
-    for j in range(width // units):
-        at = 2 * width + j * units
-        summed = dot(hidden[0], own_ref[at : at + units, :]) * scales[0]
-        summed = summed + dot(hidden[1], other_ref[at : at + units, :]) * scales[1]
-        out_ref[:, j * units : (j + 1) * units] = summed.astype(BF16)
+    for q in range(quarters):
+        pieces = []
+        for j in range(q * quarter // units, (q + 1) * quarter // units):
+            at = 2 * width + j * units
+            summed = dot(hidden[0], own_ref[at : at + units, :]) * scales[0]
+            pieces.append(summed + dot(hidden[1], other_ref[at : at + units, :]) * scales[1])
+        whole = jnp.concatenate(pieces, axis=1).astype(BF16)
+        out_ref[:, q] = whole.reshape(chips, cap, quarter)
+
+
+def mix_body(index_ref, arr_ref, placing_ref, resid_ref, out_hbm, out_ref, sem):
+    parts, near_chips, planes, quarters, cap, quarter = arr_ref.shape
+    totals = []
+    for p in range(parts):
+        total = jnp.zeros((planes, cap, quarter), F32)
+        for y in range(near_chips):
+            for x in range(quarters):
+                total = total + arr_ref[p, y, :, x].astype(F32)
+        totals.append(total.reshape(planes * cap, quarter))
+    picked = dot(placing_ref[...], jnp.concatenate(totals, axis=0).astype(BF16))
+    resid = resid_ref[:, :quarter]
+    for i in range(1, quarters):
+        resid = jnp.where(index_ref[0] == i, resid_ref[:, i * quarter : (i + 1) * quarter], resid)
+    out_ref[...] = (resid.astype(F32) + picked).astype(BF16)
+    copy = pltpu.make_async_copy(out_ref, out_hbm, sem.at[0])
+    copy.start()
+    copy.wait()
 
 
 def shards(
@@ -336,13 +373,15 @@
     cores = lax.axis_size(CORE)
     chips_in_group = EPG // cores
     slots = chips // chips_in_group * GROUP_CAP
+    planes = lax.axis_size(CHIPS[1])
+    parts = chips // planes // chips_in_group
     turns = ROPE_BASE ** (-np.arange(half_dim, dtype=np.float32) / np.float32(half_dim))
     turns = turns.astype(np.float32)
     angles = turns[:, None] * np.arange(cache_latent.shape[1], dtype=np.float32)
     cos_table = jnp.asarray(np.cos(angles.astype(np.float64)).astype(np.float32))
     sin_table = jnp.asarray(np.sin(angles.astype(np.float64)).astype(np.float32))
     (
-        both, new_rope, cosines, sines, placing, packed_weights,
+        both, new_rope, cosines, sines, placing, placing_t, packed_weights,
         q_up_t, key_near, q_gain, kv_gain, head_gain, cos_table, sin_table, keys, lens,
     ) = down(
         (
@@ -351,6 +390,7 @@
             jax.ShapeDtypeStruct((seq_count, half_dim), F32),
             jax.ShapeDtypeStruct((seq_count, half_dim), F32),
             jax.ShapeDtypeStruct((slots, seq_count), BF16),
+            jax.ShapeDtypeStruct((seq_count, slots), BF16),
             jax.ShapeDtypeStruct((slots, EXTRA), BF16),
         ),
         (
@@ -375,13 +415,11 @@
             cache_rope,
             lengths[None],
         ),
+        parts,
     )
     expert_here = (lax.axis_index(EP) % EPG).astype(jnp.int32)[None]
     quarter_cols = width // tp_count
-    first_col = (tp_index * quarter_cols).astype(jnp.int32)
-    both, index, expert_here, first_col = lax.optimization_barrier(
-        (both, index, expert_here, first_col)
-    )
+    both, index, expert_here = lax.optimization_barrier((both, index, expert_here))
     latents = lax.all_to_all(both, "tp", 0, 0, tiled=True)
     send, latent_new, mine_new, cache = run(
         query_body,
@@ -407,18 +445,14 @@
     )
     queries = lax.all_to_all(send, "tp", 0, 0, tiled=True)
     units = expert_gate.shape[2]
-    attended, own_weights, new_latent, new_rope = run(
+    attended, new_latent, new_rope = run(
         attend_body,
         (
             jax.ShapeDtypeStruct((tp_count, each, rank), BF16),
-            jax.ShapeDtypeStruct((3 * width, units), BF16),
             jax.ShapeDtypeStruct((seq_count, kv_cols), BF16),
             jax.ShapeDtypeStruct(new_rope.shape, BF16),
         ),
         index,
-        expert_gate[0],
-        expert_up[0],
-        expert_down[0],
         queries,
         cache,
         keys,
@@ -431,12 +465,9 @@
         sines,
         lens,
         scalars=1,
-        hbm_in=3,
         hbm_out=2,
-        sems=4 + width // units,
-    )
-    swap = [(i, cores - 1 - i) for i in range(cores)]
-    other_weights = lax.ppermute(own_weights, CORE, swap)
+        sems=2,
+    )
     attended_heads = lax.all_to_all(attended, "tp", 0, 0, tiled=True)
     (partials,) = run(
         heads_body,
@@ -445,19 +476,35 @@
         value_up,
         attn_out,
     )
-    head_sum = lax.all_to_all(partials, "tp", 0, 0, tiled=True).astype(F32).sum(axis=0)
-    attn_resid = (tokens.astype(jnp.float32) + head_sum).astype(jnp.bfloat16)
-    moe_input = rms_scaled(attn_resid, moe_gain).astype(jnp.bfloat16)
-    packed = jnp.dot(placing, moe_input, preferred_element_type=F32).astype(BF16)
-    packed = jnp.concatenate([packed, packed_weights], axis=1)
+    partials, gate, up, lower = lax.optimization_barrier(
+        (partials, expert_gate[0], expert_up[0], expert_down[0])
+    )
+    summands = lax.all_to_all(partials, "tp", 0, 0, tiled=True)
+    (own_weights,) = run(
+        weights_body, (jax.ShapeDtypeStruct((3 * width, units), BF16),), gate, up, lower
+    )
+    swap = [(i, cores - 1 - i) for i in range(cores)]
+    other_weights = lax.ppermute(own_weights, CORE, swap)
+    attn_resid, packed = run(
+        moe_body,
+        (
+            jax.ShapeDtypeStruct((seq_count, width), BF16),
+            jax.ShapeDtypeStruct((slots, width + EXTRA), BF16),
+        ),
+        summands,
+        tokens,
+        moe_gain[None],
+        placing,
+        packed_weights,
+    )
     packed = jnp.broadcast_to(
-        packed.reshape(-1, 1, GROUP_CAP, width + EXTRA),
-        (slots // GROUP_CAP, chips_in_group, GROUP_CAP, width + EXTRA),
+        packed.reshape(parts, 1, planes, GROUP_CAP, width + EXTRA),
+        (parts, chips_in_group, planes, GROUP_CAP, width + EXTRA),
     ).reshape(chips, GROUP_CAP, width + EXTRA)
     arrived = lax.all_to_all(packed, CHIPS, 0, 0, tiled=True).reshape(-1, width + EXTRA)
     (sums,) = run(
         experts_body,
-        (jax.ShapeDtypeStruct((arrived.shape[0], width), BF16),),
+        (jax.ShapeDtypeStruct((chips, tp_count, GROUP_CAP, quarter_cols), BF16),),
         expert_here,
         arrived,
         own_weights,
@@ -465,17 +512,21 @@
         flops=100_000_000,
         scalars=1,
     )
-    sums = sums.reshape(chips, GROUP_CAP, tp_count, quarter_cols).swapaxes(1, 2)
     returned = lax.all_to_all(
         sums.reshape(chips * tp_count, GROUP_CAP, quarter_cols), (*CHIPS, "tp"), 0, 0, tiled=True
-    ).reshape(-1, chips_in_group * tp_count, GROUP_CAP, quarter_cols)
-    totals = jnp.sum(returned.astype(F32), axis=1).reshape(slots, quarter_cols)
-    high = totals.astype(BF16)
-    picked = jnp.dot(placing.T, high, preferred_element_type=F32)
-    residual = lax.dynamic_slice_in_dim(
-        attn_resid, first_col, quarter_cols, 1, allow_negative_indices=False
-    )
-    mixed_out = (residual.astype(F32) + picked).astype(BF16)
+    ).reshape(parts, chips_in_group, planes, tp_count, GROUP_CAP, quarter_cols)
+    (mixed_out,) = run(
+        mix_body,
+        (jax.ShapeDtypeStruct((seq_count, quarter_cols), BF16),),
+        index,
+        returned,
+        placing_t,
+        attn_resid,
+        scalars=1,
+        hbm_out=1,
+        sems=1,
+        scratch=(pltpu.VMEM((seq_count, quarter_cols), BF16),),
+    )
     return (mixed_out, new_latent, new_rope)
 
 

time: 98.4 us -> 98 us (level)
  blocking collectives: 73.6 us -> 78.3 us
  starting transfers between devices: 13.2 us -> 9.92 us
    all_to_all x0 -> x1, blocking collectives: none -> 7.44 us  [shards(): summands = lax.all_to_all(partials, 'tp', 0, 0, tiled=True)]
    all_to_all x1 -> x0, starting transfers between devices: 3.32 us -> none  [shards(): lax.all_to_all(partials, 'tp', 0, 0, tiled=True).astype(F32).sum(axis=0)]
    all_to_all x1, blocking collectives: 26 us -> 23.2 us  [shards(): lax.all_to_all(sums.reshape(chips * tp_count, GROUP_CAP, quarter_cols), (...]
    pallas_call x4 -> x7, Pallas kernels: 5.6 us -> 5.28 us  [run(): pl.pallas_call(body, compiler_params=pltpu.CompilerParams(vmem_limit_byte...]
  transfers between devices with their start and end apart: 2 -> 1, of which waited for: 0 -> 0; matrix products, arithmetic and copies ran while one was open for 1% -> 0% of each run, Pallas kernels for 0% -> 0%
where the time goes in v6:
time: 98 us; the launch traced here: 96.3 us
  blocking collectives  78.3 us (80%)
  starting transfers between devices  9.92 us (10%)
  Pallas kernels  7.01 us (7%)
    all_to_all x1, blocking collectives, shards(): lax.all_to_all(packed, CHIPS, 0, 0, tiled=True).reshape(-1, width + EXTRA)  25.2 us
    all_to_all x1, blocking collectives, shards(): lax.all_to_all(sums.reshape(chips * tp_count, GROUP_CAP, quarter_cols), (...  23.2 us
    ppermute x1, starting transfers between devices, shards(): other_weights = lax.ppermute(own_weights, CORE, swap)  9.92 us
    all_to_all x1, blocking collectives, shards(): latents = lax.all_to_all(both, 'tp', 0, 0, tiled=True)  8.93 us
    all_to_all x1, blocking collectives, shards(): summands = lax.all_to_all(partials, 'tp', 0, 0, tiled=True)  7.44 us
    all_to_all x1, blocking collectives, shards(): queries = lax.all_to_all(send, 'tp', 0, 0, tiled=True)  6.83 us
    all_to_all x1, blocking collectives, shards(): attended_heads = lax.all_to_all(attended, 'tp', 0, 0, tiled=True)  6.65 us
    pallas_call x7, Pallas kernels, run(): pl.pallas_call(body, compiler_params=pltpu.CompilerParams(vmem_limit_byte...  5.28 us
  transfers between devices with their start and end apart: 1, of which 0 were waited for; matrix products, arithmetic and copies ran while one was open for 0% of the time, Pallas kernels for 0%

profile of v6, /device:TPU:1, one launch (start us, length us, event | category | flops | bytes accessed | tf_op | source)
XLA Modules:
  0.0 96.3 jit_solution(12567901647557489127)
XLA Ops:
  0.7 1.7 %shard_map.247 = (bf16[4,32,128]{2,1,0:T(8,128)(2,1)S(1)}, bf16[16,32]{1,0:T(8,128)(2,1)S(1)}, f32[16,16]{1,0:T(8,128)S(1)}, f32[16,16]{1,0:T(8,128)S(1)}, bf16[...) custom-call(bf16[16,1024]{1,0:T(8,128)(2,1)} %tok_ref.1, ...), custom_call_target="tpu_custom_call" | custom-call | flops 2000000 | bytes 1156800 | tf_op jit(solution)/shard_map/pallas_call | solution.py:139
  2.4 8.9 %all_to_all.30.arr_ref = bf16[4,32,128]{2,1,0:T(8,128)(2,1)S(1)} all-to-all(bf16[4,32,128]{2,1,0:T(8,128)(2,1)S(1)} %get-tuple-element.38), channel_id=1, replica_groups=mesh['ep_0'=8,'ep_1'=8,'ep_2'=2,'tp'=4] {'tp'}, dimensions={0} | all-to-all | bytes 65536 | tf_op jit(solution)/shard_map/all_to_all | solution.py:423
  11.3 1.7 %shard_map.248 = (bf16[4,8,544]{2,1,0:T(8,128)(2,1)S(1)}, bf16[16,512]{1,0:T(8,128)(2,1)S(1)}, bf16[16,128]{1,0:T(8,128)(2,1)S(1)}, bf16[4,512,512]{2,1,0:T(8,128)(2,1)S(1)}) custom-call(s32[1]{0:T(128)} %bitcast.8.index_ref, bf16[4,512,512]{2,1,0:T(8,128)(2,1)} %cache_hbm.1, bf16[4,32,128]{2,1,0:T(8,128)(2,1)S(1)} %all_to_all.30.arr_ref, ...), custom_call_target="tpu_custom_call" | custom-call | flops 2000000 | bytes 2464516 | tf_op jit(solution)/shard_map/pallas_call | solution.py:60
  13.0 0.0 copy-start.1
  13.0 0.0 copy-start.2
  13.0 0.0 copy-start.3
  13.0 6.8 %all_to_all.31.arr_ref = bf16[4,8,544]{2,1,0:T(8,128)(2,1)S(1)} all-to-all(bf16[4,8,544]{2,1,0:T(8,128)(2,1)S(1)} %get-tuple-element.46), channel_id=1, replica_groups=mesh['ep_0'=8,'ep_1'=8,'ep_2'=2,'tp'=4] {'tp'}, dimensions={0} | all-to-all | bytes 69632 | tf_op jit(solution)/shard_map/all_to_all | solution.py:446
  19.9 1.4 %shard_map.249 = (bf16[4,8,512]{2,1,0:T(8,128)(2,1)S(1)}, bf16[16,128]{1,0:T(8,128)(2,1)}, bf16[16,32]{1,0:T(8,128)(2,1)}) custom-call(s32[1]{0:T(128)} %bitcast.8.index_ref, bf16[4,8,544]{2,1,0:T(8,128)(2,1)S(1)} %all_to_all.31.arr_ref, bf16[4,512,512]{2,1,0:T(8,128)(2,1)S(1)} %get-tuple-element.47.cache_ref, ...), custom_call_target="tpu_custom_call" | custom-call | flops 2000000 | bytes 2352196 | tf_op jit(solution)/shard_map/pallas_call | solution.py:60
  21.3 6.7 %all_to_all.32.arr_ref = bf16[4,8,512]{2,1,0:T(8,128)(2,1)S(1)} all-to-all(bf16[4,8,512]{2,1,0:T(8,128)(2,1)S(1)} %get-tuple-element.55), channel_id=1, replica_groups=mesh['ep_0'=8,'ep_1'=8,'ep_2'=2,'tp'=4] {'tp'}, dimensions={0} | all-to-all | bytes 65536 | tf_op jit(solution)/shard_map/all_to_all | solution.py:471
  28.0 0.0 copy-done
  28.0 0.0 copy-done.4
  28.0 0.4 shard_map.250
  28.4 0.0 copy-done.1
  28.4 0.1 shard_map.252.own_ref
  28.5 9.9 %collective-permute-start = (bf16[3072,128]{1,0:T(8,128)(2,1)S(1)}, bf16[3072,128]{1,0:T(8,128)(2,1)S(1)}, u32[]{:S(2)}, u32[]{:S(2)}) collective-permute-start(bf16[3072,128]{1,0:T(8,128)(2,1)S(1)} %shard_map.252.own_ref), channel_id=1, source_target_pairs={{0,4},{4,0},{1,5},{5,1},{2,6},{6,2},{3,7},{7,3},{8,12},{12,8},{9,1... | collective-permute-start | bytes 2359304 | tf_op jit(solution)/shard_map/ppermute | solution.py:487
  38.4 7.4 %all_to_all.33.arr_ref = bf16[4,16,1024]{2,1,0:T(8,128)(2,1)S(1)} all-to-all(bf16[4,16,1024]{2,1,0:T(8,128)(2,1)S(1)} %shard_map.250), channel_id=1, replica_groups=mesh['ep_0'=8,'ep_1'=8,'ep_2'=2,'tp'=4] {'tp'}, dimensions={0} | all-to-all | bytes 262144 | tf_op jit(solution)/shard_map/all_to_all | solution.py:482
  45.9 0.2 shard_map.251
  46.2 0.2 broadcast_in_dim.37
  46.3 25.2 %all_to_all.34 = bf16[64,2,1152]{2,1,0:T(2,128)(2,1)S(1)} all-to-all(bf16[64,2,1152]{2,1,0:T(2,128)(2,1)S(1)} %bitcast.23), channel_id=1, replica_groups=mesh['ep_0'=8,'ep_1'=8,'ep_2'=2,'tp'=4] {'ep_1','ep_0'}, dimensions={0} | all-to-all | bytes 589824 | tf_op jit(solution)/shard_map/all_to_all | solution.py:504
  71.5 0.1 reshape.21.rows_ref
  71.6 0.0 collective-permute-done.other_ref
  71.6 0.7 shard_map.253
  72.3 23.2 %all_to_all.35 = bf16[256,2,256]{2,1,0:T(2,128)(2,1)S(1)} all-to-all(bf16[256,2,256]{2,1,0:T(2,128)(2,1)S(1)} %bitcast.17), channel_id=1, replica_groups=mesh['ep_0'=8,'ep_1'=8,'ep_2'=2,'tp'=4] {'ep_1','ep_0','tp'}, dimensions={0} | all-to-all | bytes 524288 | tf_op jit(solution)/shard_map/all_to_all | solution.py:515
  95.5 0.8 shard_map.254
  (9 shorter events, 0.0 us)
Async XLA Ops:
  11.3 16.6 %copy-start = (bf16[128,1024]{1,0:T(8,128)(2,1)S(1)}, bf16[128,1024]{1,0:T(8,128)(2,1)}, u32[]{:S(2)}) copy-start(bf16[128,1024]{1,0:T(8,128)(2,1)} %out_w_ref.1) | copy-start | bytes 786436
  11.3 16.6 %copy-start.4 = (bf16[512,128]{1,0:T(8,128)(2,1)S(1)}, bf16[512,128]{1,0:T(8,128)(2,1)}, u32[]{:S(2)}) copy-start(bf16[512,128]{1,0:T(8,128)(2,1)} %value_ref.1) | copy-start | bytes 393220
  13.0 15.4 %copy-start.1 = (bf16[1,1024,128]{2,1,0:T(8,128)(2,1)S(1)}, bf16[1,1024,128]{2,1,0:T(8,128)(2,1)}, u32[]{:S(2)}) copy-start(bf16[1,1024,128]{2,1,0:T(8,128)(2,1)} %param.42) | copy-start | bytes 786436
  13.0 15.4 %copy-start.2 = (bf16[1,1024,128]{2,1,0:T(8,128)(2,1)S(1)}, bf16[1,1024,128]{2,1,0:T(8,128)(2,1)}, u32[]{:S(2)}) copy-start(bf16[1,1024,128]{2,1,0:T(8,128)(2,1)} %param.43) | copy-start | bytes 786436
  13.0 15.4 %copy-start.3 = (bf16[1,128,1024]{2,1,0:T(8,128)(2,1)S(1)}, bf16[1,128,1024]{2,1,0:T(8,128)(2,1)}, u32[]{:S(2)}) copy-start(bf16[1,128,1024]{2,1,0:T(8,128)(2,1)} %param.44) | copy-start | bytes 786436
  19.9 26.0 %copy-start.5 = (bf16[16,1024]{1,0:T(8,128)(2,1)S(1)}, bf16[16,1024]{1,0:T(8,128)(2,1)}, u32[]{:S(2)}) copy-start(bf16[16,1024]{1,0:T(8,128)(2,1)} %tok_ref.1) | copy-start | bytes 98308
  19.9 26.0 %copy-start.6 = (f32[1024]{0:T(1024)S(1)}, f32[1024]{0:T(1024)}, u32[]{:S(2)}) copy-start(f32[1024]{0:T(1024)} %param.39) | copy-start | bytes 12292
  28.5 43.1 %collective-permute-start = (bf16[3072,128]{1,0:T(8,128)(2,1)S(1)}, bf16[3072,128]{1,0:T(8,128)(2,1)S(1)}, u32[]{:S(2)}, u32[]{:S(2)}) collective-permute-start(bf16[3072,128]{1,0:T(8,128)(2,1)S(1)} %shard_map.252.own_ref), channel_id=1, source_target_pairs={{0,4},{4,0},{1,5},{5,1},{2,6},{6,2},{3,7},{7,3},{8,12},{12,8},{9,1... | collective-permute-start | bytes 2359304 | tf_op jit(solution)/shard_map/ppermute | solution.py:487

commit v7 on v6

--- a/solution.py
+++ b/solution.py
@@ -152,8 +152,12 @@
     index_ref, cache_hbm, arr_ref, q_gain_ref, kv_gain_ref, q_up_ref, head_gain_ref, key_up_ref,
     cos_ref, sin_ref, send_ref, latent_ref, mine_ref, cache_ref, sem,
 ):
-    copy = pltpu.make_async_copy(cache_hbm, cache_ref, sem.at[0])
-    copy.start()
+    copies = [
+        pltpu.make_async_copy(cache_hbm.at[s], cache_ref.at[s], sem.at[s])
+        for s in range(cache_ref.shape[0])
+    ]
+    for copy in copies:
+        copy.start()
     peers, both, cols = arr_ref.shape
     rows = both // 2
     rank = key_up_ref.shape[0]
@@ -185,7 +189,8 @@
             at = slice(h * each, (h + 1) * each)
             send_ref[i, at, :rank] = absorbed[i * each : (i + 1) * each].astype(BF16)
             send_ref[i, at, rank:] = turned[i * each : (i + 1) * each].astype(BF16)
-    copy.wait()
+    for copy in copies:
+        copy.wait()
 
 
 def attend_body(
@@ -270,8 +275,15 @@
     resid_ref[...] = resid
     width = resid.shape[1]
     moe_input = rms_scaled(resid, gain_ref[...]).astype(BF16)
-    out_ref[:, :width] = dot(placing_ref[...], moe_input).astype(BF16)
-    out_ref[:, width:] = weights_ref[...]
+    parts, copies, planes, cap, _ = out_ref.shape
+    rows = dot(placing_ref[...], moe_input).astype(BF16)
+    for p in range(parts):
+        at = slice(p * planes * cap, (p + 1) * planes * cap)
+        main = rows[at].reshape(planes, cap, width)
+        side = weights_ref[at, :].reshape(planes, cap, EXTRA)
+        for i in range(copies):
+            out_ref[p, i, :, :, :width] = main
+            out_ref[p, i, :, :, width:] = side
 
 
 def heads_body(arr_ref, value_ref, out_w_ref, out_ref):
@@ -296,8 +308,8 @@
     chips, quarters, cap, quarter = out_ref.shape
     width = quarters * quarter
     units = own_ref.shape[1]
-    inside = rows_ref[:, :width]
-    extra = rows_ref[:, width:].astype(F32)
+    inside = rows_ref[:, :, :width].reshape(chips * cap, width)
+    extra = rows_ref[:, :, width:].reshape(chips * cap, EXTRA).astype(F32)
     lane = lax.broadcasted_iota(jnp.int32, extra.shape, 1)
     here = index_ref[0]
     there = here + 1 - 2 * (here % 2)
@@ -441,7 +453,7 @@
         sines,
         scalars=1,
         hbm_in=1,
-        sems=1,
+        sems=seqs_mine,
     )
     queries = lax.all_to_all(send, "tp", 0, 0, tiled=True)
     units = expert_gate.shape[2]
@@ -489,7 +501,9 @@
         moe_body,
         (
             jax.ShapeDtypeStruct((seq_count, width), BF16),
-            jax.ShapeDtypeStruct((slots, width + EXTRA), BF16),
+            jax.ShapeDtypeStruct(
+                (parts, chips_in_group, planes, GROUP_CAP, width + EXTRA), BF16
+            ),
         ),
         summands,
         tokens,
@@ -497,11 +511,8 @@
         placing,
         packed_weights,
     )
-    packed = jnp.broadcast_to(
-        packed.reshape(parts, 1, planes, GROUP_CAP, width + EXTRA),
-        (parts, chips_in_group, planes, GROUP_CAP, width + EXTRA),
-    ).reshape(chips, GROUP_CAP, width + EXTRA)
-    arrived = lax.all_to_all(packed, CHIPS, 0, 0, tiled=True).reshape(-1, width + EXTRA)
+    packed = packed.reshape(chips, GROUP_CAP, width + EXTRA)
+    arrived = lax.all_to_all(packed, CHIPS, 0, 0, tiled=True)
     (sums,) = run(
         experts_body,
         (jax.ShapeDtypeStruct((chips, tp_count, GROUP_CAP, quarter_cols), BF16),),

time: 98 us -> 97.9 us (level)
  no operation moved by 1% of the time
where the time goes in v7:
time: 97.9 us; the launch traced here: 96.2 us
  blocking collectives  78.3 us (80%)
  starting transfers between devices  9.92 us (10%)
  Pallas kernels  7.21 us (7%)
    all_to_all x1, blocking collectives, shards(): arrived = lax.all_to_all(packed, CHIPS, 0, 0, tiled=True)  25.2 us
    all_to_all x1, blocking collectives, shards(): lax.all_to_all(sums.reshape(chips * tp_count, GROUP_CAP, quarter_cols), (...  23.2 us
    ppermute x1, starting transfers between devices, shards(): other_weights = lax.ppermute(own_weights, CORE, swap)  9.92 us
    all_to_all x1, blocking collectives, shards(): latents = lax.all_to_all(both, 'tp', 0, 0, tiled=True)  8.93 us
    all_to_all x1, blocking collectives, shards(): summands = lax.all_to_all(partials, 'tp', 0, 0, tiled=True)  7.44 us
    all_to_all x1, blocking collectives, shards(): queries = lax.all_to_all(send, 'tp', 0, 0, tiled=True)  6.83 us
    all_to_all x1, blocking collectives, shards(): attended_heads = lax.all_to_all(attended, 'tp', 0, 0, tiled=True)  6.65 us
    pallas_call x7, Pallas kernels, run(): pl.pallas_call(body, compiler_params=pltpu.CompilerParams(vmem_limit_byte...  5.48 us
  transfers between devices with their start and end apart: 1, of which 0 were waited for; matrix products, arithmetic and copies ran while one was open for 0% of the time, Pallas kernels for 0%

profile of v7, /device:TPU:1, one launch (start us, length us, event | category | flops | bytes accessed | tf_op | source)
XLA Modules:
  0.0 96.2 jit_solution(8759269758416139492)
XLA Ops:
  0.7 1.7 %shard_map.247 = (bf16[4,32,128]{2,1,0:T(8,128)(2,1)S(1)}, bf16[16,32]{1,0:T(8,128)(2,1)S(1)}, f32[16,16]{1,0:T(8,128)S(1)}, f32[16,16]{1,0:T(8,128)S(1)}, bf16[...) custom-call(bf16[16,1024]{1,0:T(8,128)(2,1)} %tok_ref.1, ...), custom_call_target="tpu_custom_call" | custom-call | flops 2000000 | bytes 1156800 | tf_op jit(solution)/shard_map/pallas_call | solution.py:139
  2.4 8.9 %all_to_all.30.arr_ref = bf16[4,32,128]{2,1,0:T(8,128)(2,1)S(1)} all-to-all(bf16[4,32,128]{2,1,0:T(8,128)(2,1)S(1)} %get-tuple-element.38), channel_id=1, replica_groups=mesh['ep_0'=8,'ep_1'=8,'ep_2'=2,'tp'=4] {'tp'}, dimensions={0} | all-to-all | bytes 65536 | tf_op jit(solution)/shard_map/all_to_all | solution.py:435
  11.3 1.8 %shard_map.248 = (bf16[4,8,544]{2,1,0:T(8,128)(2,1)S(1)}, bf16[16,512]{1,0:T(8,128)(2,1)S(1)}, bf16[16,128]{1,0:T(8,128)(2,1)S(1)}, bf16[4,512,512]{2,1,0:T(8,128)(2,1)S(1)}) custom-call(s32[1]{0:T(128)} %bitcast.8.index_ref, bf16[4,512,512]{2,1,0:T(8,128)(2,1)} %cache_hbm.1, bf16[4,32,128]{2,1,0:T(8,128)(2,1)S(1)} %all_to_all.30.arr_ref, ...), custom_call_target="tpu_custom_call" | custom-call | flops 2000000 | bytes 2464516 | tf_op jit(solution)/shard_map/pallas_call | solution.py:60
  13.1 0.0 copy-start.1
  13.2 0.0 copy-start.2
  13.2 0.0 copy-start.3
  13.2 6.8 %all_to_all.31.arr_ref = bf16[4,8,544]{2,1,0:T(8,128)(2,1)S(1)} all-to-all(bf16[4,8,544]{2,1,0:T(8,128)(2,1)S(1)} %get-tuple-element.46), channel_id=1, replica_groups=mesh['ep_0'=8,'ep_1'=8,'ep_2'=2,'tp'=4] {'tp'}, dimensions={0} | all-to-all | bytes 69632 | tf_op jit(solution)/shard_map/all_to_all | solution.py:458
  20.0 1.4 %shard_map.249 = (bf16[4,8,512]{2,1,0:T(8,128)(2,1)S(1)}, bf16[16,128]{1,0:T(8,128)(2,1)}, bf16[16,32]{1,0:T(8,128)(2,1)}) custom-call(s32[1]{0:T(128)} %bitcast.8.index_ref, bf16[4,8,544]{2,1,0:T(8,128)(2,1)S(1)} %all_to_all.31.arr_ref, bf16[4,512,512]{2,1,0:T(8,128)(2,1)S(1)} %get-tuple-element.47.cache_ref, ...), custom_call_target="tpu_custom_call" | custom-call | flops 2000000 | bytes 2352196 | tf_op jit(solution)/shard_map/pallas_call | solution.py:60
  21.5 6.7 %all_to_all.32.arr_ref = bf16[4,8,512]{2,1,0:T(8,128)(2,1)S(1)} all-to-all(bf16[4,8,512]{2,1,0:T(8,128)(2,1)S(1)} %get-tuple-element.55), channel_id=1, replica_groups=mesh['ep_0'=8,'ep_1'=8,'ep_2'=2,'tp'=4] {'tp'}, dimensions={0} | all-to-all | bytes 65536 | tf_op jit(solution)/shard_map/all_to_all | solution.py:483
  28.1 0.0 copy-done
  28.1 0.0 copy-done.4
  28.1 0.4 shard_map.250
  28.5 0.0 copy-done.1
  28.5 0.0 copy-done.2
  28.6 0.1 shard_map.252.own_ref
  28.6 9.9 %collective-permute-start = (bf16[3072,128]{1,0:T(8,128)(2,1)S(1)}, bf16[3072,128]{1,0:T(8,128)(2,1)S(1)}, u32[]{:S(2)}, u32[]{:S(2)}) collective-permute-start(bf16[3072,128]{1,0:T(8,128)(2,1)S(1)} %shard_map.252.own_ref), channel_id=1, source_target_pairs={{0,4},{4,0},{1,5},{5,1},{2,6},{6,2},{3,7},{7,3},{8,12},{12,8},{9,1... | collective-permute-start | bytes 2359304 | tf_op jit(solution)/shard_map/ppermute | solution.py:499
  38.6 7.4 %all_to_all.33.arr_ref = bf16[4,16,1024]{2,1,0:T(8,128)(2,1)S(1)} all-to-all(bf16[4,16,1024]{2,1,0:T(8,128)(2,1)S(1)} %shard_map.250), channel_id=1, replica_groups=mesh['ep_0'=8,'ep_1'=8,'ep_2'=2,'tp'=4] {'tp'}, dimensions={0} | all-to-all | bytes 262144 | tf_op jit(solution)/shard_map/all_to_all | solution.py:494
  46.0 0.0 copy-done.5
  46.0 0.3 shard_map.251
  46.3 25.2 %all_to_all.34.rows_ref = bf16[64,2,1152]{2,1,0:T(2,128)(2,1)S(1)} all-to-all(bf16[64,2,1152]{2,1,0:T(2,128)(2,1)S(1)} %bitcast.19), channel_id=1, replica_groups=mesh['ep_0'=8,'ep_1'=8,'ep_2'=2,'tp'=4] {'ep_1','ep_0'}, dimensions={0} | all-to-all | bytes 589824 | tf_op jit(solution)/shard_map/all_to_all | solution.py:515
  71.5 0.0 collective-permute-done.other_ref
  71.5 0.7 shard_map.253
  72.2 23.2 %all_to_all.35 = bf16[256,2,256]{2,1,0:T(2,128)(2,1)S(1)} all-to-all(bf16[256,2,256]{2,1,0:T(2,128)(2,1)S(1)} %bitcast.17), channel_id=1, replica_groups=mesh['ep_0'=8,'ep_1'=8,'ep_2'=2,'tp'=4] {'ep_1','ep_0','tp'}, dimensions={0} | all-to-all | bytes 524288 | tf_op jit(solution)/shard_map/all_to_all | solution.py:526
  95.4 0.8 shard_map.254
  (6 shorter events, 0.0 us)
Async XLA Ops:
  11.3 16.8 %copy-start = (bf16[128,1024]{1,0:T(8,128)(2,1)S(1)}, bf16[128,1024]{1,0:T(8,128)(2,1)}, u32[]{:S(2)}) copy-start(bf16[128,1024]{1,0:T(8,128)(2,1)} %out_w_ref.1) | copy-start | bytes 786436
  11.3 16.8 %copy-start.4 = (bf16[512,128]{1,0:T(8,128)(2,1)S(1)}, bf16[512,128]{1,0:T(8,128)(2,1)}, u32[]{:S(2)}) copy-start(bf16[512,128]{1,0:T(8,128)(2,1)} %value_ref.1) | copy-start | bytes 393220
  13.1 15.4 %copy-start.1 = (bf16[1,1024,128]{2,1,0:T(8,128)(2,1)S(1)}, bf16[1,1024,128]{2,1,0:T(8,128)(2,1)}, u32[]{:S(2)}) copy-start(bf16[1,1024,128]{2,1,0:T(8,128)(2,1)} %param.42) | copy-start | bytes 786436
  13.2 15.4 %copy-start.2 = (bf16[1,1024,128]{2,1,0:T(8,128)(2,1)S(1)}, bf16[1,1024,128]{2,1,0:T(8,128)(2,1)}, u32[]{:S(2)}) copy-start(bf16[1,1024,128]{2,1,0:T(8,128)(2,1)} %param.43) | copy-start | bytes 786436
  13.2 15.4 %copy-start.3 = (bf16[1,128,1024]{2,1,0:T(8,128)(2,1)S(1)}, bf16[1,128,1024]{2,1,0:T(8,128)(2,1)}, u32[]{:S(2)}) copy-start(bf16[1,128,1024]{2,1,0:T(8,128)(2,1)} %param.44) | copy-start | bytes 786436
  20.0 26.0 %copy-start.5 = (bf16[16,1024]{1,0:T(8,128)(2,1)S(1)}, bf16[16,1024]{1,0:T(8,128)(2,1)}, u32[]{:S(2)}) copy-start(bf16[16,1024]{1,0:T(8,128)(2,1)} %tok_ref.1) | copy-start | bytes 98308
  20.0 26.0 %copy-start.6 = (f32[1024]{0:T(1024)S(1)}, f32[1024]{0:T(1024)}, u32[]{:S(2)}) copy-start(f32[1024]{0:T(1024)} %param.39) | copy-start | bytes 12292
  28.6 42.8 %collective-permute-start = (bf16[3072,128]{1,0:T(8,128)(2,1)S(1)}, bf16[3072,128]{1,0:T(8,128)(2,1)S(1)}, u32[]{:S(2)}, u32[]{:S(2)}) collective-permute-start(bf16[3072,128]{1,0:T(8,128)(2,1)S(1)} %shard_map.252.own_ref), channel_id=1, source_target_pairs={{0,4},{4,0},{1,5},{5,1},{2,6},{6,2},{3,7},{7,3},{8,12},{12,8},{9,1... | collective-permute-start | bytes 2359304 | tf_op jit(solution)/shard_map/ppermute | solution.py:499

commit v8 on v7

--- a/solution.py
+++ b/solution.py
@@ -152,12 +152,8 @@
     index_ref, cache_hbm, arr_ref, q_gain_ref, kv_gain_ref, q_up_ref, head_gain_ref, key_up_ref,
     cos_ref, sin_ref, send_ref, latent_ref, mine_ref, cache_ref, sem,
 ):
-    copies = [
-        pltpu.make_async_copy(cache_hbm.at[s], cache_ref.at[s], sem.at[s])
-        for s in range(cache_ref.shape[0])
-    ]
-    for copy in copies:
-        copy.start()
+    copy = pltpu.make_async_copy(cache_hbm, cache_ref, sem.at[0])
+    copy.start()
     peers, both, cols = arr_ref.shape
     rows = both // 2
     rank = key_up_ref.shape[0]
@@ -189,8 +185,7 @@
             at = slice(h * each, (h + 1) * each)
             send_ref[i, at, :rank] = absorbed[i * each : (i + 1) * each].astype(BF16)
             send_ref[i, at, rank:] = turned[i * each : (i + 1) * each].astype(BF16)
-    for copy in copies:
-        copy.wait()
+    copy.wait()
 
 
 def attend_body(
@@ -258,13 +253,25 @@
         copy.wait()
 
 
-def weights_body(gate_ref, up_ref, down_ref, out_ref):
-    width, units = gate_ref.shape
-    out_ref[:width, :] = gate_ref[...]
-    out_ref[width : 2 * width, :] = up_ref[...]
+def weights_body(gate_hbm, up_hbm, down_hbm, out_ref, sems):
+    width, units = gate_hbm.shape
+    copies = [
+        pltpu.make_async_copy(gate_hbm, out_ref.at[:width], sems.at[0]),
+        pltpu.make_async_copy(up_hbm, out_ref.at[width : 2 * width], sems.at[1]),
+    ]
     for j in range(width // units):
         at = 2 * width + j * units
-        out_ref[at : at + units, :] = down_ref[:, j * units : (j + 1) * units]
+        copies.append(
+            pltpu.make_async_copy(
+                down_hbm.at[:, j * units : (j + 1) * units],
+                out_ref.at[at : at + units],
+                sems.at[2 + j],
+            )
+        )
+    for copy in copies:
+        copy.start()
+    for copy in copies:
+        copy.wait()
 
 
 def moe_body(arr_ref, tok_ref, gain_ref, placing_ref, weights_ref, resid_ref, out_ref):
@@ -453,7 +460,7 @@
         sines,
         scalars=1,
         hbm_in=1,
-        sems=seqs_mine,
+        sems=1,
     )
     queries = lax.all_to_all(send, "tp", 0, 0, tiled=True)
     units = expert_gate.shape[2]
@@ -480,6 +487,20 @@
         hbm_out=2,
         sems=2,
     )
+    attended, gate, up, lower = lax.optimization_barrier(
+        (attended, expert_gate[0], expert_up[0], expert_down[0])
+    )
+    (own_weights,) = run(
+        weights_body,
+        (jax.ShapeDtypeStruct((3 * width, units), BF16),),
+        gate,
+        up,
+        lower,
+        hbm_in=3,
+        sems=2 + width // units,
+    )
+    swap = [(i, cores - 1 - i) for i in range(cores)]
+    other_weights = lax.ppermute(own_weights, CORE, swap)
     attended_heads = lax.all_to_all(attended, "tp", 0, 0, tiled=True)
     (partials,) = run(
         heads_body,
@@ -488,15 +509,7 @@
         value_up,
         attn_out,
     )
-    partials, gate, up, lower = lax.optimization_barrier(
-        (partials, expert_gate[0], expert_up[0], expert_down[0])
-    )
     summands = lax.all_to_all(partials, "tp", 0, 0, tiled=True)
-    (own_weights,) = run(
-        weights_body, (jax.ShapeDtypeStruct((3 * width, units), BF16),), gate, up, lower
-    )
-    swap = [(i, cores - 1 - i) for i in range(cores)]
-    other_weights = lax.ppermute(own_weights, CORE, swap)
     attn_resid, packed = run(
         moe_body,
         (
@@ -566,6 +579,7 @@
         P(EP, None, "tp"),
         P(EP, "tp", None),
     )
+
     return jax.shard_map(
         shards,
         mesh=torus,

time: 97.9 us -> 97 us (level)
  the two profiles are of different devices: /device:TPU:1 before, /device:TPU:8 now
where the time goes in v8:
time: 97 us; the launch traced here: 96.6 us
  blocking collectives  85.9 us (89%)
  Pallas kernels  8.04 us (8%)
  starting transfers between devices  1.92 us (2%)
    all_to_all x1, blocking collectives, shards(): arrived = lax.all_to_all(packed, CHIPS, 0, 0, tiled=True)  29.1 us
    all_to_all x1, blocking collectives, shards(): lax.all_to_all(sums.reshape(chips * tp_count, GROUP_CAP, quarter_cols), (...  23 us
    all_to_all x1, blocking collectives, shards(): latents = lax.all_to_all(both, 'tp', 0, 0, tiled=True)  9.54 us
    all_to_all x1, blocking collectives, shards(): summands = lax.all_to_all(partials, 'tp', 0, 0, tiled=True)  8.36 us
    all_to_all x1, blocking collectives, shards(): queries = lax.all_to_all(send, 'tp', 0, 0, tiled=True)  7.98 us
    all_to_all x1, blocking collectives, shards(): attended_heads = lax.all_to_all(attended, 'tp', 0, 0, tiled=True)  7.8 us
    pallas_call x7, Pallas kernels, run(): pl.pallas_call(body, compiler_params=pltpu.CompilerParams(vmem_limit_byte...  6.31 us
  transfers between devices with their start and end apart: 1, of which 0 were waited for; matrix products, arithmetic and copies ran while one was open for 0% of the time, Pallas kernels for 1%

profile of v8, /device:TPU:8, one launch (start us, length us, event | category | flops | bytes accessed | tf_op | source)
XLA Modules:
  0.0 96.6 jit_solution(11008864804606147122)
XLA Ops:
  0.7 1.7 %shard_map.247 = (bf16[4,32,128]{2,1,0:T(8,128)(2,1)S(1)}, bf16[16,32]{1,0:T(8,128)(2,1)S(1)}, f32[16,16]{1,0:T(8,128)S(1)}, f32[16,16]{1,0:T(8,128)S(1)}, bf16[...) custom-call(bf16[16,1024]{1,0:T(8,128)(2,1)} %tok_ref.1, ...), custom_call_target="tpu_custom_call" | custom-call | flops 2000000 | bytes 1156800 | tf_op jit(solution)/shard_map/pallas_call | solution.py:139
  2.4 9.5 %all_to_all.30.arr_ref = bf16[4,32,128]{2,1,0:T(8,128)(2,1)S(1)} all-to-all(bf16[4,32,128]{2,1,0:T(8,128)(2,1)S(1)} %get-tuple-element.38), channel_id=1, replica_groups=mesh['ep_0'=8,'ep_1'=8,'ep_2'=2,'tp'=4] {'tp'}, dimensions={0} | all-to-all | bytes 65536 | tf_op jit(solution)/shard_map/all_to_all | solution.py:442
  11.9 1.6 %shard_map.248 = (bf16[4,8,544]{2,1,0:T(8,128)(2,1)S(1)}, bf16[16,512]{1,0:T(8,128)(2,1)S(1)}, bf16[16,128]{1,0:T(8,128)(2,1)S(1)}, bf16[4,512,512]{2,1,0:T(8,128)(2,1)S(1)}) custom-call(s32[1]{0:T(128)} %bitcast.8.index_ref, bf16[4,512,512]{2,1,0:T(8,128)(2,1)} %cache_hbm.1, bf16[4,32,128]{2,1,0:T(8,128)(2,1)S(1)} %all_to_all.30.arr_ref, ...), custom_call_target="tpu_custom_call" | custom-call | flops 2000000 | bytes 2464516 | tf_op jit(solution)/shard_map/pallas_call | solution.py:60
  13.5 0.0 copy-start
  13.6 0.0 copy-start.1
  13.6 8.0 %all_to_all.31.arr_ref = bf16[4,8,544]{2,1,0:T(8,128)(2,1)S(1)} all-to-all(bf16[4,8,544]{2,1,0:T(8,128)(2,1)S(1)} %get-tuple-element.46), channel_id=1, replica_groups=mesh['ep_0'=8,'ep_1'=8,'ep_2'=2,'tp'=4] {'tp'}, dimensions={0} | all-to-all | bytes 69632 | tf_op jit(solution)/shard_map/all_to_all | solution.py:465
  21.6 0.0 copy-start.2
  21.6 0.0 copy-start.3
  21.6 1.4 %shard_map.249 = (bf16[4,8,512]{2,1,0:T(8,128)(2,1)S(1)}, bf16[16,128]{1,0:T(8,128)(2,1)}, bf16[16,32]{1,0:T(8,128)(2,1)}) custom-call(s32[1]{0:T(128)} %bitcast.8.index_ref, bf16[4,8,544]{2,1,0:T(8,128)(2,1)S(1)} %all_to_all.31.arr_ref, bf16[4,512,512]{2,1,0:T(8,128)(2,1)S(1)} %get-tuple-element.47.cache_ref, ...), custom_call_target="tpu_custom_call" | custom-call | flops 2000000 | bytes 2352196 | tf_op jit(solution)/shard_map/pallas_call | solution.py:60
  23.0 1.1 %shard_map.252.own_ref = bf16[3072,128]{1,0:T(8,128)(2,1)S(1)} custom-call(bf16[1024,128]{1,0:T(8,128)(2,1)} %bitcast.21, bf16[1024,128]{1,0:T(8,128)(2,1)} %bitcast.22, bf16[128,1024]{1,0:T(8,128)(2,1)} %bitcast.23), custom_call_target="tpu_custom_call" | custom-call | flops 2000000 | bytes 786432 | tf_op jit(solution)/shard_map/pallas_call | solution.py:60
  24.2 1.9 %collective-permute-start = (bf16[3072,128]{1,0:T(8,128)(2,1)S(1)}, bf16[3072,128]{1,0:T(8,128)(2,1)S(1)}, u32[]{:S(2)}, u32[]{:S(2)}) collective-permute-start(bf16[3072,128]{1,0:T(8,128)(2,1)S(1)} %shard_map.252.own_ref), channel_id=1, source_target_pairs={{0,4},{4,0},{1,5},{5,1},{2,6},{6,2},{3,7},{7,3},{8,12},{12,8},{9,1... | collective-permute-start | bytes 2359304 | tf_op jit(solution)/shard_map/ppermute | solution.py:503
  26.1 7.8 %all_to_all.32.arr_ref = bf16[4,8,512]{2,1,0:T(8,128)(2,1)S(1)} all-to-all(bf16[4,8,512]{2,1,0:T(8,128)(2,1)S(1)} %get-tuple-element.56), channel_id=1, replica_groups=mesh['ep_0'=8,'ep_1'=8,'ep_2'=2,'tp'=4] {'tp'}, dimensions={0} | all-to-all | bytes 65536 | tf_op jit(solution)/shard_map/all_to_all | solution.py:504
  33.9 0.0 copy-done
  33.9 0.0 copy-done.1
  33.9 0.4 shard_map.250
  34.3 8.4 %all_to_all.33.arr_ref = bf16[4,16,1024]{2,1,0:T(8,128)(2,1)S(1)} all-to-all(bf16[4,16,1024]{2,1,0:T(8,128)(2,1)S(1)} %shard_map.250), channel_id=1, replica_groups=mesh['ep_0'=8,'ep_1'=8,'ep_2'=2,'tp'=4] {'tp'}, dimensions={0} | all-to-all | bytes 262144 | tf_op jit(solution)/shard_map/all_to_all | solution.py:512
  42.6 0.0 copy-done.2
  42.6 0.0 copy-done.3
  42.6 0.3 shard_map.251
  42.9 29.1 %all_to_all.34.rows_ref = bf16[64,2,1152]{2,1,0:T(2,128)(2,1)S(1)} all-to-all(bf16[64,2,1152]{2,1,0:T(2,128)(2,1)S(1)} %bitcast.19), channel_id=1, replica_groups=mesh['ep_0'=8,'ep_1'=8,'ep_2'=2,'tp'=4] {'ep_1','ep_0'}, dimensions={0} | all-to-all | bytes 589824 | tf_op jit(solution)/shard_map/all_to_all | solution.py:528
  72.1 0.0 collective-permute-done.other_ref
  72.1 0.7 shard_map.253
  72.8 23.0 %all_to_all.35 = bf16[256,2,256]{2,1,0:T(2,128)(2,1)S(1)} all-to-all(bf16[256,2,256]{2,1,0:T(2,128)(2,1)S(1)} %bitcast.17), channel_id=1, replica_groups=mesh['ep_0'=8,'ep_1'=8,'ep_2'=2,'tp'=4] {'ep_1','ep_0','tp'}, dimensions={0} | all-to-all | bytes 524288 | tf_op jit(solution)/shard_map/all_to_all | solution.py:539
  95.8 0.8 shard_map.254
Async XLA Ops:
  13.5 20.3 %copy-start = (bf16[128,1024]{1,0:T(8,128)(2,1)S(1)}, bf16[128,1024]{1,0:T(8,128)(2,1)}, u32[]{:S(2)}) copy-start(bf16[128,1024]{1,0:T(8,128)(2,1)} %out_w_ref.1) | copy-start | bytes 786436
  13.6 20.3 %copy-start.1 = (bf16[512,128]{1,0:T(8,128)(2,1)S(1)}, bf16[512,128]{1,0:T(8,128)(2,1)}, u32[]{:S(2)}) copy-start(bf16[512,128]{1,0:T(8,128)(2,1)} %value_ref.1) | copy-start | bytes 393220
  21.6 21.1 %copy-start.2 = (bf16[16,1024]{1,0:T(8,128)(2,1)S(1)}, bf16[16,1024]{1,0:T(8,128)(2,1)}, u32[]{:S(2)}) copy-start(bf16[16,1024]{1,0:T(8,128)(2,1)} %tok_ref.1) | copy-start | bytes 98308
  21.6 21.1 %copy-start.3 = (f32[1024]{0:T(1024)S(1)}, f32[1024]{0:T(1024)}, u32[]{:S(2)}) copy-start(f32[1024]{0:T(1024)} %param.39) | copy-start | bytes 12292
  24.2 47.9 %collective-permute-start = (bf16[3072,128]{1,0:T(8,128)(2,1)S(1)}, bf16[3072,128]{1,0:T(8,128)(2,1)S(1)}, u32[]{:S(2)}, u32[]{:S(2)}) collective-permute-start(bf16[3072,128]{1,0:T(8,128)(2,1)S(1)} %shard_map.252.own_ref), channel_id=1, source_target_pairs={{0,4},{4,0},{1,5},{5,1},{2,6},{6,2},{3,7},{7,3},{8,12},{12,8},{9,1... | collective-permute-start | bytes 2359304 | tf_op jit(solution)/shard_map/ppermute | solution.py:503

commit v9 on v8

--- a/solution.py
+++ b/solution.py
@@ -92,6 +92,7 @@
 
 
 OWN = 9
+EARLY = 1
 MADE = 7
 
 
@@ -100,7 +101,14 @@
     hbm, made, last = refs[:count], refs[count : count + MADE], refs[count + MADE : -1]
     sems = refs[-1]
     near_refs = last[count - OWN :] + last[: count - OWN]
-    copies = [pltpu.make_async_copy(hbm[i], near_refs[i], sems.at[i]) for i in range(count)]
+    copies = [
+        pltpu.make_async_copy(
+            hbm[i] if i < count - 1 else hbm[i].at[: near_refs[i].shape[0]],
+            near_refs[i],
+            sems.at[i],
+        )
+        for i in range(count)
+    ]
     for copy in copies:
         copy.start()
     tok_ref, gain_ref, q_ref, kv_ref, rope_ref, len_ref, turn_ref, route_ref, weight_ref = near_refs[
@@ -132,10 +140,10 @@
         copy.wait()
 
 
-def down(made, own, others, parts):
+def down(made, own, others, early, parts):
     args = (*own, *others)
     moved = sum(a.size * a.dtype.itemsize for a in args)
-    outs = [pltpu.VMEM(o.shape, o.dtype) for o in (*made, *others)]
+    outs = [pltpu.VMEM(o.shape, o.dtype) for o in (*made, *others[:-1], early)]
     return pl.pallas_call(
         lambda *refs: down_body(parts, *refs),
         compiler_params=pltpu.CompilerParams(vmem_limit_bytes=16 * 1024 * 1024),
@@ -152,7 +160,7 @@
     index_ref, cache_hbm, arr_ref, q_gain_ref, kv_gain_ref, q_up_ref, head_gain_ref, key_up_ref,
     cos_ref, sin_ref, send_ref, latent_ref, mine_ref, cache_ref, sem,
 ):
-    copy = pltpu.make_async_copy(cache_hbm, cache_ref, sem.at[0])
+    copy = pltpu.make_async_copy(cache_hbm.at[EARLY:], cache_ref, sem.at[0])
     copy.start()
     peers, both, cols = arr_ref.shape
     rows = both // 2
@@ -189,7 +197,7 @@
 
 
 def attend_body(
-    index_ref, arr_ref, cache_ref, keys_ref, cos_table_ref, sin_table_ref, latent_ref, mine_ref,
+    index_ref, arr_ref, first_ref, cache_ref, keys_ref, cos_table_ref, sin_table_ref, latent_ref, mine_ref,
     rope_ref, cos_ref, sin_ref, len_ref, out_ref, latent_out, rope_out, sems,
 ):
     copies = [
@@ -198,7 +206,9 @@
     ]
     for copy in copies:
         copy.start()
-    seqs, places, rank = cache_ref.shape
+    later, places, rank = cache_ref.shape
+    seqs = later + EARLY
+    caches = [first_ref[s] for s in range(EARLY)] + [cache_ref[s] for s in range(later)]
     peers, each, _ = arr_ref.shape
     rows = peers * each
     half = cos_ref.shape[1]
@@ -237,7 +247,7 @@
             ],
             axis=0,
         ).astype(BF16)
-        part = dot_t(absorbed, cache_ref[s]) + dot(turned, keys)
+        part = dot_t(absorbed, caches[s]) + dot(turned, keys)
         scores = jnp.where(row_seq == s, part, scores)
     valid = lax.broadcasted_iota(jnp.int32, (rows, places), 1) < lengths
     scores = jnp.where(valid, scores * scale, NEG)
@@ -247,7 +257,7 @@
     total = jnp.sum(weights, axis=1, keepdims=True) + self_weight
     summed = self_weight.astype(BF16).astype(F32) * latent
     for s in range(seqs):
-        summed = summed + dot(jnp.where(row_seq == s, weights, 0.0).astype(BF16), cache_ref[s])
+        summed = summed + dot(jnp.where(row_seq == s, weights, 0.0).astype(BF16), caches[s])
     out_ref[...] = (summed / total).astype(BF16).reshape(out_ref.shape)
     for copy in copies:
         copy.wait()
@@ -401,7 +411,7 @@
     sin_table = jnp.asarray(np.sin(angles.astype(np.float64)).astype(np.float32))
     (
         both, new_rope, cosines, sines, placing, placing_t, packed_weights,
-        q_up_t, key_near, q_gain, kv_gain, head_gain, cos_table, sin_table, keys, lens,
+        q_up_t, key_near, q_gain, kv_gain, head_gain, cos_table, sin_table, keys, lens, cache_first,
     ) = down(
         (
             jax.ShapeDtypeStruct((tp_count, 2 * seq_count, kv_cols), BF16),
@@ -433,7 +443,9 @@
             sin_table,
             cache_rope,
             lengths[None],
+            cache_latent,
         ),
+        jax.ShapeDtypeStruct((EARLY, *cache_latent.shape[1:]), BF16),
         parts,
     )
     expert_here = (lax.axis_index(EP) % EPG).astype(jnp.int32)[None]
@@ -446,7 +458,7 @@
             jax.ShapeDtypeStruct((tp_count, each, rank + 2 * half_dim), BF16),
             jax.ShapeDtypeStruct((seq_count, rank), BF16),
             jax.ShapeDtypeStruct((seq_count, kv_cols), BF16),
-            jax.ShapeDtypeStruct(cache_latent.shape, BF16),
+            jax.ShapeDtypeStruct((seqs_mine - EARLY, *cache_latent.shape[1:]), BF16),
         ),
         index,
         cache_latent,
@@ -473,6 +485,7 @@
         ),
         index,
         queries,
+        cache_first,
         cache,
         keys,
         cos_table,
@@ -487,20 +500,6 @@
         hbm_out=2,
         sems=2,
     )
-    attended, gate, up, lower = lax.optimization_barrier(
-        (attended, expert_gate[0], expert_up[0], expert_down[0])
-    )
-    (own_weights,) = run(
-        weights_body,
-        (jax.ShapeDtypeStruct((3 * width, units), BF16),),
-        gate,
-        up,
-        lower,
-        hbm_in=3,
-        sems=2 + width // units,
-    )
-    swap = [(i, cores - 1 - i) for i in range(cores)]
-    other_weights = lax.ppermute(own_weights, CORE, swap)
     attended_heads = lax.all_to_all(attended, "tp", 0, 0, tiled=True)
     (partials,) = run(
         heads_body,
@@ -525,6 +524,20 @@
         packed_weights,
     )
     packed = packed.reshape(chips, GROUP_CAP, width + EXTRA)
+    packed, gate, up, lower = lax.optimization_barrier(
+        (packed, expert_gate[0], expert_up[0], expert_down[0])
+    )
+    (own_weights,) = run(
+        weights_body,
+        (jax.ShapeDtypeStruct((3 * width, units), BF16),),
+        gate,
+        up,
+        lower,
+        hbm_in=3,
+        sems=2 + width // units,
+    )
+    swap = [(i, cores - 1 - i) for i in range(cores)]
+    other_weights = lax.ppermute(own_weights, CORE, swap)
     arrived = lax.all_to_all(packed, CHIPS, 0, 0, tiled=True)
     (sums,) = run(
         experts_body,

time: 97 us -> 99.9 us (1.030)
  the two profiles are of different devices: /device:TPU:8 before, /device:TPU:1 now
where the time goes in v9:
time: 99.9 us; the launch traced here: 98.4 us
  blocking collectives  78.4 us (78%)
  starting transfers between devices  11.1 us (11%)
  Pallas kernels  8.14 us (8%)
    all_to_all x1, blocking collectives, shards(): arrived = lax.all_to_all(packed, CHIPS, 0, 0, tiled=True)  26.3 us
    all_to_all x1, blocking collectives, shards(): lax.all_to_all(sums.reshape(chips * tp_count, GROUP_CAP, quarter_cols), (...  22.5 us
    ppermute x1, starting transfers between devices, shards(): other_weights = lax.ppermute(own_weights, CORE, swap)  11.1 us
    all_to_all x1, blocking collectives, shards(): latents = lax.all_to_all(both, 'tp', 0, 0, tiled=True)  8.93 us
    all_to_all x1, blocking collectives, shards(): summands = lax.all_to_all(partials, 'tp', 0, 0, tiled=True)  7.39 us
    all_to_all x1, blocking collectives, shards(): queries = lax.all_to_all(send, 'tp', 0, 0, tiled=True)  6.7 us
    all_to_all x1, blocking collectives, shards(): attended_heads = lax.all_to_all(attended, 'tp', 0, 0, tiled=True)  6.65 us
    pallas_call x7, Pallas kernels, run(): pl.pallas_call(body, compiler_params=pltpu.CompilerParams(vmem_limit_byte...  6.4 us
  transfers between devices with their start and end apart: 1, of which 0 were waited for; matrix products, arithmetic and copies ran while one was open for 0% of the time, Pallas kernels for 0%

profile of v9, /device:TPU:1, one launch (start us, length us, event | category | flops | bytes accessed | tf_op | source)
XLA Modules:
  0.0 98.4 jit_solution(13566852294537400953)
XLA Ops:
  0.7 1.7 %shard_map.247 = (bf16[4,32,128]{2,1,0:T(8,128)(2,1)S(1)}, bf16[16,32]{1,0:T(8,128)(2,1)S(1)}, f32[16,16]{1,0:T(8,128)S(1)}, f32[16,16]{1,0:T(8,128)S(1)}, bf16[...) custom-call(bf16[16,1024]{1,0:T(8,128)(2,1)} %tok_ref.1, ...), custom_call_target="tpu_custom_call" | custom-call | flops 2000000 | bytes 3253952 | tf_op jit(solution)/shard_map/pallas_call | solution.py:147
  2.4 8.9 %all_to_all.30.arr_ref = bf16[4,32,128]{2,1,0:T(8,128)(2,1)S(1)} all-to-all(bf16[4,32,128]{2,1,0:T(8,128)(2,1)S(1)} %get-tuple-element.39), channel_id=1, replica_groups=mesh['ep_0'=8,'ep_1'=8,'ep_2'=2,'tp'=4] {'tp'}, dimensions={0} | all-to-all | bytes 65536 | tf_op jit(solution)/shard_map/all_to_all | solution.py:454
  11.3 0.0 copy-start
  11.3 0.0 copy-start.2
  11.3 1.7 %shard_map.248 = (bf16[4,8,544]{2,1,0:T(8,128)(2,1)S(1)}, bf16[16,512]{1,0:T(8,128)(2,1)S(1)}, bf16[16,128]{1,0:T(8,128)(2,1)S(1)}, bf16[3,512,512]{2,1,0:T(8,128)(2,1)S(1)}) custom-call(s32[1]{0:T(128)} %bitcast.8.index_ref, bf16[4,512,512]{2,1,0:T(8,128)(2,1)} %cache_hbm.1, bf16[4,32,128]{2,1,0:T(8,128)(2,1)S(1)} %all_to_all.30.arr_ref, ...), custom_call_target="tpu_custom_call" | custom-call | flops 2000000 | bytes 2464516 | tf_op jit(solution)/shard_map/pallas_call | solution.py:60
  13.0 0.0 copy-start.1
  13.0 0.0 copy-start.3
  13.1 6.7 %all_to_all.31.arr_ref = bf16[4,8,544]{2,1,0:T(8,128)(2,1)S(1)} all-to-all(bf16[4,8,544]{2,1,0:T(8,128)(2,1)S(1)} %get-tuple-element.47), channel_id=1, replica_groups=mesh['ep_0'=8,'ep_1'=8,'ep_2'=2,'tp'=4] {'tp'}, dimensions={0} | all-to-all | bytes 69632 | tf_op jit(solution)/shard_map/all_to_all | solution.py:477
  19.8 1.5 %shard_map.249 = (bf16[4,8,512]{2,1,0:T(8,128)(2,1)S(1)}, bf16[16,128]{1,0:T(8,128)(2,1)}, bf16[16,32]{1,0:T(8,128)(2,1)}) custom-call(s32[1]{0:T(128)} %bitcast.8.index_ref, bf16[4,8,544]{2,1,0:T(8,128)(2,1)S(1)} %all_to_all.31.arr_ref, bf16[1,512,512]{2,1,0:T(8,128)(2,1)S(1)} %get-tuple-element.48.first_ref, ...), custom_call_target="tpu_custom_call" | custom-call | flops 2000000 | bytes 2352196 | tf_op jit(solution)/shard_map/pallas_call | solution.py:60
  21.2 6.7 %all_to_all.32.arr_ref = bf16[4,8,512]{2,1,0:T(8,128)(2,1)S(1)} all-to-all(bf16[4,8,512]{2,1,0:T(8,128)(2,1)S(1)} %get-tuple-element.57), channel_id=1, replica_groups=mesh['ep_0'=8,'ep_1'=8,'ep_2'=2,'tp'=4] {'tp'}, dimensions={0} | all-to-all | bytes 65536 | tf_op jit(solution)/shard_map/all_to_all | solution.py:503
  27.9 0.0 copy-done
  27.9 0.0 copy-done.2
  27.9 0.4 shard_map.250
  28.3 7.4 %all_to_all.33.arr_ref = bf16[4,16,1024]{2,1,0:T(8,128)(2,1)S(1)} all-to-all(bf16[4,16,1024]{2,1,0:T(8,128)(2,1)S(1)} %shard_map.250), channel_id=1, replica_groups=mesh['ep_0'=8,'ep_1'=8,'ep_2'=2,'tp'=4] {'tp'}, dimensions={0} | all-to-all | bytes 262144 | tf_op jit(solution)/shard_map/all_to_all | solution.py:511
  35.7 0.0 copy-done.1
  35.7 0.0 copy-done.3
  35.7 0.3 shard_map.251
  35.9 1.1 %shard_map.252.own_ref = bf16[3072,128]{1,0:T(8,128)(2,1)S(1)} custom-call(bf16[1024,128]{1,0:T(8,128)(2,1)} %bitcast.21, bf16[1024,128]{1,0:T(8,128)(2,1)} %bitcast.22, bf16[128,1024]{1,0:T(8,128)(2,1)} %bitcast.23), custom_call_target="tpu_custom_call" | custom-call | flops 2000000 | bytes 786432 | tf_op jit(solution)/shard_map/pallas_call | solution.py:60
  37.1 11.1 %collective-permute-start = (bf16[3072,128]{1,0:T(8,128)(2,1)S(1)}, bf16[3072,128]{1,0:T(8,128)(2,1)S(1)}, u32[]{:S(2)}, u32[]{:S(2)}) collective-permute-start(bf16[3072,128]{1,0:T(8,128)(2,1)S(1)} %shard_map.252.own_ref), channel_id=1, source_target_pairs={{0,4},{4,0},{1,5},{5,1},{2,6},{6,2},{3,7},{7,3},{8,12},{12,8},{9,1... | collective-permute-start | bytes 2359304 | tf_op jit(solution)/shard_map/ppermute | solution.py:540
  48.1 26.3 %all_to_all.34.rows_ref = bf16[64,2,1152]{2,1,0:T(2,128)(2,1)S(1)} all-to-all(bf16[64,2,1152]{2,1,0:T(2,128)(2,1)S(1)} %bitcast.19), channel_id=1, replica_groups=mesh['ep_0'=8,'ep_1'=8,'ep_2'=2,'tp'=4] {'ep_1','ep_0'}, dimensions={0} | all-to-all | bytes 589824 | tf_op jit(solution)/shard_map/all_to_all | solution.py:541
  74.4 0.0 collective-permute-done.other_ref
  74.4 0.7 shard_map.253
  75.1 22.5 %all_to_all.35 = bf16[256,2,256]{2,1,0:T(2,128)(2,1)S(1)} all-to-all(bf16[256,2,256]{2,1,0:T(2,128)(2,1)S(1)} %bitcast.17), channel_id=1, replica_groups=mesh['ep_0'=8,'ep_1'=8,'ep_2'=2,'tp'=4] {'ep_1','ep_0','tp'}, dimensions={0} | all-to-all | bytes 524288 | tf_op jit(solution)/shard_map/all_to_all | solution.py:552
  97.6 0.8 shard_map.254
Async XLA Ops:
  11.3 16.5 %copy-start = (bf16[128,1024]{1,0:T(8,128)(2,1)S(1)}, bf16[128,1024]{1,0:T(8,128)(2,1)}, u32[]{:S(2)}) copy-start(bf16[128,1024]{1,0:T(8,128)(2,1)} %out_w_ref.1) | copy-start | bytes 786436
  11.3 16.5 %copy-start.2 = (bf16[512,128]{1,0:T(8,128)(2,1)S(1)}, bf16[512,128]{1,0:T(8,128)(2,1)}, u32[]{:S(2)}) copy-start(bf16[512,128]{1,0:T(8,128)(2,1)} %value_ref.1) | copy-start | bytes 393220
  13.0 22.6 %copy-start.1 = (bf16[16,1024]{1,0:T(8,128)(2,1)S(1)}, bf16[16,1024]{1,0:T(8,128)(2,1)}, u32[]{:S(2)}) copy-start(bf16[16,1024]{1,0:T(8,128)(2,1)} %tok_ref.1) | copy-start | bytes 98308
  13.0 22.6 %copy-start.3 = (f32[1024]{0:T(1024)S(1)}, f32[1024]{0:T(1024)}, u32[]{:S(2)}) copy-start(f32[1024]{0:T(1024)} %param.39) | copy-start | bytes 12292
  37.1 37.3 %collective-permute-start = (bf16[3072,128]{1,0:T(8,128)(2,1)S(1)}, bf16[3072,128]{1,0:T(8,128)(2,1)S(1)}, u32[]{:S(2)}, u32[]{:S(2)}) collective-permute-start(bf16[3072,128]{1,0:T(8,128)(2,1)S(1)} %shard_map.252.own_ref), channel_id=1, source_target_pairs={{0,4},{4,0},{1,5},{5,1},{2,6},{6,2},{3,7},{7,3},{8,12},{12,8},{9,1... | collective-permute-start | bytes 2359304 | tf_op jit(solution)/shard_map/ppermute | solution.py:540

commit v10 on v8

--- a/solution.py
+++ b/solution.py
@@ -101,8 +101,8 @@
     sems = refs[-1]
     near_refs = last[count - OWN :] + last[: count - OWN]
     copies = [pltpu.make_async_copy(hbm[i], near_refs[i], sems.at[i]) for i in range(count)]
-    for copy in copies:
-        copy.start()
+    for i in (2, 3, 0, 1, *range(4, count)):
+        copies[i].start()
     tok_ref, gain_ref, q_ref, kv_ref, rope_ref, len_ref, turn_ref, route_ref, weight_ref = near_refs[
         :OWN
     ]
@@ -487,20 +487,6 @@
         hbm_out=2,
         sems=2,
     )
-    attended, gate, up, lower = lax.optimization_barrier(
-        (attended, expert_gate[0], expert_up[0], expert_down[0])
-    )
-    (own_weights,) = run(
-        weights_body,
-        (jax.ShapeDtypeStruct((3 * width, units), BF16),),
-        gate,
-        up,
-        lower,
-        hbm_in=3,
-        sems=2 + width // units,
-    )
-    swap = [(i, cores - 1 - i) for i in range(cores)]
-    other_weights = lax.ppermute(own_weights, CORE, swap)
     attended_heads = lax.all_to_all(attended, "tp", 0, 0, tiled=True)
     (partials,) = run(
         heads_body,
@@ -525,6 +511,20 @@
         packed_weights,
     )
     packed = packed.reshape(chips, GROUP_CAP, width + EXTRA)
+    packed, gate, up, lower = lax.optimization_barrier(
+        (packed, expert_gate[0], expert_up[0], expert_down[0])
+    )
+    (own_weights,) = run(
+        weights_body,
+        (jax.ShapeDtypeStruct((3 * width, units), BF16),),
+        gate,
+        up,
+        lower,
+        hbm_in=3,
+        sems=2 + width // units,
+    )
+    swap = [(i, cores - 1 - i) for i in range(cores)]
+    other_weights = lax.ppermute(own_weights, CORE, swap)
     arrived = lax.all_to_all(packed, CHIPS, 0, 0, tiled=True)
     (sums,) = run(
         experts_body,

time: 97 us -> 99.9 us (1.030)
  the two profiles are of different devices: /device:TPU:8 before, /device:TPU:1 now
where the time goes in v10:
time: 99.9 us; the launch traced here: 98.3 us
  blocking collectives  78.4 us (78%)
  starting transfers between devices  11.1 us (11%)
  Pallas kernels  8.13 us (8%)
    all_to_all x1, blocking collectives, shards(): arrived = lax.all_to_all(packed, CHIPS, 0, 0, tiled=True)  26.3 us
    all_to_all x1, blocking collectives, shards(): lax.all_to_all(sums.reshape(chips * tp_count, GROUP_CAP, quarter_cols), (...  22.5 us
    ppermute x1, starting transfers between devices, shards(): other_weights = lax.ppermute(own_weights, CORE, swap)  11.1 us
    all_to_all x1, blocking collectives, shards(): latents = lax.all_to_all(both, 'tp', 0, 0, tiled=True)  8.93 us
    all_to_all x1, blocking collectives, shards(): summands = lax.all_to_all(partials, 'tp', 0, 0, tiled=True)  7.39 us
    all_to_all x1, blocking collectives, shards(): queries = lax.all_to_all(send, 'tp', 0, 0, tiled=True)  6.7 us
    all_to_all x1, blocking collectives, shards(): attended_heads = lax.all_to_all(attended, 'tp', 0, 0, tiled=True)  6.65 us
    pallas_call x7, Pallas kernels, run(): pl.pallas_call(body, compiler_params=pltpu.CompilerParams(vmem_limit_byte...  6.36 us
  transfers between devices with their start and end apart: 1, of which 0 were waited for; matrix products, arithmetic and copies ran while one was open for 0% of the time, Pallas kernels for 0%

profile of v10, /device:TPU:1, one launch (start us, length us, event | category | flops | bytes accessed | tf_op | source)
XLA Modules:
  0.0 98.3 jit_solution(2369523746539146341)
XLA Ops:
  0.7 1.8 %shard_map.247 = (bf16[4,32,128]{2,1,0:T(8,128)(2,1)S(1)}, bf16[16,32]{1,0:T(8,128)(2,1)S(1)}, f32[16,16]{1,0:T(8,128)S(1)}, f32[16,16]{1,0:T(8,128)S(1)}, bf16[...) custom-call(bf16[16,1024]{1,0:T(8,128)(2,1)} %tok_ref.1, ...), custom_call_target="tpu_custom_call" | custom-call | flops 2000000 | bytes 1156800 | tf_op jit(solution)/shard_map/pallas_call | solution.py:139
  2.4 8.9 %all_to_all.30.arr_ref = bf16[4,32,128]{2,1,0:T(8,128)(2,1)S(1)} all-to-all(bf16[4,32,128]{2,1,0:T(8,128)(2,1)S(1)} %get-tuple-element.38), channel_id=1, replica_groups=mesh['ep_0'=8,'ep_1'=8,'ep_2'=2,'tp'=4] {'tp'}, dimensions={0} | all-to-all | bytes 65536 | tf_op jit(solution)/shard_map/all_to_all | solution.py:442
  11.4 0.0 copy-start
  11.4 0.0 copy-start.1
  11.4 1.7 %shard_map.248 = (bf16[4,8,544]{2,1,0:T(8,128)(2,1)S(1)}, bf16[16,512]{1,0:T(8,128)(2,1)S(1)}, bf16[16,128]{1,0:T(8,128)(2,1)S(1)}, bf16[4,512,512]{2,1,0:T(8,128)(2,1)S(1)}) custom-call(s32[1]{0:T(128)} %bitcast.8.index_ref, bf16[4,512,512]{2,1,0:T(8,128)(2,1)} %cache_hbm.1, bf16[4,32,128]{2,1,0:T(8,128)(2,1)S(1)} %all_to_all.30.arr_ref, ...), custom_call_target="tpu_custom_call" | custom-call | flops 2000000 | bytes 2464516 | tf_op jit(solution)/shard_map/pallas_call | solution.py:60
  13.0 0.0 copy-start.2
  13.0 0.0 copy-start.3
  13.0 6.7 %all_to_all.31.arr_ref = bf16[4,8,544]{2,1,0:T(8,128)(2,1)S(1)} all-to-all(bf16[4,8,544]{2,1,0:T(8,128)(2,1)S(1)} %get-tuple-element.46), channel_id=1, replica_groups=mesh['ep_0'=8,'ep_1'=8,'ep_2'=2,'tp'=4] {'tp'}, dimensions={0} | all-to-all | bytes 69632 | tf_op jit(solution)/shard_map/all_to_all | solution.py:465
  19.7 1.4 %shard_map.249 = (bf16[4,8,512]{2,1,0:T(8,128)(2,1)S(1)}, bf16[16,128]{1,0:T(8,128)(2,1)}, bf16[16,32]{1,0:T(8,128)(2,1)}) custom-call(s32[1]{0:T(128)} %bitcast.8.index_ref, bf16[4,8,544]{2,1,0:T(8,128)(2,1)S(1)} %all_to_all.31.arr_ref, bf16[4,512,512]{2,1,0:T(8,128)(2,1)S(1)} %get-tuple-element.47.cache_ref, ...), custom_call_target="tpu_custom_call" | custom-call | flops 2000000 | bytes 2352196 | tf_op jit(solution)/shard_map/pallas_call | solution.py:60
  21.2 6.7 %all_to_all.32.arr_ref = bf16[4,8,512]{2,1,0:T(8,128)(2,1)S(1)} all-to-all(bf16[4,8,512]{2,1,0:T(8,128)(2,1)S(1)} %get-tuple-element.55), channel_id=1, replica_groups=mesh['ep_0'=8,'ep_1'=8,'ep_2'=2,'tp'=4] {'tp'}, dimensions={0} | all-to-all | bytes 65536 | tf_op jit(solution)/shard_map/all_to_all | solution.py:490
  27.9 0.0 copy-done
  27.9 0.0 copy-done.1
  27.9 0.4 shard_map.250
  28.2 7.4 %all_to_all.33.arr_ref = bf16[4,16,1024]{2,1,0:T(8,128)(2,1)S(1)} all-to-all(bf16[4,16,1024]{2,1,0:T(8,128)(2,1)S(1)} %shard_map.250), channel_id=1, replica_groups=mesh['ep_0'=8,'ep_1'=8,'ep_2'=2,'tp'=4] {'tp'}, dimensions={0} | all-to-all | bytes 262144 | tf_op jit(solution)/shard_map/all_to_all | solution.py:498
  35.6 0.0 copy-done.2
  35.6 0.0 copy-done.3
  35.6 0.3 shard_map.251
  35.9 1.1 %shard_map.252.own_ref = bf16[3072,128]{1,0:T(8,128)(2,1)S(1)} custom-call(bf16[1024,128]{1,0:T(8,128)(2,1)} %bitcast.21, bf16[1024,128]{1,0:T(8,128)(2,1)} %bitcast.22, bf16[128,1024]{1,0:T(8,128)(2,1)} %bitcast.23), custom_call_target="tpu_custom_call" | custom-call | flops 2000000 | bytes 786432 | tf_op jit(solution)/shard_map/pallas_call | solution.py:60
  37.1 11.1 %collective-permute-start = (bf16[3072,128]{1,0:T(8,128)(2,1)S(1)}, bf16[3072,128]{1,0:T(8,128)(2,1)S(1)}, u32[]{:S(2)}, u32[]{:S(2)}) collective-permute-start(bf16[3072,128]{1,0:T(8,128)(2,1)S(1)} %shard_map.252.own_ref), channel_id=1, source_target_pairs={{0,4},{4,0},{1,5},{5,1},{2,6},{6,2},{3,7},{7,3},{8,12},{12,8},{9,1... | collective-permute-start | bytes 2359304 | tf_op jit(solution)/shard_map/ppermute | solution.py:527
  48.1 26.3 %all_to_all.34.rows_ref = bf16[64,2,1152]{2,1,0:T(2,128)(2,1)S(1)} all-to-all(bf16[64,2,1152]{2,1,0:T(2,128)(2,1)S(1)} %bitcast.19), channel_id=1, replica_groups=mesh['ep_0'=8,'ep_1'=8,'ep_2'=2,'tp'=4] {'ep_1','ep_0'}, dimensions={0} | all-to-all | bytes 589824 | tf_op jit(solution)/shard_map/all_to_all | solution.py:528
  74.4 0.0 collective-permute-done.other_ref
  74.4 0.7 shard_map.253
  75.1 22.5 %all_to_all.35 = bf16[256,2,256]{2,1,0:T(2,128)(2,1)S(1)} all-to-all(bf16[256,2,256]{2,1,0:T(2,128)(2,1)S(1)} %bitcast.17), channel_id=1, replica_groups=mesh['ep_0'=8,'ep_1'=8,'ep_2'=2,'tp'=4] {'ep_1','ep_0','tp'}, dimensions={0} | all-to-all | bytes 524288 | tf_op jit(solution)/shard_map/all_to_all | solution.py:539
  97.5 0.8 shard_map.254
Async XLA Ops:
  11.4 16.5 %copy-start = (bf16[128,1024]{1,0:T(8,128)(2,1)S(1)}, bf16[128,1024]{1,0:T(8,128)(2,1)}, u32[]{:S(2)}) copy-start(bf16[128,1024]{1,0:T(8,128)(2,1)} %out_w_ref.1) | copy-start | bytes 786436
  11.4 16.5 %copy-start.1 = (bf16[512,128]{1,0:T(8,128)(2,1)S(1)}, bf16[512,128]{1,0:T(8,128)(2,1)}, u32[]{:S(2)}) copy-start(bf16[512,128]{1,0:T(8,128)(2,1)} %value_ref.1) | copy-start | bytes 393220
  13.0 22.6 %copy-start.2 = (bf16[16,1024]{1,0:T(8,128)(2,1)S(1)}, bf16[16,1024]{1,0:T(8,128)(2,1)}, u32[]{:S(2)}) copy-start(bf16[16,1024]{1,0:T(8,128)(2,1)} %tok_ref.1) | copy-start | bytes 98308
  13.0 22.6 %copy-start.3 = (f32[1024]{0:T(1024)S(1)}, f32[1024]{0:T(1024)}, u32[]{:S(2)}) copy-start(f32[1024]{0:T(1024)} %param.39) | copy-start | bytes 12292
  37.1 37.3 %collective-permute-start = (bf16[3072,128]{1,0:T(8,128)(2,1)S(1)}, bf16[3072,128]{1,0:T(8,128)(2,1)S(1)}, u32[]{:S(2)}, u32[]{:S(2)}) collective-permute-start(bf16[3072,128]{1,0:T(8,128)(2,1)S(1)} %shard_map.252.own_ref), channel_id=1, source_target_pairs={{0,4},{4,0},{1,5},{5,1},{2,6},{6,2},{3,7},{7,3},{8,12},{12,8},{9,1... | collective-permute-start | bytes 2359304 | tf_op jit(solution)/shard_map/ppermute | solution.py:527
